TPU v7x, 512 devices: a whole 4x4x16 slice. The times are simulated.
512 devices in a mesh: sp: 32 (over z, core), tp: 16 (over y, x).
Axes of the slice: x: 4, y: 4, z: 16, core: 2. Of those that a mesh axis runs over, the one named last changes fastest.
Arguments:
- query_rows: bfloat16 [8192, 2048], P('sp', 'tp'), may hold values from -1000 to 1000
- key_rows: bfloat16 [8192, 256], P('sp'), may hold values from -6 to 6
- value_rows: bfloat16 [8192, 256], P('sp'), may hold values from -6 to 6
- sink_logits: float32 [32], P('tp'), may hold values from 1 to 6
- out_weight: bfloat16 [2048, 2048], P('tp'), may hold values from -0.375 to 0.375
- stream_in: bfloat16 [8192, 2048], P('sp'), may hold values from -6 to 6
- norm_gain: float32 [2048], replicated, may hold values from 0.1 to 1.9
- routes: int32 [8192, 2], P('sp'), may hold values from 0 to 31, all different within a row; in each aligned block of 256 rows (0 to 255, 256 to 511, ...) at most 24 rows name the same one
- route_weights: float32 [8192, 2], P('sp'), may hold values from 0.2 to 1
- gate_weight: bfloat16 [32, 2048, 4096], P('sp', None, 'tp'), may hold values from -0.125 to 0.125
- up_weight: bfloat16 [32, 2048, 4096], P('sp', None, 'tp'), may hold values from -0.125 to 0.125
- down_weight: bfloat16 [32, 4096, 2048], P('sp', 'tp'), may hold values from -0.09375 to 0.09375
Outputs:
- layer_out: bfloat16 [8192, 2048], P(('sp', 'tp'))
Inputs may be any that keep to these rules, and one draw needn't show every extreme that they name: `routes`: each row names 2 different experts. Within the rows of one device (256 aligned rows) no expert is named more than 24 times, a bound that some block reaches.
All inputs are finite; a program needn't handle non-finite values.
Results may differ from a plain program's by a relative error of at most 0.015.
Values may be sent and summed in bfloat16 or wider, within the bound.
No kernel may reach another device: no remote copies, remote signals or barrier semaphores. Data moves between devices by JAX's collectives and lax.ppermute only.
A program may use at most 64 MiB of HBM per device.

v0:
```python
import jax
import jax.numpy as jnp
from jax import lax
from jax.sharding import Mesh
from jax.sharding import PartitionSpec as P

HEAD_DIM = 64
REP = 8
WINDOW = 128
TP = ("tp_0", "tp_1")
SP_TP = ("sp", "tp_0", "tp_1")


norm_eps = 1e-06


def shifted(block, axis, distance):
    devices = range(lax.axis_size(axis))
    route = [(i - distance, i) for i in devices if i - distance in devices]
    return lax.ppermute(block, axis, route)


def cut_along(shard, dim, count):
    before, after = (shard.shape[:dim], shard.shape[dim + 1 :])
    return jnp.moveaxis(shard.reshape(*before, count, -1, *after), dim, 0)


def sum_at_owner(shard, axis, dim):
    pieces = cut_along(shard, dim, lax.axis_size(axis))
    arrived = lax.all_to_all(pieces, axis, split_axis=0, concat_axis=0, tiled=True)
    return arrived.astype(jnp.float32).sum(axis=0)


def laid_out(pieces, dim):
    lengths = list(pieces.shape[1:])
    lengths[dim] *= pieces.shape[0]
    return jnp.moveaxis(pieces, 0, dim).reshape(lengths)


def sent_to_all(shard, axis):
    copies = jnp.broadcast_to(shard, (lax.axis_size(axis), *shard.shape))
    return lax.all_to_all(copies, axis, split_axis=0, concat_axis=0, tiled=True)


def gathered_copies(shard, axis, dim):
    return laid_out(sent_to_all(shard, axis), dim)


def gathered_by_axis(shard, axes, dim):
    result = shard
    for number in range(len(axes) - 1, -1, -1):
        result = lax.all_gather(result, axes[number], axis=dim, tiled=True)
    return result


def piece_ends(length, count):
    hop = length // count
    if hop >= 8:
        hop -= hop % 8
    return [hop * k for k in range(1, count)]


def exchange_in_pieces(shard, axis, pieces, split_dim, concat_dim):
    blocks = cut_along(shard, split_dim, lax.axis_size(axis))
    split_at = max(range(1, max(2, blocks.ndim - 1)), key=lambda d: blocks.shape[d])
    finished = []
    for slab in jnp.split(blocks, piece_ends(blocks.shape[split_at], pieces), axis=split_at):
        if slab.size:
            finished.append(lax.all_to_all(slab, axis, split_axis=0, concat_axis=0, tiled=True))
    return laid_out(jnp.concatenate(finished, axis=split_at), concat_dim)


def rms_scale(stream, norm_gain):
    values = stream.astype(jnp.float32)
    scaled = values * lax.rsqrt(jnp.mean(values * values, axis=-1, keepdims=True) + norm_eps)
    return (scaled * norm_gain).astype(jnp.bfloat16)


def slot_tables(routes, experts_n, slot_cap):
    flat_ids = routes.reshape(-1)
    onehot = (flat_ids[:, None] == jnp.arange(experts_n, dtype=jnp.int32)[None, :]).astype(
        jnp.int32
    )
    before = jnp.cumsum(onehot, axis=0) - onehot
    targets = flat_ids * slot_cap + jnp.sum(before * onehot, axis=1)
    pair_token = jnp.arange(flat_ids.shape[0], dtype=jnp.int32) // routes.shape[1]
    slot_token = jnp.zeros((experts_n * slot_cap,), jnp.int32).at[targets].set(pair_token)
    slot_live = jnp.zeros((experts_n * slot_cap,), jnp.int32).at[targets].set(1)
    return (targets, slot_token, slot_live)


def per_device(
    query_rows,
    key_rows,
    value_rows,
    sink_logits,
    out_weight,
    stream_in,
    norm_gain,
    routes,
    route_weights,
    gate_weight,
    up_weight,
    down_weight,
):
    tok_count = query_rows.shape[0]
    local_heads = query_rows.shape[1] // HEAD_DIM
    tp_index = lax.axis_index(TP)
    kv_group = tp_index * local_heads // REP
    own_keys = lax.dynamic_slice_in_dim(key_rows, kv_group * HEAD_DIM, HEAD_DIM, 1)
    own_values = lax.dynamic_slice_in_dim(value_rows, kv_group * HEAD_DIM, HEAD_DIM, 1)
    prior_keys, prior_values = shifted(
        (own_keys[tok_count - WINDOW :], own_values[tok_count - WINDOW :]), "sp", 1
    )
    key_block = jnp.concatenate([prior_keys, own_keys], axis=0)
    value_block = jnp.concatenate([prior_values, own_values], axis=0)
    offset = lax.axis_index("sp") * tok_count
    query_pos = offset + jnp.arange(tok_count, dtype=jnp.int32)
    key_pos = offset - WINDOW + jnp.arange(tok_count + WINDOW, dtype=jnp.int32)
    distance = query_pos[:, None] - key_pos[None, :]
    allowed = (distance >= 0) & (distance < WINDOW) & (key_pos >= 0)[None, :]
    queries = query_rows.reshape(tok_count, local_heads, HEAD_DIM)
    scores = jnp.einsum(
        "qhd,kd->hqk", queries, key_block, preferred_element_type=jnp.float32
    ) * HEAD_DIM ** (-0.5)
    scores = jnp.where(allowed[None], scores, -1e30)
    sink_col = sink_logits.reshape(local_heads, 1, 1)
    row_peak = jnp.maximum(jnp.max(scores, axis=-1, keepdims=True), sink_col)
    exp_terms = jnp.exp(scores - row_peak)
    denom_sum = jnp.sum(exp_terms, axis=-1, keepdims=True) + jnp.exp(sink_col - row_peak)
    attn_probs = (exp_terms / denom_sum).astype(jnp.bfloat16)
    attended = jnp.einsum(
        "hqk,kd->qhd", attn_probs, value_block, preferred_element_type=jnp.float32
    )
    attended = attended.astype(jnp.bfloat16).reshape(tok_count, local_heads * HEAD_DIM)
    row_share = tok_count // lax.axis_size(TP)
    projected = sum_at_owner(
        jnp.dot(attended, out_weight, preferred_element_type=jnp.float32).astype(jnp.bfloat16),
        TP,
        0,
    )
    own_input = lax.dynamic_slice_in_dim(stream_in, tp_index * row_share, row_share, 0)
    own_stream = (own_input.astype(jnp.float32) + projected).astype(jnp.bfloat16)
    normed_all = gathered_copies(rms_scale(own_stream, norm_gain), TP, 0)
    experts_n = lax.axis_size("sp")
    top_count = routes.shape[1]
    slot_cap = 3 * tok_count * top_count // (2 * experts_n)
    targets, slot_token, slot_live = slot_tables(routes, experts_n, slot_cap)
    width_share = normed_all.shape[1] // lax.axis_size(TP)
    columns = lax.dynamic_slice_in_dim(normed_all, tp_index * width_share, width_share, 1)
    outgoing = jnp.where(slot_live[:, None] > 0, columns[slot_token], jnp.zeros((), jnp.bfloat16))
    outgoing = outgoing.reshape(experts_n, slot_cap, width_share)
    arrived = lax.all_to_all(outgoing, "sp", split_axis=0, concat_axis=0, tiled=True)
    arrived = gathered_by_axis(arrived, TP, 2)
    sources = arrived.shape[0]
    item_count = arrived.shape[1]
    flat_rows = arrived.reshape(sources * item_count, arrived.shape[2])
    gate_act = jnp.dot(flat_rows, gate_weight[0], preferred_element_type=jnp.float32)
    up_act = jnp.dot(flat_rows, up_weight[0], preferred_element_type=jnp.float32)
    hidden = (jax.nn.silu(gate_act) * up_act).astype(jnp.bfloat16)
    partial_value = jnp.dot(hidden, down_weight[0], preferred_element_type=jnp.float32).astype(
        jnp.bfloat16
    )
    pieces = exchange_in_pieces(partial_value[None], TP, 2, 2, 0)
    summed = jnp.sum(pieces.astype(jnp.float32), axis=0)
    summed = summed.reshape(sources, item_count, summed.shape[1])
    returned = lax.all_to_all(
        summed.astype(jnp.bfloat16), "sp", split_axis=0, concat_axis=0, tiled=True
    ).astype(summed.dtype)
    returned_flat = returned.reshape(experts_n * slot_cap, returned.shape[2])
    pair_weights = route_weights.reshape(-1)
    chosen = returned_flat[targets] * pair_weights[:, None]
    moe_columns = jnp.sum(chosen.reshape(tok_count, top_count, chosen.shape[1]), axis=1)
    moe_rows = lax.all_to_all(
        moe_columns.astype(jnp.bfloat16), TP, split_axis=0, concat_axis=1, tiled=True
    ).astype(moe_columns.dtype)
    return (own_stream.astype(jnp.float32) + moe_rows).astype(jnp.bfloat16)


def solution(mesh):
    finer = Mesh(mesh.devices.reshape(mesh.shape["sp"], 4, 4), ("sp", "tp_0", "tp_1"))
    placed = (
        P("sp", TP),
        P("sp", None),
        P("sp", None),
        P(TP),
        P(TP, None),
        P("sp", None),
        P(),
        P("sp", None),
        P("sp", None),
        P("sp", None, TP),
        P("sp", None, TP),
        P("sp", TP, None),
    )
    return jax.shard_map(
        per_device, mesh=finer, in_specs=placed, out_specs=P(SP_TP, None), check_vma=False
    )
```

profile of v0, /device:TPU:2, one launch (start us, length us, event | category | flops | bytes accessed | tf_op | source)
XLA Modules:
  0.0 275.1 jit_solution(10418790207975938657)
XLA Ops:
  6.5 1.0 constant_dynamic-slice_fusion.1
  7.7 1.7 collective-permute-start.1
  9.4 0.9 constant_dynamic-slice_fusion.2
  10.5 4.1 %collective-permute-start = (bf16[128,64]{0,1:T(8,128)(2,1)S(1)}, bf16[128,64]{0,1:T(8,128)(2,1)S(1)}, u32[]{:S(2)}, u32[]{:S(2)}) collective-permute-start(bf16[128,64]{0,1:T(8,128)(2,1)S(1)} %slice.20), channel_id=1, source_target_pairs={{0,16},{16,32},{32,48},{48,64},{64,80},{80,96},{96,112},{112,128},... | collective-permute-start | bytes 49160 | tf_op jit(solution)/shard_map/ppermute | solution.py:20
  14.8 0.9 copy.39
  16.1 0.7 broadcast_maximum_fusion
  16.9 0.7 exponential_add_fusion
  18.0 1.4 convolution_convert_fusion.1
  19.4 7.5 %all-to-all-start = ((bf16[16,16,2048]{2,1,0:T(8,128)(2,1)}), bf16[16,16,2048]{2,1,0:T(8,128)(2,1)S(1)}, u32[]{:S(2)}, u32[]{:S(2)}) async-start(bf16[16,16,2048]{2,1,0:T(8,128)(2,1)} %bitcast.6), calls=%async_computation | async-start | bytes 2097152 | tf_op jit(solution)/shard_map/all_to_all | solution.py:30
  27.3 1.2 reduce-window.6
  29.1 13.8 %all-to-all-done = bf16[16,16,2048]{2,1,0:T(8,128)(2,1)S(1)} async-done(((bf16[16,16,2048]{2,1,0:T(8,128)(2,1)}), bf16[16,16,2048]{2,1,0:T(8,128)(2,1)S(1)}, u32[]{:S(2)}, u32[]{:S(2)}) %all-to-all-start) | async-done | bytes 1048608 | tf_op jit(solution)/shard_map/all_to_all | solution.py:30
  43.0 1.0 fusion.14
  44.1 1.1 broadcast_in_dim.53
  45.2 5.3 %all-to-all-start.1 = ((bf16[16,16,2048]{2,1,0:T(8,128)(2,1)}), bf16[16,16,2048]{2,1,0:T(8,128)(2,1)S(1)}, u32[]{:S(2)}, u32[]{:S(2)}) async-start(bf16[16,16,2048]{2,1,0:T(8,128)(2,1)} %broadcast_in_dim.53), calls=%async_computation.1 | async-start | bytes 2097152 | tf_op jit(solution)/shard_map/all_to_all | solution.py:42
  50.7 2.4 scatter_custom_fusion.1
  53.2 2.4 scatter_custom_fusion
  55.8 10.2 %all-to-all-done.1 = bf16[16,16,2048]{2,1,0:T(8,128)(2,1)S(1)} async-done(((bf16[16,16,2048]{2,1,0:T(8,128)(2,1)}), bf16[16,16,2048]{2,1,0:T(8,128)(2,1)S(1)}, u32[]{:S(2)}, u32[]{:S(2)}) %all-to-all-start.1) | async-done | bytes 1048608 | tf_op jit(solution)/shard_map/all_to_all | solution.py:42
  66.0 1.9 gather_fusion
  68.1 34.2 %all_to_all.40 = bf16[32,24,128]{2,1,0:T(8,128)(2,1)S(1)} all-to-all(bf16[32,24,128]{2,1,0:T(8,128)(2,1)S(1)} %broadcast_select_fusion), channel_id=1, replica_groups=mesh['sp'=32,'tp_0'=4,'tp_1'=4] {'sp'}, dimensions={0} | all-to-all | bytes 393216 | tf_op jit(solution)/shard_map/all_to_all | solution.py:153
  102.2 18.0 %all_gather.6 = bf16[32,24,512]{2,1,0:T(8,128)(2,1)} all-gather(bf16[32,24,128]{2,1,0:T(8,128)(2,1)S(1)} %all_to_all.40), channel_id=1, replica_groups=mesh['sp'=32,'tp_0'=4,'tp_1'=4] {'tp_1'}, dimensions={2}, use_global_device_ids=true | all-gather | bytes 983040 | tf_op jit(solution)/shard_map/all_gather | solution.py:52
  120.2 35.3 %all-gather.2.cloned.1.call-done = bf16[32,24,2048]{2,1,0:T(8,128)(2,1)} async-done(((bf16[32,24,512]{2,1,0:T(8,128)(2,1)}), bf16[32,24,2048]{2,1,0:T(8,128)(2,1)}) %all-gather.2.cloned.1.call-update) | async-done | bytes 3145744 | tf_op jit(solution)/shard_map/all_gather | solution.py:52
  155.5 3.2 %fusion.6 = f32[768,256]{1,0:T(8,128)S(1)} fusion(bf16[768,2048]{1,0:T(8,128)(2,1)} %bitcast.88, bf16[1,2048,256]{2,1,0:T(8,128)(2,1)} %param.21), kind=kOutput, calls=%fused_computation.18 | convolution fusion | flops 805306368 | bytes 4980736 | tf_op jit(solution)/shard_map/dot_general | solution.py:158
  158.7 6.9 %fusion = bf16[96,8,16,128]{3,1,2,0:T(8,128)(2,1)} fusion(bf16[1,256,2048]{2,1,0:T(8,128)(2,1)S(1)} %copy-done, bf16[768,2048]{1,0:T(8,128)(2,1)} %bitcast.89, bf16[1,2048,256]{2,1,0:T(8,128)(2,1)S(1)} %copy-done.5, f32[768,256]{1,0:T(8,128)S(1)} %fusion.6), kind=kOutput, calls=%fused_computation.9 | convolution fusion | flops 1613365248 | bytes 9175040 | tf_op jit(solution)/shard_map/dot_general | solution.py:161
  165.6 2.9 %copy.53 = bf16[96,8,16,128]{3,2,1,0:T(8,128)(2,1)S(1)} copy(bf16[96,8,16,128]{3,1,2,0:T(8,128)(2,1)} %fusion) | data formatting | bytes 6291456
  168.5 0.8 copy.57
  169.7 27.2 %all_to_all.41 = bf16[16,1,384,128]{3,2,1,0:T(8,128)(2,1)S(1)} all-to-all(bf16[16,1,384,128]{3,2,1,0:T(8,128)(2,1)S(1)} %get-tuple-element.7), channel_id=1, replica_groups=mesh['sp'=32,'tp_0'=4,'tp_1'=4] {'tp_0','tp_1'}, dimensions={0} | all-to-all | bytes 3145728 | tf_op jit(solution)/shard_map/all_to_all | solution.py:69
  196.9 25.0 %all_to_all.42 = bf16[16,1,384,128]{3,2,1,0:T(8,128)(2,1)S(1)} all-to-all(bf16[16,1,384,128]{3,2,1,0:T(8,128)(2,1)S(1)} %get-tuple-element.8), channel_id=1, replica_groups=mesh['sp'=32,'tp_0'=4,'tp_1'=4] {'tp_0','tp_1'}, dimensions={0} | all-to-all | bytes 3145728 | tf_op jit(solution)/shard_map/all_to_all | solution.py:69
  221.9 1.1 maximum_reduce_fusion
  223.0 12.6 %all-to-all-start.5 = ((bf16[32,24,128]{2,1,0:T(8,128)(2,1)}), bf16[32,24,128]{2,1,0:T(8,128)(2,1)S(1)}, u32[]{:S(2)}, u32[]{:S(2)}) async-start(bf16[32,24,128]{2,1,0:T(8,128)(2,1)} %bitcast.17), calls=%async_computation.5 | async-start | bytes 393216 | tf_op jit(solution)/shard_map/all_to_all | solution.py:167
  235.8 19.8 %all-to-all-done.5 = bf16[32,24,128]{2,1,0:T(8,128)(2,1)S(1)} async-done(((bf16[32,24,128]{2,1,0:T(8,128)(2,1)}), bf16[32,24,128]{2,1,0:T(8,128)(2,1)S(1)}, u32[]{:S(2)}, u32[]{:S(2)}) %all-to-all-start.5) | async-done | bytes 196640 | tf_op jit(solution)/shard_map/all_to_all | solution.py:167
  255.6 1.0 gather_fusion.1
  257.1 10.5 %all_to_all.43 = bf16[16,16,128]{2,1,0:T(8,128)(2,1)S(1)} all-to-all(bf16[16,16,128]{2,1,0:T(8,128)(2,1)S(1)} %bitcast.81), channel_id=1, replica_groups=mesh['sp'=32,'tp_0'=4,'tp_1'=4] {'tp_0','tp_1'}, dimensions={0} | all-to-all | bytes 131072 | tf_op jit(solution)/shard_map/all_to_all | solution.py:174
  (56 shorter events, 4.3 us)
Async XLA Ops:
  6.5 152.1 %copy-start = (bf16[1,256,2048]{2,1,0:T(8,128)(2,1)S(1)}, bf16[1,256,2048]{2,1,0:T(8,128)(2,1)}, u32[]{:S(2)}) copy-start(bf16[1,256,2048]{2,1,0:T(8,128)(2,1)} %param.23) | copy-start | bytes 3145732
  6.5 11.4 %copy-start.1 = (bf16[128,2048]{1,0:T(8,128)(2,1)S(1)}, bf16[128,2048]{1,0:T(8,128)(2,1)}, u32[]{:S(2)}) copy-start(bf16[128,2048]{1,0:T(8,128)(2,1)} %param.16) | copy-start | bytes 1572868
  7.7 8.1 %collective-permute-start.1 = (bf16[128,64]{0,1:T(8,128)(2,1)S(1)}, bf16[128,64]{0,1:T(8,128)(2,1)S(1)}, u32[]{:S(2)}, u32[]{:S(2)}) collective-permute-start(bf16[128,64]{0,1:T(8,128)(2,1)S(1)} %slice.21), channel_id=1, source_target_pairs={{0,16},{16,32},{32,48},{48,64},{64,80},{80,96},{96,112},{112,128},... | collective-permute-start | bytes 49160 | tf_op jit(solution)/shard_map/ppermute | solution.py:20
  10.5 7.2 %collective-permute-start = (bf16[128,64]{0,1:T(8,128)(2,1)S(1)}, bf16[128,64]{0,1:T(8,128)(2,1)S(1)}, u32[]{:S(2)}, u32[]{:S(2)}) collective-permute-start(bf16[128,64]{0,1:T(8,128)(2,1)S(1)} %slice.20), channel_id=1, source_target_pairs={{0,16},{16,32},{32,48},{48,64},{64,80},{80,96},{96,112},{112,128},... | collective-permute-start | bytes 49160 | tf_op jit(solution)/shard_map/ppermute | solution.py:20
  17.7 9.2 %copy-start.2 = (s32[256,2]{0,1:T(2,128)S(1)}, s32[256,2]{0,1:T(2,128)}, u32[]{:S(2)}) copy-start(s32[256,2]{0,1:T(2,128)} %param.19) | copy-start | bytes 6148
  17.9 26.1 %copy-start.3 = (f32[2048]{0:T(1024)S(1)}, f32[2048]{0:T(1024)}, u32[]{:S(2)}) copy-start(f32[2048]{0:T(1024)} %param.18) | copy-start | bytes 24580
  19.4 23.5 %all-to-all-start = ((bf16[16,16,2048]{2,1,0:T(8,128)(2,1)}), bf16[16,16,2048]{2,1,0:T(8,128)(2,1)S(1)}, u32[]{:S(2)}, u32[]{:S(2)}) async-start(bf16[16,16,2048]{2,1,0:T(8,128)(2,1)} %bitcast.6), calls=%async_computation | async-start | bytes 2097152 | tf_op jit(solution)/shard_map/all_to_all | solution.py:30
  45.2 20.8 %all-to-all-start.1 = ((bf16[16,16,2048]{2,1,0:T(8,128)(2,1)}), bf16[16,16,2048]{2,1,0:T(8,128)(2,1)S(1)}, u32[]{:S(2)}, u32[]{:S(2)}) async-start(bf16[16,16,2048]{2,1,0:T(8,128)(2,1)} %broadcast_in_dim.53), calls=%async_computation.1 | async-start | bytes 2097152 | tf_op jit(solution)/shard_map/all_to_all | solution.py:42
  50.6 105.0 %all-gather.2.cloned.1.call-start = ((), (), s32[]{:S(2)}) async-start(), calls=%async_computation.7 | async-start | bytes 3932160 | tf_op jit(solution)/shard_map/all_gather | solution.py:52
  120.2 38.5 %copy-start.5 = (bf16[1,2048,256]{2,1,0:T(8,128)(2,1)S(1)}, bf16[1,2048,256]{2,1,0:T(8,128)(2,1)}, u32[]{:S(2)}) copy-start(bf16[1,2048,256]{2,1,0:T(8,128)(2,1)} %param.22) | copy-start | bytes 3145732
  196.9 38.7 %copy-start.4 = (f32[256,2]{0,1:T(2,128)S(1)}, f32[256,2]{0,1:T(2,128)}, u32[]{:S(2)}) copy-start(f32[256,2]{0,1:T(2,128)} %param.20) | copy-start | bytes 6148
  223.0 32.6 %all-to-all-start.5 = ((bf16[32,24,128]{2,1,0:T(8,128)(2,1)}), bf16[32,24,128]{2,1,0:T(8,128)(2,1)S(1)}, u32[]{:S(2)}, u32[]{:S(2)}) async-start(bf16[32,24,128]{2,1,0:T(8,128)(2,1)} %bitcast.17), calls=%async_computation.5 | async-start | bytes 393216 | tf_op jit(solution)/shard_map/all_to_all | solution.py:167
Sparse Core Ops, SparseCore 0:
  120.4 35.1 all-gather.1
where the time goes:
time: 276 us; the launch traced here: 275 us
  blocking collectives  115 us (42%)
  waiting for transfers between devices  79.1 us (29%)
  starting transfers between devices  31.3 us (11%)
  local copies, waits for them, and re-layouts  17.3 us (6%)
  between operations  13.8 us (5%)
  matrix products  12.1 us (4%)
  other arithmetic  6.72 us (2%)
    all_to_all x2, blocking collectives, exchange_in_pieces(): lax.all_to_all(slab, axis, split_axis=0, concat_axis=0, tiled=True)  52.2 us
    all_gather x1, waiting for transfers between devices, gathered_by_axis(): result = lax.all_gather(result, axes[number], axis=dim, tiled=True)  35.3 us
    all_to_all x1, blocking collectives, per_device(): lax.all_to_all(outgoing, 'sp', split_axis=0, concat_axis=0, tiled=True)  34.2 us
    all_to_all x1, waiting for transfers between devices, per_device(): lax.all_to_all(summed.astype(jnp.bfloat16), 'sp', split_axis=0, concat_ax...  19.8 us
    all_gather x1, blocking collectives, gathered_by_axis(): result = lax.all_gather(result, axes[number], axis=dim, tiled=True)  18 us
    all_to_all x1, waiting for transfers between devices, sum_at_owner(): lax.all_to_all(pieces, axis, split_axis=0, concat_axis=0, tiled=True)  13.8 us
    all_to_all x1, starting transfers between devices, per_device(): lax.all_to_all(summed.astype(jnp.bfloat16), 'sp', split_axis=0, concat_ax...  12.6 us
    all_to_all x1, blocking collectives, per_device(): lax.all_to_all(moe_columns.astype(jnp.bfloat16), TP, split_axis=0, concat...  10.5 us
  transfers between devices with their start and end apart: 6, of which 4 were waited for; matrix products, arithmetic and copies ran while one was open for 4% of the time, Pallas kernels for 0%

commit v1 on v0

--- a/solution.py
+++ b/solution.py
@@ -133,25 +133,23 @@
         "hqk,kd->qhd", attn_probs, value_block, preferred_element_type=jnp.float32
     )
     attended = attended.astype(jnp.bfloat16).reshape(tok_count, local_heads * HEAD_DIM)
-    row_share = tok_count // lax.axis_size(TP)
+    width = out_weight.shape[1]
+    width_share = width // lax.axis_size(TP)
     projected = sum_at_owner(
         jnp.dot(attended, out_weight, preferred_element_type=jnp.float32).astype(jnp.bfloat16),
         TP,
-        0,
+        1,
     )
-    own_input = lax.dynamic_slice_in_dim(stream_in, tp_index * row_share, row_share, 0)
-    own_stream = (own_input.astype(jnp.float32) + projected).astype(jnp.bfloat16)
-    normed_all = gathered_copies(rms_scale(own_stream, norm_gain), TP, 0)
+    own_input = lax.dynamic_slice_in_dim(stream_in, tp_index * width_share, width_share, 1)
+    columns = (own_input.astype(jnp.float32) + projected).astype(jnp.bfloat16)
     experts_n = lax.axis_size("sp")
     top_count = routes.shape[1]
     slot_cap = 3 * tok_count * top_count // (2 * experts_n)
     targets, slot_token, slot_live = slot_tables(routes, experts_n, slot_cap)
-    width_share = normed_all.shape[1] // lax.axis_size(TP)
-    columns = lax.dynamic_slice_in_dim(normed_all, tp_index * width_share, width_share, 1)
     outgoing = jnp.where(slot_live[:, None] > 0, columns[slot_token], jnp.zeros((), jnp.bfloat16))
     outgoing = outgoing.reshape(experts_n, slot_cap, width_share)
     arrived = lax.all_to_all(outgoing, "sp", split_axis=0, concat_axis=0, tiled=True)
-    arrived = gathered_by_axis(arrived, TP, 2)
+    arrived = rms_scale(gathered_copies(arrived, TP, 2), norm_gain)
     sources = arrived.shape[0]
     item_count = arrived.shape[1]
     flat_rows = arrived.reshape(sources * item_count, arrived.shape[2])
@@ -161,7 +159,7 @@
     partial_value = jnp.dot(hidden, down_weight[0], preferred_element_type=jnp.float32).astype(
         jnp.bfloat16
     )
-    pieces = exchange_in_pieces(partial_value[None], TP, 2, 2, 0)
+    pieces = exchange_in_pieces(partial_value[None], TP, 1, 2, 0)
     summed = jnp.sum(pieces.astype(jnp.float32), axis=0)
     summed = summed.reshape(sources, item_count, summed.shape[1])
     returned = lax.all_to_all(
@@ -171,10 +169,8 @@
     pair_weights = route_weights.reshape(-1)
     chosen = returned_flat[targets] * pair_weights[:, None]
     moe_columns = jnp.sum(chosen.reshape(tok_count, top_count, chosen.shape[1]), axis=1)
-    moe_rows = lax.all_to_all(
-        moe_columns.astype(jnp.bfloat16), TP, split_axis=0, concat_axis=1, tiled=True
-    ).astype(moe_columns.dtype)
-    return (own_stream.astype(jnp.float32) + moe_rows).astype(jnp.bfloat16)
+    out_columns = (columns.astype(jnp.float32) + moe_columns).astype(jnp.bfloat16)
+    return lax.all_to_all(out_columns, TP, split_axis=0, concat_axis=1, tiled=True)
 
 
 def solution(mesh):

time: 276 us -> 223 us (0.81)
  waiting for transfers between devices: 79.1 us -> 30.6 us
  blocking collectives: 115 us -> 130 us
  starting transfers between devices: 31.3 us -> 17.3 us
  between operations: 13.8 us -> 0.4 us
  local copies, waits for them, and re-layouts: 17.3 us -> 24.5 us
  matrix products: 12.1 us -> 8.91 us
  other arithmetic: 6.72 us -> 9.61 us
    all_to_all x1 -> x2, blocking collectives: 10.5 us -> 52.7 us  [the longest x1 42.4 us: sent_to_all(): return lax.all_to_all(copies, axis, split_axis=0, concat_axis=0, tiled=True)]
    all_gather x1 -> x0, waiting for transfers between devices: 35.3 us -> none  [gathered_by_axis(): result = lax.all_gather(result, axes[number], axis=dim, tiled=True)]
    all_gather x1 -> x0, blocking collectives: 18 us -> none  [gathered_by_axis(): result = lax.all_gather(result, axes[number], axis=dim, tiled=True)]
    all_to_all x1 -> x0, waiting for transfers between devices: 10.2 us -> none  [sent_to_all(): return lax.all_to_all(copies, axis, split_axis=0, concat_axis=0, tiled=True)]
    all_to_all x2 -> x1, blocking collectives: 52.2 us -> 43.4 us  [exchange_in_pieces(): lax.all_to_all(slab, axis, split_axis=0, concat_axis=0, tiled=True)]
    all_to_all x1, starting transfers between devices: 12.6 us -> 3.87 us  [per_device(): lax.all_to_all(summed.astype(jnp.bfloat16), 'sp', split_axis=0, concat_ax...]
    all_to_all x1 -> x0, starting transfers between devices: 5.35 us -> none  [sent_to_all(): return lax.all_to_all(copies, axis, split_axis=0, concat_axis=0, tiled=True)]
    convert_element_type x0 -> x1, local copies, waits for them, and re-layouts: none -> 3.65 us  [rms_scale(): return (scaled * norm_gain).astype(jnp.bfloat16)]
  transfers between devices with their start and end apart: 6 -> 4, of which waited for: 4 -> 2; matrix products, arithmetic and copies ran while one was open for 4% -> 5% of each run, Pallas kernels for 0% -> 0%
where the time goes in v1:
time: 223 us; the launch traced here: 222 us
  blocking collectives  130 us (58%)
  waiting for transfers between devices  30.6 us (14%)
  local copies, waits for them, and re-layouts  24.5 us (11%)
  starting transfers between devices  17.3 us (8%)
  other arithmetic  9.61 us (4%)
  matrix products  8.91 us (4%)
    all_to_all x1, blocking collectives, exchange_in_pieces(): lax.all_to_all(slab, axis, split_axis=0, concat_axis=0, tiled=True)  43.4 us
    all_to_all x1, blocking collectives, sent_to_all(): return lax.all_to_all(copies, axis, split_axis=0, concat_axis=0, tiled=True)  42.4 us
    all_to_all x1, blocking collectives, per_device(): lax.all_to_all(outgoing, 'sp', split_axis=0, concat_axis=0, tiled=True)  34.4 us
    all_to_all x1, waiting for transfers between devices, per_device(): lax.all_to_all(summed.astype(jnp.bfloat16), 'sp', split_axis=0, concat_ax...  19.8 us
    all_to_all x1, waiting for transfers between devices, sum_at_owner(): lax.all_to_all(pieces, axis, split_axis=0, concat_axis=0, tiled=True)  10.8 us
    all_to_all x1, blocking collectives, per_device(): lax.all_to_all(out_columns, TP, split_axis=0, concat_axis=1, tiled=True)  10.2 us
    all_to_all x1, starting transfers between devices, sum_at_owner(): lax.all_to_all(pieces, axis, split_axis=0, concat_axis=0, tiled=True)  7.48 us
    dot_general x1, matrix products, per_device(): jnp.dot(hidden, down_weight[0], preferred_element_type=jnp.float32)  6.92 us
  transfers between devices with their start and end apart: 4, of which 2 were waited for; matrix products, arithmetic and copies ran while one was open for 5% of the time, Pallas kernels for 0%

profile of v1, /device:TPU:2, one launch (start us, length us, event | category | flops | bytes accessed | tf_op | source)
XLA Modules:
  0.0 221.7 jit_solution(14790796120273187725)
XLA Ops:
  0.0 1.0 constant_dynamic-slice_fusion
  1.1 1.7 collective-permute-start.1
  2.9 0.9 constant_dynamic-slice_fusion.1
  3.9 4.2 %collective-permute-start = (bf16[128,64]{0,1:T(8,128)(2,1)S(1)}, bf16[128,64]{0,1:T(8,128)(2,1)S(1)}, u32[]{:S(2)}, u32[]{:S(2)}) collective-permute-start(bf16[128,64]{0,1:T(8,128)(2,1)S(1)} %slice.20), channel_id=1, source_target_pairs={{0,16},{16,32},{32,48},{48,64},{64,80},{80,96},{96,112},{112,128},... | collective-permute-start | bytes 49160 | tf_op jit(solution)/shard_map/ppermute | solution.py:20
  8.2 0.8 copy.35
  9.1 0.7 broadcast_multiply_fusion
  9.9 1.2 reduce-window.6
  11.6 0.9 copy.31
  13.2 0.7 broadcast_maximum_fusion
  14.9 1.3 copy.69
  16.2 7.5 %all-to-all-start = ((bf16[16,256,128]{2,1,0:T(8,128)(2,1)}), bf16[16,256,128]{2,1,0:T(8,128)(2,1)S(1)}, u32[]{:S(2)}, u32[]{:S(2)}) async-start(bf16[16,256,128]{2,1,0:T(8,128)(2,1)} %bitcast.94), calls=%async_computation | async-start | bytes 2097152 | tf_op jit(solution)/shard_map/all_to_all | solution.py:30
  23.8 2.4 %scatter_custom_fusion.1 = s32[768]{0:T(1024)S(1)} fusion(s32[512]{0:T(512)S(1)} %bitcast.105, s32[512]{0:T(512)S(1)} %add_select_fusion, s32[]{:T(128)} %constant.30.clone.1), kind=kCustom, calls=%fused_computation.72 | custom fusion | bytes 3076 | tf_op jit(solution)/shard_map/scatter | solution.py:87
  26.2 2.4 %scatter_custom_fusion = s32[768]{0:T(1024)S(1)} fusion(s32[512]{0:T(512)S(1)} %bitcast.106, s32[512]{0:T(512)S(1)} %broadcast.197, s32[]{:T(128)} %constant.30.clone.1), kind=kCustom, calls=%fused_computation.75 | custom fusion | bytes 3076 | tf_op jit(solution)/shard_map/scatter | solution.py:88
  28.8 10.8 %all-to-all-done = bf16[16,256,128]{2,1,0:T(8,128)(2,1)S(1)} async-done(((bf16[16,256,128]{2,1,0:T(8,128)(2,1)}), bf16[16,256,128]{2,1,0:T(8,128)(2,1)S(1)}, u32[]{:S(2)}, u32[]{:S(2)}) %all-to-all-start) | async-done | bytes 1048608 | tf_op jit(solution)/shard_map/all_to_all | solution.py:30
  39.7 0.9 add_convert_fusion.1
  40.6 1.9 gather_fusion
  42.7 34.4 %all_to_all.44 = bf16[32,24,128]{2,1,0:T(8,128)(2,1)S(1)} all-to-all(bf16[32,24,128]{2,1,0:T(8,128)(2,1)S(1)} %broadcast_select_fusion), channel_id=1, replica_groups=mesh['sp'=32,'tp_0'=4,'tp_1'=4] {'sp'}, dimensions={0} | all-to-all | bytes 393216 | tf_op jit(solution)/shard_map/all_to_all | solution.py:151
  77.7 42.4 %all_to_all.45 = bf16[16,32,24,128]{3,2,1,0:T(8,128)(2,1)S(1)} all-to-all(bf16[16,32,24,128]{3,2,1,0:T(8,128)(2,1)S(1)} %broadcast_in_dim.55), channel_id=1, replica_groups=mesh['sp'=32,'tp_0'=4,'tp_1'=4] {'tp_0','tp_1'}, dimensions={0} | all-to-all | bytes 6291456 | tf_op jit(solution)/shard_map/all_to_all | solution.py:42
  120.1 0.7 fusion
  120.8 1.1 fusion.3
  121.9 3.6 %copy.38 = bf16[32,24,16,128]{3,2,1,0:T(8,128)(2,1)S(1)} copy(bf16[32,24,16,128]{3,1,0,2:T(8,128)(2,1)S(1)} %fusion.3) | data formatting | bytes 6291456 | tf_op jit(solution)/shard_map/convert_element_type | solution.py:76
  125.6 1.7 copy-done.1
  127.2 1.0 fusion.6
  128.5 6.9 %fusion.10 = bf16[96,8,16,128]{3,1,2,0:T(8,128)(2,1)} fusion(bf16[1,256,2048]{2,1,0:T(8,128)(2,1)S(1)} %copy-done, bf16[96,8,16,128]{3,2,1,0:T(8,128)(2,1)} %bitcast.98, bf16[1,2048,256]{2,1,0:T(8,128)(2,1)S(1)} %copy-done.7, f32[768,256]{1,0:T(8,128)S(1)} %fusion.6), kind=kOutput, calls=%fused_computation.20 | convolution fusion | flops 1613365248 | bytes 9175040 | tf_op jit(solution)/shard_map/dot_general | solution.py:159
  135.4 2.9 %copy.49 = bf16[96,8,16,128]{3,2,1,0:T(8,128)(2,1)S(1)} copy(bf16[96,8,16,128]{3,1,2,0:T(8,128)(2,1)} %fusion.10) | data formatting | bytes 6291456
  138.3 0.8 copy.68
  139.1 43.4 %all_to_all.46 = bf16[16,1,768,128]{3,2,1,0:T(8,128)(2,1)} all-to-all(bf16[16,1,768,128]{3,2,1,0:T(8,128)(2,1)S(1)} %bitcast.96), channel_id=1, replica_groups=mesh['sp'=32,'tp_0'=4,'tp_1'=4] {'tp_0','tp_1'}, dimensions={0} | all-to-all | bytes 6291456 | tf_op jit(solution)/shard_map/all_to_all | solution.py:69
  182.5 3.1 %reduce_sum.64 = bf16[768,128]{1,0:T(8,128)(2,1)} reduce(bf16[16,1,768,128]{3,2,1,0:T(8,128)(2,1)} %all_to_all.46, bf16[]{:T(256)} %constant.87.clone.1), dimensions={0,1}, to_apply=%region_9.10 | reduce | flops 1474560 | bytes 3342338 | tf_op jit(solution)/shard_map/reduce_sum | solution.py:163
  185.5 3.9 %all-to-all-start.4 = ((bf16[32,24,128]{2,1,0:T(8,128)(2,1)}), bf16[32,24,128]{2,1,0:T(8,128)(2,1)S(1)}, u32[]{:S(2)}, u32[]{:S(2)}) async-start(bf16[32,24,128]{2,1,0:T(8,128)(2,1)} %bitcast.17), calls=%async_computation.4 | async-start | bytes 393216 | tf_op jit(solution)/shard_map/all_to_all | solution.py:165
  189.6 19.8 %all-to-all-done.4 = bf16[32,24,128]{2,1,0:T(8,128)(2,1)S(1)} async-done(((bf16[32,24,128]{2,1,0:T(8,128)(2,1)}), bf16[32,24,128]{2,1,0:T(8,128)(2,1)S(1)}, u32[]{:S(2)}, u32[]{:S(2)}) %all-to-all-start.4) | async-done | bytes 196640 | tf_op jit(solution)/shard_map/all_to_all | solution.py:165
  209.4 1.0 gather_fusion.1
  210.9 10.2 %all_to_all.47 = bf16[16,16,128]{2,1,0:T(8,128)(2,1)S(1)} all-to-all(bf16[16,16,128]{2,1,0:T(8,128)(2,1)S(1)} %bitcast.101), channel_id=1, replica_groups=mesh['sp'=32,'tp_0'=4,'tp_1'=4] {'tp_0','tp_1'}, dimensions={0} | all-to-all | bytes 131072 | tf_op jit(solution)/shard_map/all_to_all | solution.py:173
  (56 shorter events, 5.0 us)
Async XLA Ops:
  0.0 128.2 %copy-start = (bf16[1,256,2048]{2,1,0:T(8,128)(2,1)S(1)}, bf16[1,256,2048]{2,1,0:T(8,128)(2,1)}, u32[]{:S(2)}) copy-start(bf16[1,256,2048]{2,1,0:T(8,128)(2,1)} %param.23) | copy-start | bytes 3145732
  0.0 14.1 %copy-start.5 = (f32[2]{0:T(128)S(1)}, f32[2]{0:T(128)}, u32[]{:S(2)}) copy-start(f32[2]{0:T(128)} %param.15) | copy-start | bytes 28
  1.1 11.8 %collective-permute-start.1 = (bf16[128,64]{0,1:T(8,128)(2,1)S(1)}, bf16[128,64]{0,1:T(8,128)(2,1)S(1)}, u32[]{:S(2)}, u32[]{:S(2)}) collective-permute-start(bf16[128,64]{0,1:T(8,128)(2,1)S(1)} %slice.21), channel_id=1, source_target_pairs={{0,16},{16,32},{32,48},{48,64},{64,80},{80,96},{96,112},{112,128},... | collective-permute-start | bytes 49160 | tf_op jit(solution)/shard_map/ppermute | solution.py:20
  3.9 10.5 %copy-start.2 = (bf16[128,2048]{1,0:T(8,128)(2,1)S(1)}, bf16[128,2048]{1,0:T(8,128)(2,1)}, u32[]{:S(2)}) copy-start(bf16[128,2048]{1,0:T(8,128)(2,1)} %param.16) | copy-start | bytes 1572868
  3.9 10.2 %collective-permute-start = (bf16[128,64]{0,1:T(8,128)(2,1)S(1)}, bf16[128,64]{0,1:T(8,128)(2,1)S(1)}, u32[]{:S(2)}, u32[]{:S(2)}) collective-permute-start(bf16[128,64]{0,1:T(8,128)(2,1)S(1)} %slice.20), channel_id=1, source_target_pairs={{0,16},{16,32},{32,48},{48,64},{64,80},{80,96},{96,112},{112,128},... | collective-permute-start | bytes 49160 | tf_op jit(solution)/shard_map/ppermute | solution.py:20
  16.2 23.4 %all-to-all-start = ((bf16[16,256,128]{2,1,0:T(8,128)(2,1)}), bf16[16,256,128]{2,1,0:T(8,128)(2,1)S(1)}, u32[]{:S(2)}, u32[]{:S(2)}) async-start(bf16[16,256,128]{2,1,0:T(8,128)(2,1)} %bitcast.94), calls=%async_computation | async-start | bytes 2097152 | tf_op jit(solution)/shard_map/all_to_all | solution.py:30
  120.1 0.7 copy-start.3
  121.9 5.3 %copy-start.6 = (bf16[1,2048,256]{2,1,0:T(8,128)(2,1)S(1)}, bf16[1,2048,256]{2,1,0:T(8,128)(2,1)}, u32[]{:S(2)}) copy-start(bf16[1,2048,256]{2,1,0:T(8,128)(2,1)} %param.21) | copy-start | bytes 3145732
  125.6 1.7 copy-start.1
  127.2 1.2 copy-start.7
  182.5 6.9 %copy-start.4 = (f32[256,2]{0,1:T(2,128)S(1)}, f32[256,2]{0,1:T(2,128)}, u32[]{:S(2)}) copy-start(f32[256,2]{0,1:T(2,128)} %param.20) | copy-start | bytes 6148
  185.5 23.8 %all-to-all-start.4 = ((bf16[32,24,128]{2,1,0:T(8,128)(2,1)}), bf16[32,24,128]{2,1,0:T(8,128)(2,1)S(1)}, u32[]{:S(2)}, u32[]{:S(2)}) async-start(bf16[32,24,128]{2,1,0:T(8,128)(2,1)} %bitcast.17), calls=%async_computation.4 | async-start | bytes 393216 | tf_op jit(solution)/shard_map/all_to_all | solution.py:165

commit v2 on v1

v2 whole, which is shorter than its diff:
```python
import functools

import jax
import jax.numpy as jnp
from jax import lax
from jax.experimental import pallas as pl
from jax.experimental.pallas import tpu as pltpu
from jax.sharding import Mesh
from jax.sharding import PartitionSpec as P

HEAD_DIM = 64
REP = 8
WINDOW = 128
LANES = 128
TP = ("tp_0", "tp_1")
SP_TP = ("sp", "tp_0", "tp_1")
NORM_EPS = 1e-06
BF16 = jnp.bfloat16
F32 = jnp.float32
VMEM_SPEC = pl.BlockSpec(memory_space=pltpu.VMEM)
SMEM_SPEC = pl.BlockSpec(memory_space=pltpu.SMEM)


def dot(a, b, contract=(1, 0)):
    return lax.dot_general(a, b, (((contract[0],), (contract[1],)), ((), ())), preferred_element_type=F32)


def head_pair(block, half):
    swapped = jnp.concatenate([block[:, HEAD_DIM:], block[:, :HEAD_DIM]], axis=1)
    lane = lax.broadcasted_iota(jnp.int32, block.shape, 1)
    low = jnp.where(half == 0, block, swapped)
    high = jnp.where(half == 0, swapped, block)
    zero = jnp.zeros_like(block)
    return jnp.where(lane < HEAD_DIM, low, zero), jnp.where(lane >= HEAD_DIM, high, zero)


def attention_body(place, sinks, q_ref, k_ref, v_ref, before_ref, w_ref, out_ref):
    first_block = place[0] == 0
    group = place[1]
    half = group % 2
    pair = group // 2
    pairs = k_ref.shape[1] // LANES

    def chosen(ref, row0, rows, col0):
        picked = ref[row0 : row0 + rows, col0 : col0 + LANES]
        for i in range(1, pairs):
            picked = jnp.where(pair == i, ref[row0 : row0 + rows, col0 + i * LANES : col0 + (i + 1) * LANES], picked)
        return picked.astype(F32)

    rows = q_ref.shape[0]
    width = k_ref.shape[1]
    keys = jnp.concatenate([chosen(before_ref, 0, WINDOW, 0), chosen(k_ref, 0, rows, 0)], axis=0)
    values = jnp.concatenate([chosen(before_ref, 0, WINDOW, width), chosen(v_ref, 0, rows, 0)], axis=0)
    keys = [k.astype(BF16) for k in head_pair(keys, half)]
    values = [v.astype(BF16) for v in head_pair(values, half)]
    row = lax.broadcasted_iota(jnp.int32, (WINDOW, 2 * WINDOW), 0)
    col = lax.broadcasted_iota(jnp.int32, (WINDOW, 2 * WINDOW), 1)
    inside = (col > row) & (col <= row + WINDOW)
    parts = []
    for block in range(rows // WINDOW):
        lo = block * WINDOW
        allowed = inside
        if block == 0:
            allowed = inside & ((col >= WINDOW) | jnp.logical_not(first_block))
        q = q_ref[lo : lo + WINDOW, :]
        total = None
        for h in range(2):
            scores = dot(q, keys[h][lo : lo + 2 * WINDOW], (1, 1)) * HEAD_DIM**-0.5
            scores = jnp.where(allowed, scores, -1e30)
            sink = sinks[h]
            peak = jnp.maximum(jnp.max(scores, axis=-1, keepdims=True), sink)
            terms = jnp.exp(scores - peak)
            total_terms = jnp.sum(terms, axis=-1, keepdims=True) + jnp.exp(sink - peak)
            probs = (terms / total_terms).astype(BF16)
            part = dot(probs, values[h][lo : lo + 2 * WINDOW])
            total = part if total is None else total + part
        parts.append(total.astype(BF16))
    attended = jnp.concatenate(parts, axis=0)
    for t in range(out_ref.shape[0]):
        out_ref[t] = dot(attended, w_ref[:, t * LANES : (t + 1) * LANES]).astype(BF16)


def attention(place, sinks, q, k, v, before, w):
    shares = w.shape[1] // LANES
    return pl.pallas_call(
        attention_body,
        out_shape=jax.ShapeDtypeStruct((shares, q.shape[0], LANES), BF16),
        in_specs=[SMEM_SPEC, SMEM_SPEC] + [VMEM_SPEC] * 5,
        out_specs=VMEM_SPEC,
        name="attention",
    )(place, sinks, q, k, v, before, w)


def slots_body(cap, experts, routes_ref, wide_ref, send_ref, take_ref):
    tokens = routes_ref.shape[0]
    slots = send_ref.shape[0]
    lane = lax.broadcasted_iota(jnp.int32, (tokens, LANES), 1)
    picks = [routes_ref[:, k : k + 1] for k in range(2)]
    hot = [(picks[k] == lane).astype(F32) for k in range(2)]
    r = lax.broadcasted_iota(jnp.int32, (tokens, tokens), 0)
    c = lax.broadcasted_iota(jnp.int32, (tokens, tokens), 1)
    ahead = dot((c < r).astype(BF16), (hot[0] + hot[1]).astype(BF16))
    slot_lane = lax.broadcasted_iota(jnp.int32, (tokens, slots), 1)
    for k in range(2):
        rank = jnp.sum(ahead * hot[k], axis=1, keepdims=True).astype(jnp.int32)
        target = picks[k] * cap + rank
        take_ref[k * tokens : (k + 1) * tokens, :] = (slot_lane == target).astype(F32).astype(BF16)
    sub = lax.broadcasted_iota(jnp.int32, (experts, tokens), 0)
    picks_w = [wide_ref[k : k + 1, :] for k in range(2)]
    hot_w = [(picks_w[k] == sub).astype(F32) for k in range(2)]
    ahead_w = dot((hot_w[0] + hot_w[1]).astype(BF16), (r < c).astype(BF16))
    slot_sub = lax.broadcasted_iota(jnp.int32, (slots, tokens), 0)
    hit = None
    for k in range(2):
        rank = jnp.sum(ahead_w * hot_w[k], axis=0, keepdims=True).astype(jnp.int32)
        target = picks_w[k] * cap + rank
        here = slot_sub == target
        hit = here if hit is None else hit | here
    send_ref[...] = hit.astype(F32).astype(BF16)


def slot_matrices(routes, experts, cap):
    tokens = routes.shape[0]
    slots = experts * cap
    return pl.pallas_call(
        functools.partial(slots_body, cap, experts),
        out_shape=(
            jax.ShapeDtypeStruct((slots, tokens), BF16),
            jax.ShapeDtypeStruct((2 * tokens, slots), BF16),
        ),
        in_specs=[VMEM_SPEC] * 2,
        out_specs=(VMEM_SPEC, VMEM_SPEC),
        name="slots",
    )(routes, routes.T)


def stream_body(place, arrived_ref, own_ref, send_ref, stream_ref, rows_ref):
    total = own_ref[...].astype(F32)
    summed = arrived_ref[0].astype(F32)
    for t in range(1, arrived_ref.shape[0]):
        summed = summed + arrived_ref[t].astype(F32)
    stream = (total + summed).astype(BF16)
    stream_ref[...] = stream
    rows_ref[...] = dot(send_ref[...], stream).astype(BF16)


def stream_and_rows(place, arrived, stream_in, send):
    tokens = stream_in.shape[0]
    slots = send.shape[0]
    return pl.pallas_call(
        stream_body,
        grid_spec=pltpu.PrefetchScalarGridSpec(
            num_scalar_prefetch=1,
            grid=(1,),
            in_specs=[
                pl.BlockSpec(arrived.shape, lambda i, place: (0, 0, 0)),
                pl.BlockSpec((tokens, LANES), lambda i, place: (0, place[2])),
                pl.BlockSpec(send.shape, lambda i, place: (0, 0)),
            ],
            out_specs=[
                pl.BlockSpec((tokens, LANES), lambda i, place: (0, 0)),
                pl.BlockSpec((slots, LANES), lambda i, place: (0, 0)),
            ],
        ),
        out_shape=(
            jax.ShapeDtypeStruct((tokens, LANES), BF16),
            jax.ShapeDtypeStruct((slots, LANES), BF16),
        ),
        name="stream",
    )(place, arrived, stream_in, send)


def expert_body(x_ref, gain_ref, gate_ref, up_ref, down_ref, out_ref):
    shares = x_ref.shape[0]
    stream = jnp.concatenate([x_ref[t] for t in range(shares)], axis=1).astype(F32)
    scale = lax.rsqrt(jnp.mean(stream * stream, axis=-1, keepdims=True) + NORM_EPS)
    normed = (stream * scale * gain_ref[...]).astype(BF16)
    gate_act = dot(normed, gate_ref[0])
    up_act = dot(normed, up_ref[0])
    hidden = (gate_act * jax.nn.sigmoid(gate_act) * up_act).astype(BF16)
    for t in range(shares):
        out_ref[t] = dot(hidden, down_ref[0, :, t * LANES : (t + 1) * LANES]).astype(BF16)


def expert(x, gain, gate, up, down, block):
    shares, rows, _ = x.shape
    step = pl.BlockSpec((shares, block, LANES), lambda i: (0, i, 0))

    def whole(a):
        return pl.BlockSpec(a.shape, lambda i: (0,) * a.ndim)

    return pl.pallas_call(
        expert_body,
        grid=(rows // block,),
        in_specs=[step, whole(gain), whole(gate), whole(up), whole(down)],
        out_specs=step,
        out_shape=jax.ShapeDtypeStruct(x.shape, BF16),
        name="expert",
    )(x, gain, gate, up, down)


def combine_body(rows_ref, take_ref, weights_ref, stream_ref, out_ref):
    tokens = stream_ref.shape[0]
    taken = dot(take_ref[...], rows_ref[...])
    moe = taken[:tokens] * weights_ref[:, 0:1] + taken[tokens:] * weights_ref[:, 1:2]
    out_ref[...] = (stream_ref[...].astype(F32) + moe).astype(BF16)


def combine(rows, take, weights, stream):
    return pl.pallas_call(
        combine_body,
        out_shape=jax.ShapeDtypeStruct(stream.shape, BF16),
        in_specs=[VMEM_SPEC] * 4,
        out_specs=VMEM_SPEC,
        name="combine",
    )(rows, take, weights, stream)


def per_device(
    query_rows,
    key_rows,
    value_rows,
    sink_logits,
    out_weight,
    stream_in,
    norm_gain,
    routes,
    route_weights,
    gate_weight,
    up_weight,
    down_weight,
):
    tokens = query_rows.shape[0]
    local_heads = query_rows.shape[1] // HEAD_DIM
    tp_size = lax.axis_size(TP)
    experts = lax.axis_size("sp")
    tp_index = lax.axis_index(TP)
    place = jnp.stack([lax.axis_index("sp"), tp_index * local_heads // REP, tp_index]).astype(jnp.int32)
    last = jnp.concatenate([key_rows[tokens - WINDOW :], value_rows[tokens - WINDOW :]], axis=1)
    before = lax.ppermute(last, "sp", [(i, i + 1) for i in range(experts - 1)])
    partial = attention(place, sink_logits, query_rows, key_rows, value_rows, before, out_weight)
    arrived = lax.all_to_all(partial, TP, split_axis=0, concat_axis=0, tiled=True)
    cap = 3 * tokens * routes.shape[1] // (2 * experts)
    send, take = slot_matrices(routes, experts, cap)
    stream, rows = stream_and_rows(place, arrived, stream_in, send)
    rows = lax.all_to_all(rows.reshape(experts, cap, LANES), "sp", split_axis=0, concat_axis=0, tiled=True)
    slots = experts * cap
    copies = jnp.broadcast_to(rows.reshape(slots, LANES), (tp_size, slots, LANES))
    features = lax.all_to_all(copies, TP, split_axis=0, concat_axis=0, tiled=True)
    parts = expert(features, norm_gain.reshape(1, -1), gate_weight, up_weight, down_weight, 192)
    parts = lax.all_to_all(parts, TP, split_axis=0, concat_axis=0, tiled=True)
    summed = jnp.sum(parts.astype(F32), axis=0).astype(BF16)
    returned = lax.all_to_all(summed.reshape(experts, cap, LANES), "sp", split_axis=0, concat_axis=0, tiled=True)
    out = combine(returned.reshape(slots, LANES), take, route_weights, stream)
    return lax.all_to_all(out, TP, split_axis=0, concat_axis=1, tiled=True)


def solution(mesh):
    finer = Mesh(mesh.devices.reshape(mesh.shape["sp"], 4, 4), ("sp", "tp_0", "tp_1"))
    placed = (
        P("sp", TP),
        P("sp", None),
        P("sp", None),
        P(TP),
        P(TP, None),
        P("sp", None),
        P(),
        P("sp", None),
        P("sp", None),
        P("sp", None, TP),
        P("sp", None, TP),
        P("sp", TP, None),
    )
    return jax.shard_map(
        per_device, mesh=finer, in_specs=placed, out_specs=P(SP_TP, None), check_vma=False
    )
```

time: 223 us -> 210 us (0.942)
  Pallas kernels: 0 us -> 19.6 us
  local copies, waits for them, and re-layouts: 24.5 us -> 6.82 us
  matrix products: 8.91 us -> 0 us
  other arithmetic: 9.61 us -> 1.83 us
  blocking collectives: 130 us -> 133 us
  starting transfers between devices: 17.3 us -> 14.5 us
  waiting for transfers between devices: 30.6 us -> 33 us
    pallas_call x0 -> x5, Pallas kernels: none -> 19.6 us  [the longest x1 8.19 us: expert(): pl.pallas_call(expert_body, grid=(rows // block,), in_specs=[step, whole(...]
    dot_general x5 -> x0, matrix products: 8.91 us -> none  [the longest x1 6.92 us: per_device(): jnp.dot(hidden, down_weight[0], preferred_element_type=jnp.float32)]
    scatter x2 -> x0, local copies, waits for them, and re-layouts: 4.89 us -> none  [the longest x1 2.45 us: slot_tables(): jnp.zeros((experts_n * slot_cap,), jnp.int32).at[targets].set(pair_token)]
    ppermute x2 -> x1, starting transfers between devices: 5.98 us -> 1.75 us  [per_device(): before = lax.ppermute(last, 'sp', [(i, i + 1) for i in range(experts - 1)])]
    convert_element_type x1 -> x0, local copies, waits for them, and re-layouts: 3.65 us -> none  [rms_scale(): return (scaled * norm_gain).astype(jnp.bfloat16)]
    reduce_sum x6 -> x1, other arithmetic: 4.5 us -> 1.14 us  [per_device(): summed = jnp.sum(parts.astype(F32), axis=0).astype(BF16)]
    unnamed x22 -> x12, local copies, waits for them, and re-layouts: 6.88 us -> 3.88 us
    gather x2 -> x0, local copies, waits for them, and re-layouts: 2.92 us -> none  [the longest x1 1.88 us: per_device(): columns[slot_token]]
  transfers between devices with their start and end apart: 4 -> 3, of which waited for: 2 -> 3; matrix products, arithmetic and copies ran while one was open for 5% -> 1% of each run, Pallas kernels for 0% -> 1%
where the time goes in v2:
time: 210 us; the launch traced here: 209 us
  blocking collectives  133 us (63%)
  waiting for transfers between devices  33 us (16%)
  Pallas kernels  19.6 us (9%)
  starting transfers between devices  14.5 us (7%)
  local copies, waits for them, and re-layouts  6.82 us (3%)
    all_to_all x1, blocking collectives, per_device(): parts = lax.all_to_all(parts, TP, split_axis=0, concat_axis=0, tiled=True)  43.8 us
    all_to_all x1, blocking collectives, per_device(): lax.all_to_all(copies, TP, split_axis=0, concat_axis=0, tiled=True)  43.2 us
    all_to_all x1, blocking collectives, per_device(): lax.all_to_all(rows.reshape(experts, cap, LANES), 'sp', split_axis=0, con...  35.7 us
    all_to_all x1, waiting for transfers between devices, per_device(): lax.all_to_all(summed.reshape(experts, cap, LANES), 'sp', split_axis=0, c...  19.2 us
    all_to_all x1, waiting for transfers between devices, per_device(): lax.all_to_all(partial, TP, split_axis=0, concat_axis=0, tiled=True)  13.6 us
    all_to_all x1, blocking collectives, per_device(): return lax.all_to_all(out, TP, split_axis=0, concat_axis=1, tiled=True)  10.5 us
    all_to_all x1, starting transfers between devices, per_device(): lax.all_to_all(partial, TP, split_axis=0, concat_axis=0, tiled=True)  8.88 us
    pallas_call x1, Pallas kernels, expert(): pl.pallas_call(expert_body, grid=(rows // block,), in_specs=[step, whole(...  8.19 us
  transfers between devices with their start and end apart: 3, of which 3 were waited for; matrix products, arithmetic and copies ran while one was open for 1% of the time, Pallas kernels for 1%

profile of v2, /device:TPU:2, one launch (start us, length us, event | category | flops | bytes accessed | tf_op | source)
XLA Modules:
  0.0 209.0 jit_solution(9567876671059543423)
XLA Ops:
  0.0 0.9 slice.6
  0.9 0.8 slice.7
  1.7 1.7 collective-permute-start
  3.5 0.7 pad_add_fusion.place
  4.2 0.3 collective-permute-done.before_ref
  4.4 0.0 copy-start.2
  4.4 0.7 copy-done.2
  5.1 3.6 %attention.1 = bf16[16,256,128]{2,1,0:T(8,128)(2,1)} custom-call(s32[3]{0:T(128)} %pad_add_fusion.place, f32[2]{0:T(128)} %sinks.1, bf16[256,128]{1,0:T(8,128)(2,1)} %q_ref.1, bf16[256,256]{1,0:T(8,128)(2,1)} %k_ref.1, bf16[256,256]{1,0:T(8,128)(2,1)} %v_ref.1, bf16[128,512]{1,0:T(8,128)(2,1)} %copy-done.2, bf16[128,2048]{1,0:T(8,128)(2,1)} %w_ref.1), custom_call_target="tpu_custom_call" | custom-call | tf_op jit(solution)/shard_map/attention/pallas_call | solution.py:85
  8.7 8.9 %all-to-all-start = ((bf16[16,256,128]{2,1,0:T(8,128)(2,1)}), bf16[16,256,128]{2,1,0:T(8,128)(2,1)S(1)}, u32[]{:S(2)}, u32[]{:S(2)}) async-start(bf16[16,256,128]{2,1,0:T(8,128)(2,1)} %attention.1), calls=%async_computation | async-start | bytes 2097152 | tf_op jit(solution)/shard_map/all_to_all | solution.py:242
  17.5 0.0 copy-done.3
  17.6 0.8 copy.13.routes_ref
  18.3 2.6 %slots.1 = (bf16[768,256]{1,0:T(8,128)(2,1)}, bf16[512,768]{1,0:T(8,128)(2,1)}) custom-call(s32[256,2]{1,0:T(8,128)} %copy.13.routes_ref, s32[2,256]{1,0:T(2,128)} %bitcast.20), custom_call_target="tpu_custom_call" | custom-call | tf_op jit(solution)/shard_map/slots/pallas_call | solution.py:125
  20.9 13.6 %all-to-all-done.arrived_ref = bf16[16,256,128]{2,1,0:T(8,128)(2,1)S(1)} async-done(((bf16[16,256,128]{2,1,0:T(8,128)(2,1)}), bf16[16,256,128]{2,1,0:T(8,128)(2,1)S(1)}, u32[]{:S(2)}, u32[]{:S(2)}) %all-to-all-start) | async-done | bytes 1048608 | tf_op jit(solution)/shard_map/all_to_all | solution.py:242
  34.5 0.0 copy-start
  34.5 1.0 copy-done
  35.5 3.1 %stream.1 = (bf16[256,128]{1,0:T(8,128)(2,1)}, bf16[768,128]{1,0:T(8,128)(2,1)}) custom-call(s32[3]{0:T(128)} %pad_add_fusion.place, bf16[16,256,128]{2,1,0:T(8,128)(2,1)} %copy-done, bf16[256,2048]{1,0:T(8,128)(2,1)} %own_ref.1, bf16[768,256]{1,0:T(8,128)(2,1)} %get-tuple-element.9.send_ref), custom_call_target="tpu_custom_call" | custom-call | tf_op jit(solution)/shard_map/stream/pallas_call | solution.py:150
  38.6 35.7 %all_to_all.44 = bf16[32,24,128]{2,1,0:T(8,128)(2,1)S(1)} all-to-all(bf16[32,24,128]{2,1,0:T(8,128)(2,1)} %bitcast.19), channel_id=1, replica_groups=mesh['sp'=32,'tp_0'=4,'tp_1'=4] {'sp'}, dimensions={0} | all-to-all | bytes 393216 | tf_op jit(solution)/shard_map/all_to_all | solution.py:246
  74.3 0.6 broadcast_in_dim.3
  74.9 43.2 %all_to_all.45.x_ref = bf16[16,768,128]{2,1,0:T(8,128)(2,1)} all-to-all(bf16[16,768,128]{2,1,0:T(8,128)(2,1)S(1)} %broadcast_in_dim.3), channel_id=1, replica_groups=mesh['sp'=32,'tp_0'=4,'tp_1'=4] {'tp_0','tp_1'}, dimensions={0} | all-to-all | bytes 6291456 | tf_op jit(solution)/shard_map/all_to_all | solution.py:249
  118.1 8.2 %expert.1 = bf16[16,768,128]{2,1,0:T(8,128)(2,1)} custom-call(bf16[16,768,128]{2,1,0:T(8,128)(2,1)} %all_to_all.45.x_ref, f32[1,2048]{1,0:T(1,128)} %bitcast.21, bf16[1,2048,256]{2,1,0:T(8,128)(2,1)} %gate_ref.1, bf16[1,2048,256]{2,1,0:T(8,128)(2,1)} %up_ref.1, bf16[1,256,2048]{2,1,0:T(8,128)(2,1)} %down_ref.1), custom_call_target="tpu_custom_call" | custom-call | tf_op jit(solution)/shard_map/expert/pallas_call | solution.py:192
  126.3 43.8 %all_to_all.46 = bf16[16,768,128]{2,1,0:T(8,128)(2,1)S(1)} all-to-all(bf16[16,768,128]{2,1,0:T(8,128)(2,1)} %expert.1), channel_id=1, replica_groups=mesh['sp'=32,'tp_0'=4,'tp_1'=4] {'tp_0','tp_1'}, dimensions={0} | all-to-all | bytes 6291456 | tf_op jit(solution)/shard_map/all_to_all | solution.py:251
  170.0 0.0 copy-start.4
  170.0 1.1 reduce_sum.12
  171.2 3.9 %all-to-all-start.4 = ((bf16[32,24,128]{2,1,0:T(8,128)(2,1)}), bf16[32,24,128]{2,1,0:T(8,128)(2,1)S(1)}, u32[]{:S(2)}, u32[]{:S(2)}) async-start(bf16[32,24,128]{2,1,0:T(8,128)(2,1)} %bitcast.7), calls=%async_computation.4 | async-start | bytes 393216 | tf_op jit(solution)/shard_map/all_to_all | solution.py:253
  175.1 0.0 copy-done.4
  175.1 0.8 copy.14.weights_ref
  175.9 19.2 %all-to-all-done.4 = bf16[32,24,128]{2,1,0:T(8,128)(2,1)S(1)} async-done(((bf16[32,24,128]{2,1,0:T(8,128)(2,1)}), bf16[32,24,128]{2,1,0:T(8,128)(2,1)S(1)}, u32[]{:S(2)}, u32[]{:S(2)}) %all-to-all-start.4) | async-done | bytes 196640 | tf_op jit(solution)/shard_map/all_to_all | solution.py:253
  195.0 0.0 copy-start.1
  195.0 0.7 copy-done.1
  195.7 2.2 %combine.1 = bf16[256,128]{1,0:T(8,128)(2,1)} custom-call(bf16[768,128]{1,0:T(8,128)(2,1)} %bitcast.16, bf16[512,768]{1,0:T(8,128)(2,1)} %get-tuple-element.11.take_ref, f32[256,2]{1,0:T(8,128)} %copy.14.weights_ref, bf16[256,128]{1,0:T(8,128)(2,1)} %get-tuple-element.12.stream_ref), custom_call_target="tpu_custom_call" | custom-call | tf_op jit(solution)/shard_map/combine/pallas_call | solution.py:210
  197.9 10.5 %all_to_all.47 = bf16[16,16,128]{2,1,0:T(8,128)(2,1)S(1)} all-to-all(bf16[16,16,128]{2,1,0:T(8,128)(2,1)} %bitcast.18), channel_id=1, replica_groups=mesh['sp'=32,'tp_0'=4,'tp_1'=4] {'tp_0','tp_1'}, dimensions={0} | all-to-all | bytes 131072 | tf_op jit(solution)/shard_map/all_to_all | solution.py:255
  208.4 0.6 copy_bitcast_fusion
  (2 shorter events, 0.0 us)
Async XLA Ops:
  0.0 17.5 %copy-start.3 = (s32[256,2]{0,1:T(2,128)S(1)}, s32[256,2]{0,1:T(2,128)}, u32[]{:S(2)}) copy-start(s32[256,2]{0,1:T(2,128)} %param.19) | copy-start | bytes 6148
  1.7 2.7 %collective-permute-start = (bf16[128,512]{1,0:T(8,128)(2,1)S(1)}, bf16[128,512]{1,0:T(8,128)(2,1)S(1)}, u32[]{:S(2)}, u32[]{:S(2)}) collective-permute-start(bf16[128,512]{1,0:T(8,128)(2,1)S(1)} %pad_maximum_fusion), channel_id=1, source_target_pairs={{0,16},{16,32},{32,48},{48,64},{64,80},{80,96},{96,112},{112,128},... | collective-permute-start | bytes 393224 | tf_op jit(solution)/shard_map/ppermute | solution.py:240
  4.4 0.7 copy-start.2
  8.7 25.9 %all-to-all-start = ((bf16[16,256,128]{2,1,0:T(8,128)(2,1)}), bf16[16,256,128]{2,1,0:T(8,128)(2,1)S(1)}, u32[]{:S(2)}, u32[]{:S(2)}) async-start(bf16[16,256,128]{2,1,0:T(8,128)(2,1)} %attention.1), calls=%async_computation | async-start | bytes 2097152 | tf_op jit(solution)/shard_map/all_to_all | solution.py:242
  34.5 1.0 copy-start
  170.0 5.0 %copy-start.4 = (f32[256,2]{0,1:T(2,128)S(1)}, f32[256,2]{0,1:T(2,128)}, u32[]{:S(2)}) copy-start(f32[256,2]{0,1:T(2,128)} %param.20) | copy-start | bytes 6148
  171.2 23.8 %all-to-all-start.4 = ((bf16[32,24,128]{2,1,0:T(8,128)(2,1)}), bf16[32,24,128]{2,1,0:T(8,128)(2,1)S(1)}, u32[]{:S(2)}, u32[]{:S(2)}) async-start(bf16[32,24,128]{2,1,0:T(8,128)(2,1)} %bitcast.7), calls=%async_computation.4 | async-start | bytes 393216 | tf_op jit(solution)/shard_map/all_to_all | solution.py:253
  195.0 0.7 copy-start.1

commit v3 on v2

--- a/solution.py
+++ b/solution.py
@@ -19,6 +19,21 @@
 F32 = jnp.float32
 VMEM_SPEC = pl.BlockSpec(memory_space=pltpu.VMEM)
 SMEM_SPEC = pl.BlockSpec(memory_space=pltpu.SMEM)
+PLANE = ("tp_1", "tp_0")
+SIDE = 4
+PIECES = 2
+
+
+def in_vmem(*arrays):
+    return [pltpu.with_memory_space_constraint(a, pltpu.VMEM) for a in arrays]
+
+
+def vmem_out(shape):
+    return pltpu.VMEM(shape, BF16)
+
+
+def share_of(member, side):
+    return member % side * side + member // side
 
 
 def dot(a, b, contract=(1, 0)):
@@ -76,19 +91,21 @@
             total = part if total is None else total + part
         parts.append(total.astype(BF16))
     attended = jnp.concatenate(parts, axis=0)
-    for t in range(out_ref.shape[0]):
-        out_ref[t] = dot(attended, w_ref[:, t * LANES : (t + 1) * LANES]).astype(BF16)
+    for p in range(out_ref.shape[0]):
+        t = share_of(p, SIDE)
+        out_ref[p] = dot(attended, w_ref[:, t * LANES : (t + 1) * LANES]).astype(BF16)
 
 
 def attention(place, sinks, q, k, v, before, w):
     shares = w.shape[1] // LANES
     return pl.pallas_call(
         attention_body,
-        out_shape=jax.ShapeDtypeStruct((shares, q.shape[0], LANES), BF16),
+        out_shape=vmem_out((shares, q.shape[0], LANES)),
         in_specs=[SMEM_SPEC, SMEM_SPEC] + [VMEM_SPEC] * 5,
         out_specs=VMEM_SPEC,
+        compiler_params=pltpu.CompilerParams(vmem_limit_bytes=16 * 2**20),
         name="attention",
-    )(place, sinks, q, k, v, before, w)
+    )(place, sinks, q, k, v, *in_vmem(before), w)
 
 
 def slots_body(cap, experts, routes_ref, wide_ref, send_ref, take_ref):
@@ -125,78 +142,61 @@
     return pl.pallas_call(
         functools.partial(slots_body, cap, experts),
         out_shape=(
-            jax.ShapeDtypeStruct((slots, tokens), BF16),
-            jax.ShapeDtypeStruct((2 * tokens, slots), BF16),
+            vmem_out((slots, tokens)),
+            vmem_out((2 * tokens, slots)),
         ),
         in_specs=[VMEM_SPEC] * 2,
         out_specs=(VMEM_SPEC, VMEM_SPEC),
+        compiler_params=pltpu.CompilerParams(vmem_limit_bytes=16 * 2**20),
         name="slots",
-    )(routes, routes.T)
-
-
-def stream_body(place, arrived_ref, own_ref, send_ref, stream_ref, rows_ref):
-    total = own_ref[...].astype(F32)
+    )(*in_vmem(routes, routes.T))
+
+
+def stream_body(arrived_ref, own_ref, send_ref, stream_ref, rows_ref):
     summed = arrived_ref[0].astype(F32)
     for t in range(1, arrived_ref.shape[0]):
         summed = summed + arrived_ref[t].astype(F32)
-    stream = (total + summed).astype(BF16)
+    stream = (own_ref[...].astype(F32) + summed).astype(BF16)
     stream_ref[...] = stream
     rows_ref[...] = dot(send_ref[...], stream).astype(BF16)
 
 
-def stream_and_rows(place, arrived, stream_in, send):
-    tokens = stream_in.shape[0]
-    slots = send.shape[0]
+def stream_and_rows(arrived, own, send):
     return pl.pallas_call(
         stream_body,
-        grid_spec=pltpu.PrefetchScalarGridSpec(
-            num_scalar_prefetch=1,
-            grid=(1,),
-            in_specs=[
-                pl.BlockSpec(arrived.shape, lambda i, place: (0, 0, 0)),
-                pl.BlockSpec((tokens, LANES), lambda i, place: (0, place[2])),
-                pl.BlockSpec(send.shape, lambda i, place: (0, 0)),
-            ],
-            out_specs=[
-                pl.BlockSpec((tokens, LANES), lambda i, place: (0, 0)),
-                pl.BlockSpec((slots, LANES), lambda i, place: (0, 0)),
-            ],
-        ),
-        out_shape=(
-            jax.ShapeDtypeStruct((tokens, LANES), BF16),
-            jax.ShapeDtypeStruct((slots, LANES), BF16),
-        ),
+        out_shape=(vmem_out(own.shape), vmem_out((send.shape[0], LANES))),
+        in_specs=[VMEM_SPEC] * 3,
+        out_specs=(VMEM_SPEC, VMEM_SPEC),
+        compiler_params=pltpu.CompilerParams(vmem_limit_bytes=16 * 2**20),
         name="stream",
-    )(place, arrived, stream_in, send)
-
-
-def expert_body(x_ref, gain_ref, gate_ref, up_ref, down_ref, out_ref):
-    shares = x_ref.shape[0]
-    stream = jnp.concatenate([x_ref[t] for t in range(shares)], axis=1).astype(F32)
-    scale = lax.rsqrt(jnp.mean(stream * stream, axis=-1, keepdims=True) + NORM_EPS)
-    normed = (stream * scale * gain_ref[...]).astype(BF16)
-    gate_act = dot(normed, gate_ref[0])
-    up_act = dot(normed, up_ref[0])
-    hidden = (gate_act * jax.nn.sigmoid(gate_act) * up_act).astype(BF16)
-    for t in range(shares):
-        out_ref[t] = dot(hidden, down_ref[0, :, t * LANES : (t + 1) * LANES]).astype(BF16)
+    )(*in_vmem(arrived, own, send))
+
+
+def expert_body(block, x_ref, gain_ref, gate_ref, up_ref, down_ref, out_ref):
+    shares, rows, _ = x_ref.shape
+    order = sorted(range(shares), key=lambda p: share_of(p, SIDE))
+    for lo in range(0, rows, block):
+        stream = jnp.concatenate([x_ref[p, lo : lo + block, :] for p in order], axis=1).astype(F32)
+        scale = lax.rsqrt(jnp.mean(stream * stream, axis=-1, keepdims=True) + NORM_EPS)
+        normed = (stream * scale * gain_ref[...]).astype(BF16)
+        gate_act = dot(normed, gate_ref[0])
+        up_act = dot(normed, up_ref[0])
+        hidden = (gate_act * jax.nn.sigmoid(gate_act) * up_act).astype(BF16)
+        for p in range(shares):
+            t = share_of(p, SIDE)
+            out_ref[p, lo : lo + block, :] = dot(hidden, down_ref[0, :, t * LANES : (t + 1) * LANES]).astype(BF16)
 
 
 def expert(x, gain, gate, up, down, block):
-    shares, rows, _ = x.shape
-    step = pl.BlockSpec((shares, block, LANES), lambda i: (0, i, 0))
-
-    def whole(a):
-        return pl.BlockSpec(a.shape, lambda i: (0,) * a.ndim)
-
-    return pl.pallas_call(
-        expert_body,
-        grid=(rows // block,),
-        in_specs=[step, whole(gain), whole(gate), whole(up), whole(down)],
-        out_specs=step,
-        out_shape=jax.ShapeDtypeStruct(x.shape, BF16),
+    return pl.pallas_call(
+        functools.partial(expert_body, block),
+        out_shape=vmem_out(x.shape),
+        in_specs=[VMEM_SPEC] * 5,
+        out_specs=VMEM_SPEC,
+        cost_estimate=pl.CostEstimate(flops=6 * x.shape[1] * gate.shape[1] * gate.shape[2], bytes_accessed=2 * x.size * 2, transcendentals=0),
+        compiler_params=pltpu.CompilerParams(vmem_limit_bytes=24 * 2**20),
         name="expert",
-    )(x, gain, gate, up, down)
+    )(*in_vmem(x), gain, gate, up, down)
 
 
 def combine_body(rows_ref, take_ref, weights_ref, stream_ref, out_ref):
@@ -209,11 +209,12 @@
 def combine(rows, take, weights, stream):
     return pl.pallas_call(
         combine_body,
-        out_shape=jax.ShapeDtypeStruct(stream.shape, BF16),
+        out_shape=vmem_out(stream.shape),
         in_specs=[VMEM_SPEC] * 4,
         out_specs=VMEM_SPEC,
+        compiler_params=pltpu.CompilerParams(vmem_limit_bytes=16 * 2**20),
         name="combine",
-    )(rows, take, weights, stream)
+    )(*in_vmem(rows, take), weights, *in_vmem(stream))
 
 
 def per_device(
@@ -235,22 +236,27 @@
     tp_size = lax.axis_size(TP)
     experts = lax.axis_size("sp")
     tp_index = lax.axis_index(TP)
-    place = jnp.stack([lax.axis_index("sp"), tp_index * local_heads // REP, tp_index]).astype(jnp.int32)
+    place = jnp.stack([lax.axis_index("sp"), tp_index * local_heads // REP]).astype(jnp.int32)
     last = jnp.concatenate([key_rows[tokens - WINDOW :], value_rows[tokens - WINDOW :]], axis=1)
     before = lax.ppermute(last, "sp", [(i, i + 1) for i in range(experts - 1)])
     partial = attention(place, sink_logits, query_rows, key_rows, value_rows, before, out_weight)
-    arrived = lax.all_to_all(partial, TP, split_axis=0, concat_axis=0, tiled=True)
+    arrived = lax.all_to_all(partial, PLANE, split_axis=0, concat_axis=0, tiled=True)
     cap = 3 * tokens * routes.shape[1] // (2 * experts)
     send, take = slot_matrices(routes, experts, cap)
-    stream, rows = stream_and_rows(place, arrived, stream_in, send)
+    own = lax.dynamic_slice_in_dim(stream_in, tp_index * LANES, LANES, 1)
+    stream, rows = stream_and_rows(arrived, own, send)
     rows = lax.all_to_all(rows.reshape(experts, cap, LANES), "sp", split_axis=0, concat_axis=0, tiled=True)
     slots = experts * cap
-    copies = jnp.broadcast_to(rows.reshape(slots, LANES), (tp_size, slots, LANES))
-    features = lax.all_to_all(copies, TP, split_axis=0, concat_axis=0, tiled=True)
-    parts = expert(features, norm_gain.reshape(1, -1), gate_weight, up_weight, down_weight, 192)
-    parts = lax.all_to_all(parts, TP, split_axis=0, concat_axis=0, tiled=True)
-    summed = jnp.sum(parts.astype(F32), axis=0).astype(BF16)
-    returned = lax.all_to_all(summed.reshape(experts, cap, LANES), "sp", split_axis=0, concat_axis=0, tiled=True)
+    gain = norm_gain.reshape(1, -1)
+    returned = []
+    for piece in jnp.split(rows.reshape(slots, LANES), PIECES):
+        copies = jnp.broadcast_to(piece, (tp_size, *piece.shape))
+        features = lax.all_to_all(copies, PLANE, split_axis=0, concat_axis=0, tiled=True)
+        parts = expert(features, gain, gate_weight, up_weight, down_weight, 192)
+        parts = lax.all_to_all(parts, PLANE, split_axis=0, concat_axis=0, tiled=True)
+        returned.append(jnp.sum(parts.astype(F32), axis=0).astype(BF16))
+    returned = jnp.concatenate(returned, axis=0).reshape(experts, cap, LANES)
+    returned = lax.all_to_all(returned, "sp", split_axis=0, concat_axis=0, tiled=True)
     out = combine(returned.reshape(slots, LANES), take, route_weights, stream)
     return lax.all_to_all(out, TP, split_axis=0, concat_axis=1, tiled=True)
 

time: 210 us -> 220 us (1.048)
  blocking collectives: 133 us -> 72.6 us
  waiting for transfers between devices: 33 us -> 76.5 us
  starting transfers between devices: 14.5 us -> 35.6 us
  local copies, waits for them, and re-layouts: 6.82 us -> 19.9 us
  Pallas kernels: 19.6 us -> 8.72 us
  other arithmetic: 1.83 us -> 4.85 us
    all_to_all x2 -> x1, blocking collectives: 87 us -> 25.7 us  [per_device(): lax.all_to_all(copies, PLANE, split_axis=0, concat_axis=0, tiled=True)]
    all_to_all x2 -> x5, waiting for transfers between devices: 32.8 us -> 75.7 us  [the longest x2 29.4 us: per_device(): lax.all_to_all(parts, PLANE, split_axis=0, concat_axis=0, tiled=True)]
    all_to_all x2 -> x5, starting transfers between devices: 12.7 us -> 33.9 us  [the longest x2 11.7 us: per_device(): lax.all_to_all(parts, PLANE, split_axis=0, concat_axis=0, tiled=True)]
    unnamed x12 -> x38, local copies, waits for them, and re-layouts: 3.88 us -> 15.7 us
    pallas_call x5 -> x6, Pallas kernels: 19.6 us -> 8.72 us  [the longest x2 4.28 us: expert(): pl.pallas_call(functools.partial(expert_body, block), out_shape=vmem_out(...]
  transfers between devices with their start and end apart: 3 -> 6, of which waited for: 3 -> 6; matrix products, arithmetic and copies ran while one was open for 1% -> 1% of each run, Pallas kernels for 1% -> 2%
where the time goes in v3:
time: 220 us; the launch traced here: 218 us
  waiting for transfers between devices  76.5 us (35%)
  blocking collectives  72.6 us (33%)
  starting transfers between devices  35.6 us (16%)
  local copies, waits for them, and re-layouts  19.9 us (9%)
  Pallas kernels  8.72 us (4%)
  other arithmetic  4.85 us (2%)
    all_to_all x1, blocking collectives, per_device(): lax.all_to_all(rows.reshape(experts, cap, LANES), 'sp', split_axis=0, con...  35.4 us
    all_to_all x2, waiting for transfers between devices, per_device(): lax.all_to_all(parts, PLANE, split_axis=0, concat_axis=0, tiled=True)  29.4 us
    all_to_all x1, blocking collectives, per_device(): lax.all_to_all(copies, PLANE, split_axis=0, concat_axis=0, tiled=True)  25.7 us
    all_to_all x1, waiting for transfers between devices, per_device(): lax.all_to_all(returned, 'sp', split_axis=0, concat_axis=0, tiled=True)  19.8 us
    unnamed x38, local copies, waits for them, and re-layouts  15.7 us
    all_to_all x1, waiting for transfers between devices, per_device(): lax.all_to_all(partial, PLANE, split_axis=0, concat_axis=0, tiled=True)  15 us
    all_to_all x2, starting transfers between devices, per_device(): lax.all_to_all(parts, PLANE, split_axis=0, concat_axis=0, tiled=True)  11.7 us
    all_to_all x1, blocking collectives, per_device(): return lax.all_to_all(out, TP, split_axis=0, concat_axis=1, tiled=True)  11.5 us
  transfers between devices with their start and end apart: 6, of which 6 were waited for; matrix products, arithmetic and copies ran while one was open for 1% of the time, Pallas kernels for 2%

profile of v3, /device:TPU:2, one launch (start us, length us, event | category | flops | bytes accessed | tf_op | source)
XLA Modules:
  0.0 218.4 jit_solution(9864486265123673389)
XLA Ops:
  0.0 0.9 slice.8
  1.8 1.7 collective-permute-start
  4.5 1.0 copy-done.10
  5.6 0.9 copy-done.11
  8.9 2.9 %attention.1 = bf16[16,256,128]{2,1,0:T(8,128)(2,1)} custom-call(s32[2]{0:T(128)S(1)} %pad_add_fusion.place, f32[2]{0:T(128)S(1)} %copy-done.16, bf16[256,128]{1,0:T(8,128)(2,1)S(1)} %copy-done.13, bf16[256,256]{1,0:T(8,128)(2,1)S(1)} %copy-done.11, bf16[256,256]{1,0:T(8,128)(2,1)S(1)} %copy-done.12, bf16[128,512]{1,0:T(8,128)(2,1)S(1)} %collective-permute-done.before_ref, ...), custom_call_target="tpu_custom_call" | custom-call | tf_op jit(solution)/shard_map/attention/pallas_call | solution.py:101
  11.7 8.9 %all-to-all-start = ((bf16[16,256,128]{2,1,0:T(8,128)(2,1)}), bf16[16,256,128]{2,1,0:T(8,128)(2,1)S(1)}, u32[]{:S(2)}, u32[]{:S(2)}) async-start(bf16[16,256,128]{2,1,0:T(8,128)(2,1)} %attention.1), calls=%async_computation | async-start | bytes 2097152 | tf_op jit(solution)/shard_map/all_to_all | solution.py:243
  21.7 15.0 %all-to-all-done.arrived_ref = bf16[16,256,128]{2,1,0:T(8,128)(2,1)S(1)} async-done(((bf16[16,256,128]{2,1,0:T(8,128)(2,1)}), bf16[16,256,128]{2,1,0:T(8,128)(2,1)S(1)}, u32[]{:S(2)}, u32[]{:S(2)}) %all-to-all-start) | async-done | bytes 1048608 | tf_op jit(solution)/shard_map/all_to_all | solution.py:243
  37.0 35.4 %all_to_all.54 = bf16[32,24,128]{2,1,0:T(8,128)(2,1)S(1)} all-to-all(bf16[32,24,128]{2,1,0:T(8,128)(2,1)S(1)} %bitcast.18), channel_id=1, replica_groups=mesh['sp'=32,'tp_0'=4,'tp_1'=4] {'sp'}, dimensions={0} | all-to-all | bytes 393216 | tf_op jit(solution)/shard_map/all_to_all | solution.py:248
  72.8 25.7 %all_to_all.55.x_ref = bf16[16,384,128]{2,1,0:T(8,128)(2,1)} all-to-all(bf16[16,384,128]{2,1,0:T(8,128)(2,1)S(1)} %broadcast_in_dim.6), channel_id=1, replica_groups=mesh['sp'=32,'tp_0'=4,'tp_1'=4] {'tp_1','tp_0'}, dimensions={0} | all-to-all | bytes 3145728 | tf_op jit(solution)/shard_map/all_to_all | solution.py:254
  98.5 1.5 broadcast_in_dim.7
  100.0 6.0 %all-to-all-start.4 = ((bf16[16,384,128]{2,1,0:T(8,128)(2,1)}), bf16[16,384,128]{2,1,0:T(8,128)(2,1)S(1)}, u32[]{:S(2)}, u32[]{:S(2)}) async-start(bf16[16,384,128]{2,1,0:T(8,128)(2,1)} %broadcast_in_dim.7), calls=%async_computation.4 | async-start | bytes 3145728 | tf_op jit(solution)/shard_map/all_to_all | solution.py:254
  106.0 1.4 copy-done.3
  107.4 1.2 copy-done.4
  108.6 1.2 copy-done.6
  109.8 1.2 copy-done.8
  111.0 2.1 expert.2
  113.2 1.2 copy-done.1
  114.3 11.5 %all-to-all-done.4.x_ref = bf16[16,384,128]{2,1,0:T(8,128)(2,1)S(1)} async-done(((bf16[16,384,128]{2,1,0:T(8,128)(2,1)}), bf16[16,384,128]{2,1,0:T(8,128)(2,1)S(1)}, u32[]{:S(2)}, u32[]{:S(2)}) %all-to-all-start.4) | async-done | bytes 1572896 | tf_op jit(solution)/shard_map/all_to_all | solution.py:254
  125.8 6.3 %all-to-all-start.3 = ((bf16[16,384,128]{2,1,0:T(8,128)(2,1)}), bf16[16,384,128]{2,1,0:T(8,128)(2,1)}, u32[]{:S(2)}, u32[]{:S(2)}) async-start(bf16[16,384,128]{2,1,0:T(8,128)(2,1)} %copy-done.1), calls=%async_computation.3 | async-start | bytes 3145728 | tf_op jit(solution)/shard_map/all_to_all | solution.py:256
  132.1 1.2 copy-done.5
  133.3 1.2 copy-done.7
  134.6 1.2 copy-done.9
  135.8 2.2 expert.3
  138.0 1.1 copy-done.2
  139.1 12.6 %all-to-all-done.3 = bf16[16,384,128]{2,1,0:T(8,128)(2,1)} async-done(((bf16[16,384,128]{2,1,0:T(8,128)(2,1)}), bf16[16,384,128]{2,1,0:T(8,128)(2,1)}, u32[]{:S(2)}, u32[]{:S(2)}) %all-to-all-start.3) | async-done | bytes 1572896 | tf_op jit(solution)/shard_map/all_to_all | solution.py:256
  151.7 5.4 %all-to-all-start.5 = ((bf16[16,384,128]{2,1,0:T(8,128)(2,1)}), bf16[16,384,128]{2,1,0:T(8,128)(2,1)S(1)}, u32[]{:S(2)}, u32[]{:S(2)}) async-start(bf16[16,384,128]{2,1,0:T(8,128)(2,1)} %copy-done.2), calls=%async_computation.5 | async-start | bytes 3145728 | tf_op jit(solution)/shard_map/all_to_all | solution.py:256
  157.1 2.3 %reduce_sum.24 = bf16[384,128]{1,0:T(8,128)(2,1)} reduce(bf16[16,384,128]{2,1,0:T(8,128)(2,1)} %all-to-all-done.3, bf16[]{:T(256)} %constant.41.clone.1), dimensions={0}, to_apply=%region_0.1 | reduce | flops 737280 | bytes 1671170 | tf_op jit(solution)/shard_map/reduce_sum | solution.py:257
  159.4 16.8 %all-to-all-done.5 = bf16[16,384,128]{2,1,0:T(8,128)(2,1)S(1)} async-done(((bf16[16,384,128]{2,1,0:T(8,128)(2,1)}), bf16[16,384,128]{2,1,0:T(8,128)(2,1)S(1)}, u32[]{:S(2)}, u32[]{:S(2)}) %all-to-all-start.5) | async-done | bytes 1572896 | tf_op jit(solution)/shard_map/all_to_all | solution.py:256
  177.0 1.6 pad_maximum_fusion
  178.6 7.3 %all-to-all-start.6 = ((bf16[32,24,128]{2,1,0:T(8,128)(2,1)}), bf16[32,24,128]{2,1,0:T(8,128)(2,1)S(1)}, u32[]{:S(2)}, u32[]{:S(2)}) async-start(bf16[32,24,128]{2,1,0:T(8,128)(2,1)} %bitcast.7), calls=%async_computation.6 | async-start | bytes 393216 | tf_op jit(solution)/shard_map/all_to_all | solution.py:259
  186.1 19.8 %all-to-all-done.6 = bf16[32,24,128]{2,1,0:T(8,128)(2,1)S(1)} async-done(((bf16[32,24,128]{2,1,0:T(8,128)(2,1)}), bf16[32,24,128]{2,1,0:T(8,128)(2,1)S(1)}, u32[]{:S(2)}, u32[]{:S(2)}) %all-to-all-start.6) | async-done | bytes 196640 | tf_op jit(solution)/shard_map/all_to_all | solution.py:259
  206.3 11.5 %all_to_all.56 = bf16[16,16,128]{2,1,0:T(8,128)(2,1)S(1)} all-to-all(bf16[16,16,128]{2,1,0:T(8,128)(2,1)S(1)} %bitcast.17), channel_id=1, replica_groups=mesh['sp'=32,'tp_0'=4,'tp_1'=4] {'tp_0','tp_1'}, dimensions={0} | all-to-all | bytes 131072 | tf_op jit(solution)/shard_map/all_to_all | solution.py:261
  (39 shorter events, 7.9 us)
Async XLA Ops:
  0.0 21.6 %copy-start = (bf16[256,2048]{1,0:T(8,128)(2,1)S(1)}, bf16[256,2048]{1,0:T(8,128)(2,1)}, u32[]{:S(2)}) copy-start(bf16[256,2048]{1,0:T(8,128)(2,1)} %param.17) | copy-start | bytes 3145732
  1.8 2.7 %collective-permute-start = (bf16[128,512]{1,0:T(8,128)(2,1)S(1)}, bf16[128,512]{1,0:T(8,128)(2,1)S(1)}, u32[]{:S(2)}, u32[]{:S(2)}) collective-permute-start(bf16[128,512]{1,0:T(8,128)(2,1)S(1)} %pad_maximum_fusion.1), channel_id=1, source_target_pairs={{0,16},{16,32},{32,48},{48,64},{64,80},{80,96},{96,112},{112,128},... | collective-permute-start | bytes 393224 | tf_op jit(solution)/shard_map/ppermute | solution.py:241
  4.5 1.0 copy-start.10
  5.6 0.9 copy-start.11
  6.5 0.9 copy-start.12
  7.4 0.8 copy-start.13
  8.2 0.7 copy-start.16
  8.9 11.8 %copy-start.15 = (s32[256,2]{0,1:T(2,128)S(1)}, s32[256,2]{0,1:T(2,128)}, u32[]{:S(2)}) copy-start(s32[256,2]{0,1:T(2,128)} %param.19) | copy-start | bytes 6148
  11.7 24.9 %all-to-all-start = ((bf16[16,256,128]{2,1,0:T(8,128)(2,1)}), bf16[16,256,128]{2,1,0:T(8,128)(2,1)S(1)}, u32[]{:S(2)}, u32[]{:S(2)}) async-start(bf16[16,256,128]{2,1,0:T(8,128)(2,1)} %attention.1), calls=%async_computation | async-start | bytes 2097152 | tf_op jit(solution)/shard_map/all_to_all | solution.py:243
  100.0 6.0 %copy-start.14 = (f32[2048]{0:T(1024)S(1)}, f32[2048]{0:T(1024)}, u32[]{:S(2)}) copy-start(f32[2048]{0:T(1024)} %param.18) | copy-start | bytes 24580
  100.0 25.8 %all-to-all-start.4 = ((bf16[16,384,128]{2,1,0:T(8,128)(2,1)}), bf16[16,384,128]{2,1,0:T(8,128)(2,1)S(1)}, u32[]{:S(2)}, u32[]{:S(2)}) async-start(bf16[16,384,128]{2,1,0:T(8,128)(2,1)} %broadcast_in_dim.7), calls=%async_computation.4 | async-start | bytes 3145728 | tf_op jit(solution)/shard_map/all_to_all | solution.py:254
  106.0 1.4 copy-start.3
  107.4 1.2 copy-start.4
  108.6 1.2 copy-start.6
  109.8 1.2 copy-start.8
  113.1 1.2 copy-start.1
  125.8 25.9 %all-to-all-start.3 = ((bf16[16,384,128]{2,1,0:T(8,128)(2,1)}), bf16[16,384,128]{2,1,0:T(8,128)(2,1)}, u32[]{:S(2)}, u32[]{:S(2)}) async-start(bf16[16,384,128]{2,1,0:T(8,128)(2,1)} %copy-done.1), calls=%async_computation.3 | async-start | bytes 3145728 | tf_op jit(solution)/shard_map/all_to_all | solution.py:256
  132.1 1.2 copy-start.5
  133.3 1.2 copy-start.7
  134.6 1.2 copy-start.9
  138.0 1.1 copy-start.2
  151.7 24.5 %all-to-all-start.5 = ((bf16[16,384,128]{2,1,0:T(8,128)(2,1)}), bf16[16,384,128]{2,1,0:T(8,128)(2,1)S(1)}, u32[]{:S(2)}, u32[]{:S(2)}) async-start(bf16[16,384,128]{2,1,0:T(8,128)(2,1)} %copy-done.2), calls=%async_computation.5 | async-start | bytes 3145728 | tf_op jit(solution)/shard_map/all_to_all | solution.py:256
  159.4 26.6 %copy-start.17 = (f32[256,2]{0,1:T(2,128)S(1)}, f32[256,2]{0,1:T(2,128)}, u32[]{:S(2)}) copy-start(f32[256,2]{0,1:T(2,128)} %param.20) | copy-start | bytes 6148
  178.6 27.3 %all-to-all-start.6 = ((bf16[32,24,128]{2,1,0:T(8,128)(2,1)}), bf16[32,24,128]{2,1,0:T(8,128)(2,1)S(1)}, u32[]{:S(2)}, u32[]{:S(2)}) async-start(bf16[32,24,128]{2,1,0:T(8,128)(2,1)} %bitcast.7), calls=%async_computation.6 | async-start | bytes 393216 | tf_op jit(solution)/shard_map/all_to_all | solution.py:259

commit v4 on v3

--- a/solution.py
+++ b/solution.py
@@ -21,11 +21,19 @@
 SMEM_SPEC = pl.BlockSpec(memory_space=pltpu.SMEM)
 PLANE = ("tp_1", "tp_0")
 SIDE = 4
-PIECES = 2
+LAG_NS = 16000
 
 
 def in_vmem(*arrays):
     return [pltpu.with_memory_space_constraint(a, pltpu.VMEM) for a in arrays]
+
+
+def in_hbm(*arrays):
+    return [pltpu.with_memory_space_constraint(a, pltpu.HBM) for a in arrays]
+
+
+def small_kernel(mib):
+    return pltpu.CompilerParams(vmem_limit_bytes=mib * 2**20)
 
 
 def vmem_out(shape):
@@ -103,9 +111,71 @@
         out_shape=vmem_out((shares, q.shape[0], LANES)),
         in_specs=[SMEM_SPEC, SMEM_SPEC] + [VMEM_SPEC] * 5,
         out_specs=VMEM_SPEC,
-        compiler_params=pltpu.CompilerParams(vmem_limit_bytes=16 * 2**20),
+        compiler_params=small_kernel(16),
         name="attention",
-    )(place, sinks, q, k, v, *in_vmem(before), w)
+    )(place, *in_hbm(sinks, q, k, v), *in_vmem(before), *in_hbm(w))
+
+
+def pack_body(k_ref, v_ref, out_ref):
+    width = k_ref.shape[1]
+    out_ref[:, :width] = k_ref[...]
+    out_ref[:, width:] = v_ref[...]
+
+
+def last_window(k, v):
+    rows, width = k.shape
+    tail = pl.BlockSpec((WINDOW, width), lambda i: (rows // WINDOW - 1, 0))
+    return pl.pallas_call(
+        pack_body,
+        grid=(1,),
+        out_shape=vmem_out((WINDOW, 2 * width)),
+        in_specs=[tail, tail],
+        out_specs=VMEM_SPEC,
+        compiler_params=small_kernel(16),
+        name="pack",
+    )(*in_hbm(k, v))
+
+
+def copies_body(place, rows_ref, out_ref):
+    @pl.when(place[0] % 2 == 1)
+    def _():
+        pl.delay(LAG_NS)
+
+    rows = rows_ref[...]
+    for t in range(out_ref.shape[0]):
+        out_ref[t] = rows
+
+
+def copied(place, rows, count):
+    return pl.pallas_call(
+        copies_body,
+        out_shape=vmem_out((count, *rows.shape)),
+        in_specs=[SMEM_SPEC, VMEM_SPEC],
+        out_specs=VMEM_SPEC,
+        compiler_params=small_kernel(16),
+        name="copies",
+    )(place, *in_vmem(rows))
+
+
+def total_body(parts_ref, out_ref):
+    rows = parts_ref.shape[1]
+    block = 128
+    for lo in range(0, rows, block):
+        summed = parts_ref[0, lo : lo + block, :].astype(F32)
+        for t in range(1, parts_ref.shape[0]):
+            summed = summed + parts_ref[t, lo : lo + block, :].astype(F32)
+        out_ref[lo : lo + block, :] = summed.astype(BF16)
+
+
+def total(parts):
+    return pl.pallas_call(
+        total_body,
+        out_shape=vmem_out(parts.shape[1:]),
+        in_specs=[VMEM_SPEC],
+        out_specs=VMEM_SPEC,
+        compiler_params=small_kernel(16),
+        name="total",
+    )(*in_vmem(parts))
 
 
 def slots_body(cap, experts, routes_ref, wide_ref, send_ref, take_ref):
@@ -147,7 +217,7 @@
         ),
         in_specs=[VMEM_SPEC] * 2,
         out_specs=(VMEM_SPEC, VMEM_SPEC),
-        compiler_params=pltpu.CompilerParams(vmem_limit_bytes=16 * 2**20),
+        compiler_params=small_kernel(16),
         name="slots",
     )(*in_vmem(routes, routes.T))
 
@@ -167,21 +237,30 @@
         out_shape=(vmem_out(own.shape), vmem_out((send.shape[0], LANES))),
         in_specs=[VMEM_SPEC] * 3,
         out_specs=(VMEM_SPEC, VMEM_SPEC),
-        compiler_params=pltpu.CompilerParams(vmem_limit_bytes=16 * 2**20),
+        compiler_params=small_kernel(16),
         name="stream",
     )(*in_vmem(arrived, own, send))
 
 
-def expert_body(block, x_ref, gain_ref, gate_ref, up_ref, down_ref, out_ref):
+def expert_body(block, x_ref, gain_ref, gate_hbm, up_hbm, down_hbm, out_ref, gate_ref, up_ref, down_ref, sems):
+    pairs = ((gate_hbm, gate_ref), (up_hbm, up_ref), (down_hbm, down_ref))
+    copies = [pltpu.make_async_copy(source, target, sems.at[i]) for i, (source, target) in enumerate(pairs)]
+    for copy in copies:
+        copy.start()
     shares, rows, _ = x_ref.shape
     order = sorted(range(shares), key=lambda p: share_of(p, SIDE))
     for lo in range(0, rows, block):
         stream = jnp.concatenate([x_ref[p, lo : lo + block, :] for p in order], axis=1).astype(F32)
         scale = lax.rsqrt(jnp.mean(stream * stream, axis=-1, keepdims=True) + NORM_EPS)
         normed = (stream * scale * gain_ref[...]).astype(BF16)
+        if lo == 0:
+            copies[0].wait()
+            copies[1].wait()
         gate_act = dot(normed, gate_ref[0])
         up_act = dot(normed, up_ref[0])
         hidden = (gate_act * jax.nn.sigmoid(gate_act) * up_act).astype(BF16)
+        if lo == 0:
+            copies[2].wait()
         for p in range(shares):
             t = share_of(p, SIDE)
             out_ref[p, lo : lo + block, :] = dot(hidden, down_ref[0, :, t * LANES : (t + 1) * LANES]).astype(BF16)
@@ -191,12 +270,13 @@
     return pl.pallas_call(
         functools.partial(expert_body, block),
         out_shape=vmem_out(x.shape),
-        in_specs=[VMEM_SPEC] * 5,
-        out_specs=VMEM_SPEC,
+        in_specs=[VMEM_SPEC] * 2 + [pl.BlockSpec(memory_space=pltpu.HBM)] * 3,
+        out_specs=VMEM_SPEC,
+        scratch_shapes=[pltpu.VMEM(a.shape, BF16) for a in (gate, up, down)] + [pltpu.SemaphoreType.DMA((3,))],
         cost_estimate=pl.CostEstimate(flops=6 * x.shape[1] * gate.shape[1] * gate.shape[2], bytes_accessed=2 * x.size * 2, transcendentals=0),
-        compiler_params=pltpu.CompilerParams(vmem_limit_bytes=24 * 2**20),
+        compiler_params=small_kernel(24),
         name="expert",
-    )(*in_vmem(x), gain, gate, up, down)
+    )(*in_vmem(x, gain), *in_hbm(gate, up, down))
 
 
 def combine_body(rows_ref, take_ref, weights_ref, stream_ref, out_ref):
@@ -212,7 +292,7 @@
         out_shape=vmem_out(stream.shape),
         in_specs=[VMEM_SPEC] * 4,
         out_specs=VMEM_SPEC,
-        compiler_params=pltpu.CompilerParams(vmem_limit_bytes=16 * 2**20),
+        compiler_params=small_kernel(16),
         name="combine",
     )(*in_vmem(rows, take), weights, *in_vmem(stream))
 
@@ -237,7 +317,7 @@
     experts = lax.axis_size("sp")
     tp_index = lax.axis_index(TP)
     place = jnp.stack([lax.axis_index("sp"), tp_index * local_heads // REP]).astype(jnp.int32)
-    last = jnp.concatenate([key_rows[tokens - WINDOW :], value_rows[tokens - WINDOW :]], axis=1)
+    last = last_window(key_rows, value_rows)
     before = lax.ppermute(last, "sp", [(i, i + 1) for i in range(experts - 1)])
     partial = attention(place, sink_logits, query_rows, key_rows, value_rows, before, out_weight)
     arrived = lax.all_to_all(partial, PLANE, split_axis=0, concat_axis=0, tiled=True)
@@ -248,15 +328,10 @@
     rows = lax.all_to_all(rows.reshape(experts, cap, LANES), "sp", split_axis=0, concat_axis=0, tiled=True)
     slots = experts * cap
     gain = norm_gain.reshape(1, -1)
-    returned = []
-    for piece in jnp.split(rows.reshape(slots, LANES), PIECES):
-        copies = jnp.broadcast_to(piece, (tp_size, *piece.shape))
-        features = lax.all_to_all(copies, PLANE, split_axis=0, concat_axis=0, tiled=True)
-        parts = expert(features, gain, gate_weight, up_weight, down_weight, 192)
-        parts = lax.all_to_all(parts, PLANE, split_axis=0, concat_axis=0, tiled=True)
-        returned.append(jnp.sum(parts.astype(F32), axis=0).astype(BF16))
-    returned = jnp.concatenate(returned, axis=0).reshape(experts, cap, LANES)
-    returned = lax.all_to_all(returned, "sp", split_axis=0, concat_axis=0, tiled=True)
+    features = lax.all_to_all(copied(place, rows.reshape(slots, LANES), tp_size), PLANE, split_axis=0, concat_axis=0, tiled=True)
+    parts = expert(features, gain, gate_weight, up_weight, down_weight, 192)
+    summed = total(lax.all_to_all(parts, PLANE, split_axis=0, concat_axis=0, tiled=True))
+    returned = lax.all_to_all(summed.reshape(experts, cap, LANES), "sp", split_axis=0, concat_axis=0, tiled=True)
     out = combine(returned.reshape(slots, LANES), take, route_weights, stream)
     return lax.all_to_all(out, TP, split_axis=0, concat_axis=1, tiled=True)
 

time: 220 us -> 185 us (0.84)
  waiting for transfers between devices: 76.5 us -> 35.7 us
  blocking collectives: 72.6 us -> 110 us
  local copies, waits for them, and re-layouts: 19.9 us -> 0.95 us
  starting transfers between devices: 35.6 us -> 24.3 us
  Pallas kernels: 8.72 us -> 13.8 us
  other arithmetic: 4.85 us -> 0.08 us
    all_to_all x4 -> x1, waiting for transfers between devices: 60.7 us -> 19.8 us  [per_device(): lax.all_to_all(summed.reshape(experts, cap, LANES), 'sp', split_axis=0, c...]
    all_to_all x1 -> x2, blocking collectives: 25.7 us -> 62.8 us  [the longest x1 32.1 us: per_device(): lax.all_to_all(parts, PLANE, split_axis=0, concat_axis=0, tiled=True)]
    unnamed x38 -> x10, local copies, waits for them, and re-layouts: 15.7 us -> 0.28 us
    all_to_all x4 -> x1, starting transfers between devices: 25 us -> 13.7 us  [per_device(): lax.all_to_all(summed.reshape(experts, cap, LANES), 'sp', split_axis=0, c...]
    pallas_call x0 -> x3, Pallas kernels: none -> 3.21 us  [the longest x1 1.15 us: copied(): pl.pallas_call(copies_body, out_shape=vmem_out((count, *rows.shape)), in_...]
    reduce_sum x2 -> x0, other arithmetic: 3.13 us -> none  [per_device(): returned.append(jnp.sum(parts.astype(F32), axis=0).astype(BF16))]
    pallas_call x2 -> x1, Pallas kernels: 4.28 us -> 5.47 us  [expert(): pl.pallas_call(functools.partial(expert_body, block), out_shape=vmem_out(...]
  transfers between devices with their start and end apart: 6 -> 3, of which waited for: 6 -> 3; matrix products, arithmetic and copies ran while one was open for 1% -> 0% of each run, Pallas kernels for 2% -> 0%
where the time goes in v4:
time: 185 us
  blocking collectives  110 us (59%)
  waiting for transfers between devices  35.7 us (19%)
  starting transfers between devices  24.3 us (13%)
  Pallas kernels  13.8 us (7%)
    all_to_all x1, blocking collectives, per_device(): lax.all_to_all(rows.reshape(experts, cap, LANES), 'sp', split_axis=0, con...  35.4 us
    all_to_all x1, blocking collectives, per_device(): lax.all_to_all(parts, PLANE, split_axis=0, concat_axis=0, tiled=True)  32.1 us
    all_to_all x1, blocking collectives, per_device(): lax.all_to_all(copied(place, rows.reshape(slots, LANES), tp_size), PLANE,...  30.7 us
    all_to_all x1, waiting for transfers between devices, per_device(): lax.all_to_all(summed.reshape(experts, cap, LANES), 'sp', split_axis=0, c...  19.8 us
    all_to_all x1, waiting for transfers between devices, per_device(): lax.all_to_all(partial, PLANE, split_axis=0, concat_axis=0, tiled=True)  15 us
    all_to_all x1, starting transfers between devices, per_device(): lax.all_to_all(summed.reshape(experts, cap, LANES), 'sp', split_axis=0, c...  13.7 us
    all_to_all x1, blocking collectives, per_device(): return lax.all_to_all(out, TP, split_axis=0, concat_axis=1, tiled=True)  11.8 us
    all_to_all x1, starting transfers between devices, per_device(): lax.all_to_all(partial, PLANE, split_axis=0, concat_axis=0, tiled=True)  8.89 us
  transfers between devices with their start and end apart: 3, of which 3 were waited for; matrix products, arithmetic and copies ran while one was open for 0% of the time, Pallas kernels for 0%

profile of v4, /device:TPU:2, one launch (start us, length us, event | category | flops | bytes accessed | tf_op | source)
XLA Modules:
  0.0 184.9 jit_solution(14188771558036846782)
XLA Ops:
  0.0 0.0 copy-start
  0.0 0.0 copy-start.1
  0.0 1.0 pack.1
  1.0 1.7 collective-permute-start
  2.8 0.1 pad_add_fusion.place
  2.8 0.9 collective-permute-done.before_ref
  3.7 3.5 %attention.1 = bf16[16,256,128]{2,1,0:T(8,128)(2,1)} custom-call(s32[2]{0:T(128)S(1)} %pad_add_fusion.place, f32[2]{0:T(128)} %sinks.1, bf16[256,128]{1,0:T(8,128)(2,1)} %q_ref.1, bf16[256,256]{1,0:T(8,128)(2,1)} %k_ref.3, bf16[256,256]{1,0:T(8,128)(2,1)} %v_ref.3, bf16[128,512]{1,0:T(8,128)(2,1)S(1)} %collective-permute-done.before_ref, bf16[128,2048]{1,0:T(8,128)(2,1)} %w_ref.1), custom_call_target="tpu_custom_call" | custom-call | tf_op jit(solution)/shard_map/attention/pallas_call | solution.py:109
  7.2 8.9 %all-to-all-start = ((bf16[16,256,128]{2,1,0:T(8,128)(2,1)}), bf16[16,256,128]{2,1,0:T(8,128)(2,1)S(1)}, u32[]{:S(2)}, u32[]{:S(2)}) async-start(bf16[16,256,128]{2,1,0:T(8,128)(2,1)} %attention.1), calls=%async_computation | async-start | bytes 2097152 | tf_op jit(solution)/shard_map/all_to_all | solution.py:323
  16.1 0.0 copy-done.1
  16.1 0.1 copy.13.routes_ref
  16.3 0.8 slots.1
  17.1 0.0 copy-done
  17.1 15.0 %all-to-all-done.arrived_ref = bf16[16,256,128]{2,1,0:T(8,128)(2,1)S(1)} async-done(((bf16[16,256,128]{2,1,0:T(8,128)(2,1)}), bf16[16,256,128]{2,1,0:T(8,128)(2,1)S(1)}, u32[]{:S(2)}, u32[]{:S(2)}) %all-to-all-start) | async-done | bytes 1048608 | tf_op jit(solution)/shard_map/all_to_all | solution.py:323
  32.1 0.4 stream.1
  32.5 35.4 %all_to_all.44 = bf16[32,24,128]{2,1,0:T(8,128)(2,1)S(1)} all-to-all(bf16[32,24,128]{2,1,0:T(8,128)(2,1)S(1)} %bitcast.18), channel_id=1, replica_groups=mesh['sp'=32,'tp_0'=4,'tp_1'=4] {'sp'}, dimensions={0} | all-to-all | bytes 393216 | tf_op jit(solution)/shard_map/all_to_all | solution.py:328
  67.9 1.2 copies.1
  69.1 0.0 copy-start.2
  69.1 30.7 %all_to_all.45.x_ref = bf16[16,768,128]{2,1,0:T(8,128)(2,1)S(1)} all-to-all(bf16[16,768,128]{2,1,0:T(8,128)(2,1)S(1)} %copies.1), channel_id=1, replica_groups=mesh['sp'=32,'tp_0'=4,'tp_1'=4] {'tp_1','tp_0'}, dimensions={0} | all-to-all | bytes 6291456 | tf_op jit(solution)/shard_map/all_to_all | solution.py:331
  99.8 0.0 copy-done.2
  99.8 5.5 %expert.1 = bf16[16,768,128]{2,1,0:T(8,128)(2,1)S(1)} custom-call(bf16[16,768,128]{2,1,0:T(8,128)(2,1)S(1)} %all_to_all.45.x_ref, f32[1,2048]{1,0:T(1,128)S(1)} %bitcast.20, bf16[1,2048,256]{2,1,0:T(8,128)(2,1)} %gate_hbm.1, bf16[1,2048,256]{2,1,0:T(8,128)(2,1)} %up_hbm.1, bf16[1,256,2048]{2,1,0:T(8,128)(2,1)} %down_hbm.1), custom_call_target="tpu_custom_call" | custom-call | flops 2415919104 | bytes 6291456 | tf_op jit(solution)/shard_map/expert/pallas_call | solution.py:270
  105.3 32.1 %all_to_all.46.parts_ref = bf16[16,768,128]{2,1,0:T(8,128)(2,1)S(1)} all-to-all(bf16[16,768,128]{2,1,0:T(8,128)(2,1)S(1)} %expert.1), channel_id=1, replica_groups=mesh['sp'=32,'tp_0'=4,'tp_1'=4] {'tp_1','tp_0'}, dimensions={0} | all-to-all | bytes 6291456 | tf_op jit(solution)/shard_map/all_to_all | solution.py:333
  137.4 0.0 copy-start.3
  137.4 1.1 total.1
  138.4 13.7 %all-to-all-start.4 = ((bf16[32,24,128]{2,1,0:T(8,128)(2,1)}), bf16[32,24,128]{2,1,0:T(8,128)(2,1)S(1)}, u32[]{:S(2)}, u32[]{:S(2)}) async-start(bf16[32,24,128]{2,1,0:T(8,128)(2,1)} %bitcast.6), calls=%async_computation.4 | async-start | bytes 393216 | tf_op jit(solution)/shard_map/all_to_all | solution.py:334
  152.2 0.0 copy-done.3
  152.2 0.1 copy.14.weights_ref
  152.3 19.8 %all-to-all-done.4 = bf16[32,24,128]{2,1,0:T(8,128)(2,1)S(1)} async-done(((bf16[32,24,128]{2,1,0:T(8,128)(2,1)}), bf16[32,24,128]{2,1,0:T(8,128)(2,1)S(1)}, u32[]{:S(2)}, u32[]{:S(2)}) %all-to-all-start.4) | async-done | bytes 196640 | tf_op jit(solution)/shard_map/all_to_all | solution.py:334
  172.1 0.4 combine.1
  172.5 11.8 %all_to_all.47 = bf16[16,16,128]{2,1,0:T(8,128)(2,1)S(1)} all-to-all(bf16[16,16,128]{2,1,0:T(8,128)(2,1)S(1)} %bitcast.17), channel_id=1, replica_groups=mesh['sp'=32,'tp_0'=4,'tp_1'=4] {'tp_0','tp_1'}, dimensions={0} | all-to-all | bytes 131072 | tf_op jit(solution)/shard_map/all_to_all | solution.py:336
  184.3 0.6 copy_bitcast_fusion
  (1 shorter events, 0.0 us)
Async XLA Ops:
  0.0 17.1 %copy-start = (bf16[256,2048]{1,0:T(8,128)(2,1)S(1)}, bf16[256,2048]{1,0:T(8,128)(2,1)}, u32[]{:S(2)}) copy-start(bf16[256,2048]{1,0:T(8,128)(2,1)} %param.17) | copy-start | bytes 3145732
  0.0 16.1 %copy-start.1 = (s32[256,2]{0,1:T(2,128)S(1)}, s32[256,2]{0,1:T(2,128)}, u32[]{:S(2)}) copy-start(s32[256,2]{0,1:T(2,128)} %param.19) | copy-start | bytes 6148
  1.0 2.7 %collective-permute-start = (bf16[128,512]{1,0:T(8,128)(2,1)S(1)}, bf16[128,512]{1,0:T(8,128)(2,1)S(1)}, u32[]{:S(2)}, u32[]{:S(2)}) collective-permute-start(bf16[128,512]{1,0:T(8,128)(2,1)S(1)} %pack.1), channel_id=1, source_target_pairs={{0,16},{16,32},{32,48},{48,64},{64,80},{80,96},{96,112},{112,128},... | collective-permute-start | bytes 393224 | tf_op jit(solution)/shard_map/ppermute | solution.py:321
  7.2 24.9 %all-to-all-start = ((bf16[16,256,128]{2,1,0:T(8,128)(2,1)}), bf16[16,256,128]{2,1,0:T(8,128)(2,1)S(1)}, u32[]{:S(2)}, u32[]{:S(2)}) async-start(bf16[16,256,128]{2,1,0:T(8,128)(2,1)} %attention.1), calls=%async_computation | async-start | bytes 2097152 | tf_op jit(solution)/shard_map/all_to_all | solution.py:323
  69.1 30.7 %copy-start.2 = (f32[2048]{0:T(1024)S(1)}, f32[2048]{0:T(1024)}, u32[]{:S(2)}) copy-start(f32[2048]{0:T(1024)} %param.18) | copy-start | bytes 24580
  137.4 14.8 %copy-start.3 = (f32[256,2]{0,1:T(2,128)S(1)}, f32[256,2]{0,1:T(2,128)}, u32[]{:S(2)}) copy-start(f32[256,2]{0,1:T(2,128)} %param.20) | copy-start | bytes 6148
  138.4 33.7 %all-to-all-start.4 = ((bf16[32,24,128]{2,1,0:T(8,128)(2,1)}), bf16[32,24,128]{2,1,0:T(8,128)(2,1)S(1)}, u32[]{:S(2)}, u32[]{:S(2)}) async-start(bf16[32,24,128]{2,1,0:T(8,128)(2,1)} %bitcast.6), calls=%async_computation.4 | async-start | bytes 393216 | tf_op jit(solution)/shard_map/all_to_all | solution.py:334

commit v5 on v4

--- a/solution.py
+++ b/solution.py
@@ -21,7 +21,7 @@
 SMEM_SPEC = pl.BlockSpec(memory_space=pltpu.SMEM)
 PLANE = ("tp_1", "tp_0")
 SIDE = 4
-LAG_NS = 16000
+LAG_NS = 17000
 
 
 def in_vmem(*arrays):
@@ -48,92 +48,124 @@
     return lax.dot_general(a, b, (((contract[0],), (contract[1],)), ((), ())), preferred_element_type=F32)
 
 
-def head_pair(block, half):
+def both_places(block):
     swapped = jnp.concatenate([block[:, HEAD_DIM:], block[:, :HEAD_DIM]], axis=1)
-    lane = lax.broadcasted_iota(jnp.int32, block.shape, 1)
-    low = jnp.where(half == 0, block, swapped)
-    high = jnp.where(half == 0, swapped, block)
+    low = lax.broadcasted_iota(jnp.int32, block.shape, 1) < HEAD_DIM
     zero = jnp.zeros_like(block)
-    return jnp.where(lane < HEAD_DIM, low, zero), jnp.where(lane >= HEAD_DIM, high, zero)
-
-
-def attention_body(place, sinks, q_ref, k_ref, v_ref, before_ref, w_ref, out_ref):
-    first_block = place[0] == 0
-    group = place[1]
-    half = group % 2
-    pair = group // 2
-    pairs = k_ref.shape[1] // LANES
-
-    def chosen(ref, row0, rows, col0):
-        picked = ref[row0 : row0 + rows, col0 : col0 + LANES]
-        for i in range(1, pairs):
-            picked = jnp.where(pair == i, ref[row0 : row0 + rows, col0 + i * LANES : col0 + (i + 1) * LANES], picked)
-        return picked.astype(F32)
-
-    rows = q_ref.shape[0]
-    width = k_ref.shape[1]
-    keys = jnp.concatenate([chosen(before_ref, 0, WINDOW, 0), chosen(k_ref, 0, rows, 0)], axis=0)
-    values = jnp.concatenate([chosen(before_ref, 0, WINDOW, width), chosen(v_ref, 0, rows, 0)], axis=0)
-    keys = [k.astype(BF16) for k in head_pair(keys, half)]
-    values = [v.astype(BF16) for v in head_pair(values, half)]
-    row = lax.broadcasted_iota(jnp.int32, (WINDOW, 2 * WINDOW), 0)
-    col = lax.broadcasted_iota(jnp.int32, (WINDOW, 2 * WINDOW), 1)
-    inside = (col > row) & (col <= row + WINDOW)
-    parts = []
-    for block in range(rows // WINDOW):
-        lo = block * WINDOW
-        allowed = inside
-        if block == 0:
-            allowed = inside & ((col >= WINDOW) | jnp.logical_not(first_block))
-        q = q_ref[lo : lo + WINDOW, :]
-        total = None
-        for h in range(2):
-            scores = dot(q, keys[h][lo : lo + 2 * WINDOW], (1, 1)) * HEAD_DIM**-0.5
-            scores = jnp.where(allowed, scores, -1e30)
-            sink = sinks[h]
-            peak = jnp.maximum(jnp.max(scores, axis=-1, keepdims=True), sink)
-            terms = jnp.exp(scores - peak)
-            total_terms = jnp.sum(terms, axis=-1, keepdims=True) + jnp.exp(sink - peak)
-            probs = (terms / total_terms).astype(BF16)
-            part = dot(probs, values[h][lo : lo + 2 * WINDOW])
-            total = part if total is None else total + part
-        parts.append(total.astype(BF16))
-    attended = jnp.concatenate(parts, axis=0)
+    keys = (jnp.where(low, block, zero), jnp.where(low, zero, swapped))
+    values = (jnp.where(low, swapped, zero), jnp.where(low, zero, block))
+    return [k.astype(BF16) for k in keys], [v.astype(BF16) for v in values]
+
+
+def attend(q, keys, values, allowed, sinks):
+    total = None
+    for h in range(2):
+        scores = dot(q, keys[h], (1, 1)) * HEAD_DIM**-0.5
+        scores = jnp.where(allowed, scores, -1e30)
+        sink = sinks[h]
+        peak = jnp.maximum(jnp.max(scores, axis=-1, keepdims=True), sink)
+        terms = jnp.exp(scores - peak)
+        total_terms = jnp.sum(terms, axis=-1, keepdims=True) + jnp.exp(sink - peak)
+        probs = (terms / total_terms).astype(BF16)
+        part = dot(probs, values[h])
+        total = part if total is None else total + part
+    return total.astype(BF16)
+
+
+def project(attended, w_ref, out_ref):
     for p in range(out_ref.shape[0]):
         t = share_of(p, SIDE)
         out_ref[p] = dot(attended, w_ref[:, t * LANES : (t + 1) * LANES]).astype(BF16)
 
 
-def attention(place, sinks, q, k, v, before, w):
+def window_mask():
+    row = lax.broadcasted_iota(jnp.int32, (WINDOW, 2 * WINDOW), 0)
+    col = lax.broadcasted_iota(jnp.int32, (WINDOW, 2 * WINDOW), 1)
+    return (col > row) & (col <= row + WINDOW), col
+
+
+def later_body(sinks, q_ref, kv_ref, w_ref, out_ref):
+    keys, values = both_places(kv_ref[...].astype(F32))
+    inside, _ = window_mask()
+    project(attend(q_ref[WINDOW:, :], keys, values, inside, sinks), w_ref, out_ref)
+
+
+def first_body(place, sinks, q_ref, kv_ref, before_ref, w_ref, partial_ref, out_ref):
+    keys, values = both_places(jnp.concatenate([before_ref[...], kv_ref[:WINDOW, :]], axis=0).astype(F32))
+    inside, col = window_mask()
+    allowed = inside & ((col >= WINDOW) | (place[0] > 0))
+    project(attend(q_ref[:WINDOW, :], keys, values, allowed, sinks), w_ref, out_ref)
+
+
+def half_out(shares, at):
+    return pl.BlockSpec((shares, WINDOW, LANES), lambda i: (0, at, 0))
+
+
+def attention_later(sinks, q, kv, w):
     shares = w.shape[1] // LANES
     return pl.pallas_call(
-        attention_body,
-        out_shape=vmem_out((shares, q.shape[0], LANES)),
-        in_specs=[SMEM_SPEC, SMEM_SPEC] + [VMEM_SPEC] * 5,
-        out_specs=VMEM_SPEC,
-        compiler_params=small_kernel(16),
-        name="attention",
-    )(place, *in_hbm(sinks, q, k, v), *in_vmem(before), *in_hbm(w))
-
-
-def pack_body(k_ref, v_ref, out_ref):
-    width = k_ref.shape[1]
-    out_ref[:, :width] = k_ref[...]
-    out_ref[:, width:] = v_ref[...]
-
-
-def last_window(k, v):
-    rows, width = k.shape
-    tail = pl.BlockSpec((WINDOW, width), lambda i: (rows // WINDOW - 1, 0))
-    return pl.pallas_call(
-        pack_body,
+        later_body,
         grid=(1,),
-        out_shape=vmem_out((WINDOW, 2 * width)),
-        in_specs=[tail, tail],
-        out_specs=VMEM_SPEC,
-        compiler_params=small_kernel(16),
-        name="pack",
-    )(*in_hbm(k, v))
+        out_shape=pltpu.HBM((shares, q.shape[0], LANES), BF16),
+        in_specs=[SMEM_SPEC] + [VMEM_SPEC] * 3,
+        out_specs=half_out(shares, 1),
+        compiler_params=small_kernel(16),
+        cost_estimate=pl.CostEstimate(flops=10**9, bytes_accessed=2**20, transcendentals=2**16),
+        name="attention_later",
+    )(*in_hbm(sinks), *in_vmem(q, kv, w))
+
+
+def attention_first(place, sinks, q, kv, before, w, partial):
+    shares = w.shape[1] // LANES
+    return pl.pallas_call(
+        first_body,
+        grid=(1,),
+        out_shape=pltpu.HBM(partial.shape, BF16),
+        in_specs=[SMEM_SPEC, SMEM_SPEC] + [VMEM_SPEC] * 4 + [pl.BlockSpec(memory_space=pltpu.HBM)],
+        out_specs=half_out(shares, 0),
+        input_output_aliases={6: 0},
+        compiler_params=small_kernel(16),
+        name="attention_first",
+    )(place, *in_hbm(sinks), *in_vmem(q, kv, before, w), *in_hbm(partial))
+
+
+def load_body(q_hbm, k_hbm, v_hbm, w_hbm, last_ref, kv_ref, q_ref, w_ref, k_ref, v_ref, sems):
+    pairs = ((k_hbm, k_ref), (v_hbm, v_ref), (q_hbm, q_ref), (w_hbm, w_ref))
+    copies = [pltpu.make_async_copy(source, target, sems.at[i]) for i, (source, target) in enumerate(pairs)]
+    for copy in copies:
+        copy.start()
+    group = lax.axis_index(TP) * (q_ref.shape[1] // HEAD_DIM) // REP
+    low = lax.broadcasted_iota(jnp.int32, kv_ref.shape, 1) < HEAD_DIM
+
+    def head(ref):
+        picked = ref[:, :LANES].astype(F32)
+        for c in range(LANES, ref.shape[1], LANES):
+            picked = jnp.where(group // 2 == c // LANES, ref[:, c : c + LANES].astype(F32), picked)
+        return picked, jnp.concatenate([picked[:, HEAD_DIM:], picked[:, :HEAD_DIM]], axis=1)
+
+    copies[0].wait()
+    key, key_swapped = head(k_ref)
+    copies[1].wait()
+    value, value_swapped = head(v_ref)
+    odd = group % 2 == 1
+    kv = jnp.where(low, jnp.where(odd, key_swapped, key), jnp.where(odd, value, value_swapped)).astype(BF16)
+    kv_ref[...] = kv
+    last_ref[...] = kv[kv.shape[0] - WINDOW :]
+    copies[2].wait()
+    copies[3].wait()
+
+
+def loaded(q, k, v, w):
+    rows = q.shape[0]
+    return pl.pallas_call(
+        load_body,
+        out_shape=(vmem_out((WINDOW, LANES)), vmem_out((rows, LANES)), vmem_out(q.shape), vmem_out(w.shape)),
+        in_specs=[pl.BlockSpec(memory_space=pltpu.HBM)] * 4,
+        out_specs=(VMEM_SPEC,) * 4,
+        scratch_shapes=[pltpu.VMEM(k.shape, BF16), pltpu.VMEM(v.shape, BF16), pltpu.SemaphoreType.DMA((4,))],
+        compiler_params=small_kernel(16),
+        name="load",
+    )(*in_hbm(q, k, v, w))
 
 
 def copies_body(place, rows_ref, out_ref):
@@ -242,25 +274,16 @@
     )(*in_vmem(arrived, own, send))
 
 
-def expert_body(block, x_ref, gain_ref, gate_hbm, up_hbm, down_hbm, out_ref, gate_ref, up_ref, down_ref, sems):
-    pairs = ((gate_hbm, gate_ref), (up_hbm, up_ref), (down_hbm, down_ref))
-    copies = [pltpu.make_async_copy(source, target, sems.at[i]) for i, (source, target) in enumerate(pairs)]
-    for copy in copies:
-        copy.start()
+def expert_body(block, x_ref, gain_ref, gate_ref, up_ref, down_ref, out_ref):
     shares, rows, _ = x_ref.shape
     order = sorted(range(shares), key=lambda p: share_of(p, SIDE))
     for lo in range(0, rows, block):
         stream = jnp.concatenate([x_ref[p, lo : lo + block, :] for p in order], axis=1).astype(F32)
         scale = lax.rsqrt(jnp.mean(stream * stream, axis=-1, keepdims=True) + NORM_EPS)
         normed = (stream * scale * gain_ref[...]).astype(BF16)
-        if lo == 0:
-            copies[0].wait()
-            copies[1].wait()
         gate_act = dot(normed, gate_ref[0])
         up_act = dot(normed, up_ref[0])
         hidden = (gate_act * jax.nn.sigmoid(gate_act) * up_act).astype(BF16)
-        if lo == 0:
-            copies[2].wait()
         for p in range(shares):
             t = share_of(p, SIDE)
             out_ref[p, lo : lo + block, :] = dot(hidden, down_ref[0, :, t * LANES : (t + 1) * LANES]).astype(BF16)
@@ -270,13 +293,12 @@
     return pl.pallas_call(
         functools.partial(expert_body, block),
         out_shape=vmem_out(x.shape),
-        in_specs=[VMEM_SPEC] * 2 + [pl.BlockSpec(memory_space=pltpu.HBM)] * 3,
+        in_specs=[VMEM_SPEC] * 5,
         out_specs=VMEM_SPEC,
-        scratch_shapes=[pltpu.VMEM(a.shape, BF16) for a in (gate, up, down)] + [pltpu.SemaphoreType.DMA((3,))],
         cost_estimate=pl.CostEstimate(flops=6 * x.shape[1] * gate.shape[1] * gate.shape[2], bytes_accessed=2 * x.size * 2, transcendentals=0),
         compiler_params=small_kernel(24),
         name="expert",
-    )(*in_vmem(x, gain), *in_hbm(gate, up, down))
+    )(*in_vmem(x, gain, gate, up, down))
 
 
 def combine_body(rows_ref, take_ref, weights_ref, stream_ref, out_ref):
@@ -312,14 +334,14 @@
     down_weight,
 ):
     tokens = query_rows.shape[0]
-    local_heads = query_rows.shape[1] // HEAD_DIM
     tp_size = lax.axis_size(TP)
     experts = lax.axis_size("sp")
     tp_index = lax.axis_index(TP)
-    place = jnp.stack([lax.axis_index("sp"), tp_index * local_heads // REP]).astype(jnp.int32)
-    last = last_window(key_rows, value_rows)
+    place = lax.axis_index("sp").reshape(1).astype(jnp.int32)
+    last, kv, queries, out_share = loaded(query_rows, key_rows, value_rows, out_weight)
     before = lax.ppermute(last, "sp", [(i, i + 1) for i in range(experts - 1)])
-    partial = attention(place, sink_logits, query_rows, key_rows, value_rows, before, out_weight)
+    later = attention_later(sink_logits, queries, kv, out_share)
+    partial = attention_first(place, sink_logits, queries, kv, before, out_share, later)
     arrived = lax.all_to_all(partial, PLANE, split_axis=0, concat_axis=0, tiled=True)
     cap = 3 * tokens * routes.shape[1] // (2 * experts)
     send, take = slot_matrices(routes, experts, cap)
@@ -328,7 +350,8 @@
     rows = lax.all_to_all(rows.reshape(experts, cap, LANES), "sp", split_axis=0, concat_axis=0, tiled=True)
     slots = experts * cap
     gain = norm_gain.reshape(1, -1)
-    features = lax.all_to_all(copied(place, rows.reshape(slots, LANES), tp_size), PLANE, split_axis=0, concat_axis=0, tiled=True)
+    copies = copied(place, rows.reshape(slots, LANES), tp_size)
+    features = lax.all_to_all(copies, PLANE, split_axis=0, concat_axis=0, tiled=True)
     parts = expert(features, gain, gate_weight, up_weight, down_weight, 192)
     summed = total(lax.all_to_all(parts, PLANE, split_axis=0, concat_axis=0, tiled=True))
     returned = lax.all_to_all(summed.reshape(experts, cap, LANES), "sp", split_axis=0, concat_axis=0, tiled=True)

time: 185 us -> 183 us (0.989)
  blocking collectives: 110 us -> 107 us
    pallas_call x2 -> x3, Pallas kernels: 4.51 us -> 6.08 us  [the longest x1 2.44 us: attention_first(): pl.pallas_call(first_body, grid=(1,), out_shape=pltpu.HBM(partial.shape,...]
  transfers between devices with their start and end apart: 3 -> 3, of which waited for: 3 -> 2; matrix products, arithmetic and copies ran while one was open for 0% -> 0% of each run, Pallas kernels for 0% -> 2%
where the time goes in v5:
time: 183 us; the launch traced here: 182 us
  blocking collectives  107 us (58%)
  waiting for transfers between devices  35.3 us (19%)
  starting transfers between devices  26 us (14%)
  Pallas kernels  13.3 us (7%)
    all_to_all x1, blocking collectives, per_device(): lax.all_to_all(rows.reshape(experts, cap, LANES), 'sp', split_axis=0, con...  34.2 us
    all_to_all x1, blocking collectives, per_device(): lax.all_to_all(parts, PLANE, split_axis=0, concat_axis=0, tiled=True)  31.2 us
    all_to_all x1, blocking collectives, per_device(): lax.all_to_all(copies, PLANE, split_axis=0, concat_axis=0, tiled=True)  29.4 us
    all_to_all x1, waiting for transfers between devices, per_device(): lax.all_to_all(summed.reshape(experts, cap, LANES), 'sp', split_axis=0, c...  19.8 us
    all_to_all x1, waiting for transfers between devices, per_device(): lax.all_to_all(partial, PLANE, split_axis=0, concat_axis=0, tiled=True)  15.4 us
    all_to_all x1, starting transfers between devices, per_device(): lax.all_to_all(summed.reshape(experts, cap, LANES), 'sp', split_axis=0, c...  15.4 us
    all_to_all x1, blocking collectives, per_device(): return lax.all_to_all(out, TP, split_axis=0, concat_axis=1, tiled=True)  11.7 us
    all_to_all x1, starting transfers between devices, per_device(): lax.all_to_all(partial, PLANE, split_axis=0, concat_axis=0, tiled=True)  8.89 us
  transfers between devices with their start and end apart: 3, of which 2 were waited for; matrix products, arithmetic and copies ran while one was open for 0% of the time, Pallas kernels for 2%

profile of v5, /device:TPU:2, one launch (start us, length us, event | category | flops | bytes accessed | tf_op | source)
XLA Modules:
  0.0 182.2 jit_solution(5542891211965709552)
XLA Ops:
  0.0 0.0 copy-start
  0.0 1.3 load.1
  1.3 1.7 collective-permute-start
  3.1 2.3 %attention_later.1.partial_ref = bf16[16,256,128]{2,1,0:T(8,128)(2,1)} custom-call(f32[2]{0:T(128)} %sinks.3, bf16[256,128]{1,0:T(8,128)(2,1)S(1)} %get-tuple-element.13.q_ref, bf16[256,128]{1,0:T(8,128)(2,1)S(1)} %get-tuple-element.14.kv_ref, bf16[128,2048]{1,0:T(8,128)(2,1)S(1)} %get-tuple-element.16.w_ref), custom_call_target="tpu_custom_call" | custom-call | flops 1000000000 | bytes 1048576 | tf_op jit(solution)/shard_map/attention_later/pallas_call | solution.py:106
  5.4 0.0 collective-permute-done.before_ref
  5.4 2.4 %attention_first.1 = bf16[16,256,128]{2,1,0:T(8,128)(2,1)} custom-call(s32[1]{0:T(128)} %bitcast.place, f32[2]{0:T(128)} %sinks.3, bf16[256,128]{1,0:T(8,128)(2,1)S(1)} %get-tuple-element.13.q_ref, bf16[256,128]{1,0:T(8,128)(2,1)S(1)} %get-tuple-element.14.kv_ref, ...), custom_call_target="tpu_custom_call", output_to_operand_aliasing={{}: (6, {})} | custom-call | tf_op jit(solution)/shard_map/attention_first/pallas_call | solution.py:120
  7.8 8.9 %all-to-all-start = ((bf16[16,256,128]{2,1,0:T(8,128)(2,1)}), bf16[16,256,128]{2,1,0:T(8,128)(2,1)S(1)}, u32[]{:S(2)}, u32[]{:S(2)}) async-start(bf16[16,256,128]{2,1,0:T(8,128)(2,1)} %attention_first.1), calls=%async_computation | async-start | bytes 2097152 | tf_op jit(solution)/shard_map/all_to_all | solution.py:345
  16.7 0.0 copy-done.4
  16.7 0.1 copy.14.routes_ref
  16.9 0.8 slots.1
  17.7 0.0 copy-done
  17.7 15.4 %all-to-all-done.arrived_ref = bf16[16,256,128]{2,1,0:T(8,128)(2,1)S(1)} async-done(((bf16[16,256,128]{2,1,0:T(8,128)(2,1)}), bf16[16,256,128]{2,1,0:T(8,128)(2,1)S(1)}, u32[]{:S(2)}, u32[]{:S(2)}) %all-to-all-start) | async-done | bytes 1048608 | tf_op jit(solution)/shard_map/all_to_all | solution.py:345
  33.2 0.4 stream.1
  33.6 34.2 %all_to_all.44 = bf16[32,24,128]{2,1,0:T(8,128)(2,1)S(1)} all-to-all(bf16[32,24,128]{2,1,0:T(8,128)(2,1)S(1)} %bitcast.17), channel_id=1, replica_groups=mesh['sp'=32,'tp_0'=4,'tp_1'=4] {'sp'}, dimensions={0} | all-to-all | bytes 393216 | tf_op jit(solution)/shard_map/all_to_all | solution.py:350
  67.8 0.6 copies.1
  68.4 0.0 copy-start.1
  68.4 0.0 copy-start.2
  68.4 0.0 copy-start.3
  68.4 0.0 copy-start.5
  68.4 29.4 %all_to_all.45.x_ref = bf16[16,768,128]{2,1,0:T(8,128)(2,1)S(1)} all-to-all(bf16[16,768,128]{2,1,0:T(8,128)(2,1)S(1)} %copies.1), channel_id=1, replica_groups=mesh['sp'=32,'tp_0'=4,'tp_1'=4] {'tp_1','tp_0'}, dimensions={0} | all-to-all | bytes 6291456 | tf_op jit(solution)/shard_map/all_to_all | solution.py:354
  97.9 0.0 copy-done.1
  97.9 0.0 copy-done.3
  97.9 0.0 copy-done.5
  97.9 3.9 %expert.1 = bf16[16,768,128]{2,1,0:T(8,128)(2,1)S(1)} custom-call(bf16[16,768,128]{2,1,0:T(8,128)(2,1)S(1)} %all_to_all.45.x_ref, f32[1,2048]{1,0:T(1,128)S(1)} %bitcast.19, bf16[1,2048,256]{2,1,0:T(8,128)(2,1)S(1)} %copy-done.1, bf16[1,2048,256]{2,1,0:T(8,128)(2,1)S(1)} %copy-done.2, bf16[1,256,2048]{2,1,0:T(8,128)(2,1)S(1)} %copy-done.3), custom_call_target="tpu_custom_call" | custom-call | flops 2415919104 | bytes 6291456 | tf_op jit(solution)/shard_map/expert/pallas_call | solution.py:293
  101.8 31.2 %all_to_all.46.parts_ref = bf16[16,768,128]{2,1,0:T(8,128)(2,1)S(1)} all-to-all(bf16[16,768,128]{2,1,0:T(8,128)(2,1)S(1)} %expert.1), channel_id=1, replica_groups=mesh['sp'=32,'tp_0'=4,'tp_1'=4] {'tp_1','tp_0'}, dimensions={0} | all-to-all | bytes 6291456 | tf_op jit(solution)/shard_map/all_to_all | solution.py:356
  133.1 1.1 total.1
  134.2 15.4 %all-to-all-start.4 = ((bf16[32,24,128]{2,1,0:T(8,128)(2,1)}), bf16[32,24,128]{2,1,0:T(8,128)(2,1)S(1)}, u32[]{:S(2)}, u32[]{:S(2)}) async-start(bf16[32,24,128]{2,1,0:T(8,128)(2,1)} %bitcast.5), calls=%async_computation.4 | async-start | bytes 393216 | tf_op jit(solution)/shard_map/all_to_all | solution.py:357
  149.6 0.1 copy.15.weights_ref
  149.7 19.8 %all-to-all-done.4 = bf16[32,24,128]{2,1,0:T(8,128)(2,1)S(1)} async-done(((bf16[32,24,128]{2,1,0:T(8,128)(2,1)}), bf16[32,24,128]{2,1,0:T(8,128)(2,1)S(1)}, u32[]{:S(2)}, u32[]{:S(2)}) %all-to-all-start.4) | async-done | bytes 196640 | tf_op jit(solution)/shard_map/all_to_all | solution.py:357
  169.5 0.4 combine.1
  169.9 11.7 %all_to_all.47 = bf16[16,16,128]{2,1,0:T(8,128)(2,1)S(1)} all-to-all(bf16[16,16,128]{2,1,0:T(8,128)(2,1)S(1)} %bitcast.16), channel_id=1, replica_groups=mesh['sp'=32,'tp_0'=4,'tp_1'=4] {'tp_0','tp_1'}, dimensions={0} | all-to-all | bytes 131072 | tf_op jit(solution)/shard_map/all_to_all | solution.py:359
  181.6 0.6 copy_bitcast_fusion
  (5 shorter events, 0.0 us)
Async XLA Ops:
  0.0 17.7 %copy-start = (bf16[256,2048]{1,0:T(8,128)(2,1)S(1)}, bf16[256,2048]{1,0:T(8,128)(2,1)}, u32[]{:S(2)}) copy-start(bf16[256,2048]{1,0:T(8,128)(2,1)} %param.17) | copy-start | bytes 3145732
  1.3 4.1 %collective-permute-start = (bf16[128,128]{1,0:T(8,128)(2,1)S(1)}, bf16[128,128]{1,0:T(8,128)(2,1)S(1)}, u32[]{:S(2)}, u32[]{:S(2)}) collective-permute-start(bf16[128,128]{1,0:T(8,128)(2,1)S(1)} %get-tuple-element.15), channel_id=1, source_target_pairs={{0,16},{16,32},{32,48},{48,64},{64,80},{80,96},{96,112},{112,128},... | collective-permute-start | bytes 98312 | tf_op jit(solution)/shard_map/ppermute | solution.py:342
  5.4 11.3 %copy-start.4 = (s32[256,2]{0,1:T(2,128)S(1)}, s32[256,2]{0,1:T(2,128)}, u32[]{:S(2)}) copy-start(s32[256,2]{0,1:T(2,128)} %param.19) | copy-start | bytes 6148
  7.8 25.3 %all-to-all-start = ((bf16[16,256,128]{2,1,0:T(8,128)(2,1)}), bf16[16,256,128]{2,1,0:T(8,128)(2,1)S(1)}, u32[]{:S(2)}, u32[]{:S(2)}) async-start(bf16[16,256,128]{2,1,0:T(8,128)(2,1)} %attention_first.1), calls=%async_computation | async-start | bytes 2097152 | tf_op jit(solution)/shard_map/all_to_all | solution.py:345
  68.4 29.5 %copy-start.1 = (bf16[1,2048,256]{2,1,0:T(8,128)(2,1)S(1)}, bf16[1,2048,256]{2,1,0:T(8,128)(2,1)}, u32[]{:S(2)}) copy-start(bf16[1,2048,256]{2,1,0:T(8,128)(2,1)} %gate_ref.1) | copy-start | bytes 3145732
  68.4 29.5 %copy-start.2 = (bf16[1,2048,256]{2,1,0:T(8,128)(2,1)S(1)}, bf16[1,2048,256]{2,1,0:T(8,128)(2,1)}, u32[]{:S(2)}) copy-start(bf16[1,2048,256]{2,1,0:T(8,128)(2,1)} %up_ref.1) | copy-start | bytes 3145732
  68.4 29.5 %copy-start.3 = (bf16[1,256,2048]{2,1,0:T(8,128)(2,1)S(1)}, bf16[1,256,2048]{2,1,0:T(8,128)(2,1)}, u32[]{:S(2)}) copy-start(bf16[1,256,2048]{2,1,0:T(8,128)(2,1)} %down_ref.1) | copy-start | bytes 3145732
  68.4 29.5 %copy-start.5 = (f32[2048]{0:T(1024)S(1)}, f32[2048]{0:T(1024)}, u32[]{:S(2)}) copy-start(f32[2048]{0:T(1024)} %param.18) | copy-start | bytes 24580
  133.1 16.5 %copy-start.6 = (f32[256,2]{0,1:T(2,128)S(1)}, f32[256,2]{0,1:T(2,128)}, u32[]{:S(2)}) copy-start(f32[256,2]{0,1:T(2,128)} %param.20) | copy-start | bytes 6148
  134.2 35.4 %all-to-all-start.4 = ((bf16[32,24,128]{2,1,0:T(8,128)(2,1)}), bf16[32,24,128]{2,1,0:T(8,128)(2,1)S(1)}, u32[]{:S(2)}, u32[]{:S(2)}) async-start(bf16[32,24,128]{2,1,0:T(8,128)(2,1)} %bitcast.5), calls=%async_computation.4 | async-start | bytes 393216 | tf_op jit(solution)/shard_map/all_to_all | solution.py:357

commit v6 on v5

--- a/solution.py
+++ b/solution.py
@@ -18,9 +18,6 @@
 BF16 = jnp.bfloat16
 F32 = jnp.float32
 VMEM_SPEC = pl.BlockSpec(memory_space=pltpu.VMEM)
-SMEM_SPEC = pl.BlockSpec(memory_space=pltpu.SMEM)
-PLANE = ("tp_1", "tp_0")
-SIDE = 4
 LAG_NS = 17000
 
 
@@ -38,10 +35,6 @@
 
 def vmem_out(shape):
     return pltpu.VMEM(shape, BF16)
-
-
-def share_of(member, side):
-    return member % side * side + member // side
 
 
 def dot(a, b, contract=(1, 0)):
@@ -62,7 +55,7 @@
     for h in range(2):
         scores = dot(q, keys[h], (1, 1)) * HEAD_DIM**-0.5
         scores = jnp.where(allowed, scores, -1e30)
-        sink = sinks[h]
+        sink = sinks[h : h + 1, :1]
         peak = jnp.maximum(jnp.max(scores, axis=-1, keepdims=True), sink)
         terms = jnp.exp(scores - peak)
         total_terms = jnp.sum(terms, axis=-1, keepdims=True) + jnp.exp(sink - peak)
@@ -72,10 +65,18 @@
     return total.astype(BF16)
 
 
-def project(attended, w_ref, out_ref):
-    for p in range(out_ref.shape[0]):
-        t = share_of(p, SIDE)
-        out_ref[p] = dot(attended, w_ref[:, t * LANES : (t + 1) * LANES]).astype(BF16)
+def project(attended, w_ref, stage_ref, out_hbm, sems, row0):
+    copies = []
+    for j in range(stage_ref.shape[0] // 2):
+        both = dot(attended, w_ref[:, 2 * j * LANES : 2 * (j + 1) * LANES]).astype(BF16)
+        stage_ref[2 * j] = both[:, :LANES]
+        stage_ref[2 * j + 1] = both[:, LANES:]
+        pair = pl.ds(2 * j, 2)
+        copy = pltpu.make_async_copy(stage_ref.at[pair], out_hbm.at[pair, pl.ds(row0, WINDOW), :], sems.at[j])
+        copy.start()
+        copies.append(copy)
+    for copy in copies:
+        copy.wait()
 
 
 def window_mask():
@@ -84,53 +85,53 @@
     return (col > row) & (col <= row + WINDOW), col
 
 
-def later_body(sinks, q_ref, kv_ref, w_ref, out_ref):
+def later_body(sinks_ref, q_ref, kv_ref, w_ref, out_hbm, stage_ref, sems):
     keys, values = both_places(kv_ref[...].astype(F32))
     inside, _ = window_mask()
-    project(attend(q_ref[WINDOW:, :], keys, values, inside, sinks), w_ref, out_ref)
-
-
-def first_body(place, sinks, q_ref, kv_ref, before_ref, w_ref, partial_ref, out_ref):
+    project(attend(q_ref[WINDOW:, :], keys, values, inside, sinks_ref[...]), w_ref, stage_ref, out_hbm, sems, WINDOW)
+
+
+def first_body(sinks_ref, q_ref, kv_ref, before_ref, w_ref, partial_ref, out_hbm, stage_ref, sems):
     keys, values = both_places(jnp.concatenate([before_ref[...], kv_ref[:WINDOW, :]], axis=0).astype(F32))
     inside, col = window_mask()
-    allowed = inside & ((col >= WINDOW) | (place[0] > 0))
-    project(attend(q_ref[:WINDOW, :], keys, values, allowed, sinks), w_ref, out_ref)
-
-
-def half_out(shares, at):
-    return pl.BlockSpec((shares, WINDOW, LANES), lambda i: (0, at, 0))
+    allowed = inside & ((col >= WINDOW) | (lax.axis_index("sp") > 0))
+    project(attend(q_ref[:WINDOW, :], keys, values, allowed, sinks_ref[...]), w_ref, stage_ref, out_hbm, sems, 0)
+
+
+def stages(shares):
+    return [pltpu.VMEM((shares, WINDOW, LANES), BF16), pltpu.SemaphoreType.DMA((shares // 2,))]
 
 
 def attention_later(sinks, q, kv, w):
     shares = w.shape[1] // LANES
     return pl.pallas_call(
         later_body,
-        grid=(1,),
         out_shape=pltpu.HBM((shares, q.shape[0], LANES), BF16),
-        in_specs=[SMEM_SPEC] + [VMEM_SPEC] * 3,
-        out_specs=half_out(shares, 1),
+        in_specs=[VMEM_SPEC] * 4,
+        out_specs=pl.BlockSpec(memory_space=pltpu.HBM),
+        scratch_shapes=stages(shares),
         compiler_params=small_kernel(16),
         cost_estimate=pl.CostEstimate(flops=10**9, bytes_accessed=2**20, transcendentals=2**16),
         name="attention_later",
-    )(*in_hbm(sinks), *in_vmem(q, kv, w))
-
-
-def attention_first(place, sinks, q, kv, before, w, partial):
+    )(*in_vmem(sinks, q, kv, w))
+
+
+def attention_first(sinks, q, kv, before, w, partial):
     shares = w.shape[1] // LANES
     return pl.pallas_call(
         first_body,
-        grid=(1,),
         out_shape=pltpu.HBM(partial.shape, BF16),
-        in_specs=[SMEM_SPEC, SMEM_SPEC] + [VMEM_SPEC] * 4 + [pl.BlockSpec(memory_space=pltpu.HBM)],
-        out_specs=half_out(shares, 0),
-        input_output_aliases={6: 0},
+        in_specs=[VMEM_SPEC] * 5 + [pl.BlockSpec(memory_space=pltpu.HBM)],
+        out_specs=pl.BlockSpec(memory_space=pltpu.HBM),
+        scratch_shapes=stages(shares),
+        input_output_aliases={5: 0},
         compiler_params=small_kernel(16),
         name="attention_first",
-    )(place, *in_hbm(sinks), *in_vmem(q, kv, before, w), *in_hbm(partial))
-
-
-def load_body(q_hbm, k_hbm, v_hbm, w_hbm, last_ref, kv_ref, q_ref, w_ref, k_ref, v_ref, sems):
-    pairs = ((k_hbm, k_ref), (v_hbm, v_ref), (q_hbm, q_ref), (w_hbm, w_ref))
+    )(*in_vmem(sinks, q, kv, before, w), *in_hbm(partial))
+
+
+def load_body(sinks_hbm, q_hbm, k_hbm, v_hbm, w_hbm, last_ref, kv_ref, sinks_ref, q_ref, w_ref, k_ref, v_ref, sinks_smem, sems):
+    pairs = ((k_hbm, k_ref), (v_hbm, v_ref), (q_hbm, q_ref), (w_hbm, w_ref), (sinks_hbm, sinks_smem))
     copies = [pltpu.make_async_copy(source, target, sems.at[i]) for i, (source, target) in enumerate(pairs)]
     for copy in copies:
         copy.start()
@@ -151,25 +152,28 @@
     kv = jnp.where(low, jnp.where(odd, key_swapped, key), jnp.where(odd, value, value_swapped)).astype(BF16)
     kv_ref[...] = kv
     last_ref[...] = kv[kv.shape[0] - WINDOW :]
+    copies[4].wait()
+    row = lax.broadcasted_iota(jnp.int32, sinks_ref.shape, 0)
+    sinks_ref[...] = jnp.where(row == 0, sinks_smem[0], sinks_smem[1])
     copies[2].wait()
     copies[3].wait()
 
 
-def loaded(q, k, v, w):
+def loaded(sinks, q, k, v, w):
     rows = q.shape[0]
     return pl.pallas_call(
         load_body,
-        out_shape=(vmem_out((WINDOW, LANES)), vmem_out((rows, LANES)), vmem_out(q.shape), vmem_out(w.shape)),
-        in_specs=[pl.BlockSpec(memory_space=pltpu.HBM)] * 4,
-        out_specs=(VMEM_SPEC,) * 4,
-        scratch_shapes=[pltpu.VMEM(k.shape, BF16), pltpu.VMEM(v.shape, BF16), pltpu.SemaphoreType.DMA((4,))],
+        out_shape=(vmem_out((WINDOW, LANES)), vmem_out((rows, LANES)), pltpu.VMEM((8, LANES), F32), vmem_out(q.shape), vmem_out(w.shape)),
+        in_specs=[pl.BlockSpec(memory_space=pltpu.HBM)] * 5,
+        out_specs=(VMEM_SPEC,) * 5,
+        scratch_shapes=[pltpu.VMEM(k.shape, BF16), pltpu.VMEM(v.shape, BF16), pltpu.SMEM(sinks.shape, F32), pltpu.SemaphoreType.DMA((5,))],
         compiler_params=small_kernel(16),
         name="load",
-    )(*in_hbm(q, k, v, w))
-
-
-def copies_body(place, rows_ref, out_ref):
-    @pl.when(place[0] % 2 == 1)
+    )(*in_hbm(sinks, q, k, v, w))
+
+
+def copies_body(rows_ref, out_ref):
+    @pl.when(lax.axis_index("sp") % 2 == 1)
     def _():
         pl.delay(LAG_NS)
 
@@ -178,20 +182,20 @@
         out_ref[t] = rows
 
 
-def copied(place, rows, count):
+def copied(rows, count):
     return pl.pallas_call(
         copies_body,
         out_shape=vmem_out((count, *rows.shape)),
-        in_specs=[SMEM_SPEC, VMEM_SPEC],
+        in_specs=[VMEM_SPEC],
         out_specs=VMEM_SPEC,
         compiler_params=small_kernel(16),
         name="copies",
-    )(place, *in_vmem(rows))
+    )(*in_vmem(rows))
 
 
 def total_body(parts_ref, out_ref):
     rows = parts_ref.shape[1]
-    block = 128
+    block = 64
     for lo in range(0, rows, block):
         summed = parts_ref[0, lo : lo + block, :].astype(F32)
         for t in range(1, parts_ref.shape[0]):
@@ -276,17 +280,17 @@
 
 def expert_body(block, x_ref, gain_ref, gate_ref, up_ref, down_ref, out_ref):
     shares, rows, _ = x_ref.shape
-    order = sorted(range(shares), key=lambda p: share_of(p, SIDE))
     for lo in range(0, rows, block):
-        stream = jnp.concatenate([x_ref[p, lo : lo + block, :] for p in order], axis=1).astype(F32)
+        stream = jnp.concatenate([x_ref[t, lo : lo + block, :] for t in range(shares)], axis=1).astype(F32)
         scale = lax.rsqrt(jnp.mean(stream * stream, axis=-1, keepdims=True) + NORM_EPS)
         normed = (stream * scale * gain_ref[...]).astype(BF16)
         gate_act = dot(normed, gate_ref[0])
         up_act = dot(normed, up_ref[0])
         hidden = (gate_act * jax.nn.sigmoid(gate_act) * up_act).astype(BF16)
-        for p in range(shares):
-            t = share_of(p, SIDE)
-            out_ref[p, lo : lo + block, :] = dot(hidden, down_ref[0, :, t * LANES : (t + 1) * LANES]).astype(BF16)
+        for t in range(0, shares, 2):
+            both = dot(hidden, down_ref[0, :, t * LANES : (t + 2) * LANES]).astype(BF16)
+            out_ref[t, lo : lo + block, :] = both[:, :LANES]
+            out_ref[t + 1, lo : lo + block, :] = both[:, LANES:]
 
 
 def expert(x, gain, gate, up, down, block):
@@ -337,12 +341,11 @@
     tp_size = lax.axis_size(TP)
     experts = lax.axis_size("sp")
     tp_index = lax.axis_index(TP)
-    place = lax.axis_index("sp").reshape(1).astype(jnp.int32)
-    last, kv, queries, out_share = loaded(query_rows, key_rows, value_rows, out_weight)
+    last, kv, sinks, queries, out_share = loaded(sink_logits, query_rows, key_rows, value_rows, out_weight)
     before = lax.ppermute(last, "sp", [(i, i + 1) for i in range(experts - 1)])
-    later = attention_later(sink_logits, queries, kv, out_share)
-    partial = attention_first(place, sink_logits, queries, kv, before, out_share, later)
-    arrived = lax.all_to_all(partial, PLANE, split_axis=0, concat_axis=0, tiled=True)
+    later = attention_later(sinks, queries, kv, out_share)
+    partial = attention_first(sinks, queries, kv, before, out_share, later)
+    arrived = lax.all_to_all(partial, TP, split_axis=0, concat_axis=0, tiled=True)
     cap = 3 * tokens * routes.shape[1] // (2 * experts)
     send, take = slot_matrices(routes, experts, cap)
     own = lax.dynamic_slice_in_dim(stream_in, tp_index * LANES, LANES, 1)
@@ -350,10 +353,10 @@
     rows = lax.all_to_all(rows.reshape(experts, cap, LANES), "sp", split_axis=0, concat_axis=0, tiled=True)
     slots = experts * cap
     gain = norm_gain.reshape(1, -1)
-    copies = copied(place, rows.reshape(slots, LANES), tp_size)
-    features = lax.all_to_all(copies, PLANE, split_axis=0, concat_axis=0, tiled=True)
-    parts = expert(features, gain, gate_weight, up_weight, down_weight, 192)
-    summed = total(lax.all_to_all(parts, PLANE, split_axis=0, concat_axis=0, tiled=True))
+    copies = copied(rows.reshape(slots, LANES), tp_size)
+    features = lax.all_to_all(copies, TP, split_axis=0, concat_axis=0, tiled=True)
+    parts = expert(features, gain, gate_weight, up_weight, down_weight, 384)
+    summed = total(lax.all_to_all(parts, TP, split_axis=0, concat_axis=0, tiled=True))
     returned = lax.all_to_all(summed.reshape(experts, cap, LANES), "sp", split_axis=0, concat_axis=0, tiled=True)
     out = combine(returned.reshape(slots, LANES), take, route_weights, stream)
     return lax.all_to_all(out, TP, split_axis=0, concat_axis=1, tiled=True)

time: 183 us -> 182 us (level)
    all_to_all x2, blocking collectives: 60.7 us -> 62.6 us  [the longest x1 32.6 us: per_device(): lax.all_to_all(parts, TP, split_axis=0, concat_axis=0, tiled=True)]
where the time goes in v6:
time: 182 us
  blocking collectives  108 us (59%)
  waiting for transfers between devices  35.6 us (20%)
  starting transfers between devices  25.7 us (14%)
  Pallas kernels  11.5 us (6%)
    all_to_all x1, blocking collectives, per_device(): lax.all_to_all(rows.reshape(experts, cap, LANES), 'sp', split_axis=0, con...  34.7 us
    all_to_all x1, blocking collectives, per_device(): lax.all_to_all(parts, TP, split_axis=0, concat_axis=0, tiled=True)  32.6 us
    all_to_all x1, blocking collectives, per_device(): lax.all_to_all(copies, TP, split_axis=0, concat_axis=0, tiled=True)  30 us
    all_to_all x1, waiting for transfers between devices, per_device(): lax.all_to_all(summed.reshape(experts, cap, LANES), 'sp', split_axis=0, c...  19.8 us
    all_to_all x1, waiting for transfers between devices, per_device(): lax.all_to_all(partial, TP, split_axis=0, concat_axis=0, tiled=True)  15.8 us
    all_to_all x1, starting transfers between devices, per_device(): lax.all_to_all(summed.reshape(experts, cap, LANES), 'sp', split_axis=0, c...  15.1 us
    all_to_all x1, blocking collectives, per_device(): return lax.all_to_all(out, TP, split_axis=0, concat_axis=1, tiled=True)  10.2 us
    all_to_all x1, starting transfers between devices, per_device(): lax.all_to_all(partial, TP, split_axis=0, concat_axis=0, tiled=True)  8.88 us
  transfers between devices with their start and end apart: 3, of which 2 were waited for; matrix products, arithmetic and copies ran while one was open for 0% of the time, Pallas kernels for 2%

profile of v6, /device:TPU:2, one launch (start us, length us, event | category | flops | bytes accessed | tf_op | source)
XLA Modules:
  0.0 181.5 jit_solution(7172827149598961003)
XLA Ops:
  0.0 0.0 copy-start
  0.0 1.3 load.1
  1.3 1.7 collective-permute-start
  3.1 1.9 %attention_later.1.partial_ref = bf16[16,256,128]{2,1,0:T(8,128)(2,1)} custom-call(f32[8,128]{1,0:T(8,128)S(1)} %get-tuple-element.14.sinks_ref, bf16[256,128]{1,0:T(8,128)(2,1)S(1)} %get-tuple-element.15.q_ref, bf16[256,128]{1,0:T(8,128)(2,1)S(1)} %get-tuple-element.16.kv_ref, bf16[128,2048]{1,0:T(8,128)(2,1)S(1)} %get-tuple-element.18.w_ref), custom_call_target="tpu_custom_call" | custom-call | flops 1000000000 | bytes 1048576 | tf_op jit(solution)/shard_map/attention_later/pallas_call | solution.py:107
  5.0 0.0 copy-start.4
  5.0 0.0 collective-permute-done.before_ref
  5.1 2.0 %attention_first.1 = bf16[16,256,128]{2,1,0:T(8,128)(2,1)} custom-call(f32[8,128]{1,0:T(8,128)S(1)} %get-tuple-element.14.sinks_ref, bf16[256,128]{1,0:T(8,128)(2,1)S(1)} %get-tuple-element.15.q_ref, bf16[256,128]{1,0:T(8,128)(2,1)S(1)} %get-tuple-element.16.kv_ref, ...), custom_call_target="tpu_custom_call", output_to_operand_aliasing={{}: (5, {})} | custom-call | tf_op jit(solution)/shard_map/attention_first/pallas_call | solution.py:121
  7.1 8.9 %all-to-all-start = ((bf16[16,256,128]{2,1,0:T(8,128)(2,1)}), bf16[16,256,128]{2,1,0:T(8,128)(2,1)S(1)}, u32[]{:S(2)}, u32[]{:S(2)}) async-start(bf16[16,256,128]{2,1,0:T(8,128)(2,1)} %attention_first.1), calls=%async_computation | async-start | bytes 2097152 | tf_op jit(solution)/shard_map/all_to_all | solution.py:348
  15.9 0.0 copy-done.4
  15.9 0.1 copy.14.routes_ref
  16.1 0.8 slots.1
  16.9 0.0 copy-done
  16.9 15.8 %all-to-all-done.arrived_ref = bf16[16,256,128]{2,1,0:T(8,128)(2,1)S(1)} async-done(((bf16[16,256,128]{2,1,0:T(8,128)(2,1)}), bf16[16,256,128]{2,1,0:T(8,128)(2,1)S(1)}, u32[]{:S(2)}, u32[]{:S(2)}) %all-to-all-start) | async-done | bytes 1048608 | tf_op jit(solution)/shard_map/all_to_all | solution.py:348
  32.7 0.4 stream.1
  33.1 34.7 %all_to_all.44 = bf16[32,24,128]{2,1,0:T(8,128)(2,1)S(1)} all-to-all(bf16[32,24,128]{2,1,0:T(8,128)(2,1)S(1)} %bitcast.16), channel_id=1, replica_groups=mesh['sp'=32,'tp_0'=4,'tp_1'=4] {'sp'}, dimensions={0} | all-to-all | bytes 393216 | tf_op jit(solution)/shard_map/all_to_all | solution.py:353
  67.8 0.6 copies.1
  68.4 0.0 copy-start.1
  68.5 0.0 copy-start.2
  68.5 0.0 copy-start.3
  68.5 0.0 copy-start.5
  68.5 30.0 %all_to_all.45.x_ref = bf16[16,768,128]{2,1,0:T(8,128)(2,1)S(1)} all-to-all(bf16[16,768,128]{2,1,0:T(8,128)(2,1)S(1)} %copies.1), channel_id=1, replica_groups=mesh['sp'=32,'tp_0'=4,'tp_1'=4] {'tp_0','tp_1'}, dimensions={0} | all-to-all | bytes 6291456 | tf_op jit(solution)/shard_map/all_to_all | solution.py:357
  98.4 0.0 copy-done.1
  98.5 0.0 copy-done.5
  98.5 3.0 %expert.1 = bf16[16,768,128]{2,1,0:T(8,128)(2,1)S(1)} custom-call(bf16[16,768,128]{2,1,0:T(8,128)(2,1)S(1)} %all_to_all.45.x_ref, f32[1,2048]{1,0:T(1,128)S(1)} %bitcast.18, bf16[1,2048,256]{2,1,0:T(8,128)(2,1)S(1)} %copy-done.1, bf16[1,2048,256]{2,1,0:T(8,128)(2,1)S(1)} %copy-done.2, bf16[1,256,2048]{2,1,0:T(8,128)(2,1)S(1)} %copy-done.3), custom_call_target="tpu_custom_call" | custom-call | flops 2415919104 | bytes 6291456 | tf_op jit(solution)/shard_map/expert/pallas_call | solution.py:297
  101.4 32.6 %all_to_all.46.parts_ref = bf16[16,768,128]{2,1,0:T(8,128)(2,1)S(1)} all-to-all(bf16[16,768,128]{2,1,0:T(8,128)(2,1)S(1)} %expert.1), channel_id=1, replica_groups=mesh['sp'=32,'tp_0'=4,'tp_1'=4] {'tp_0','tp_1'}, dimensions={0} | all-to-all | bytes 6291456 | tf_op jit(solution)/shard_map/all_to_all | solution.py:359
  134.1 1.1 total.1
  135.2 15.1 %all-to-all-start.4 = ((bf16[32,24,128]{2,1,0:T(8,128)(2,1)}), bf16[32,24,128]{2,1,0:T(8,128)(2,1)S(1)}, u32[]{:S(2)}, u32[]{:S(2)}) async-start(bf16[32,24,128]{2,1,0:T(8,128)(2,1)} %bitcast.4), calls=%async_computation.4 | async-start | bytes 393216 | tf_op jit(solution)/shard_map/all_to_all | solution.py:360
  150.3 0.1 copy.15.weights_ref
  150.4 19.8 %all-to-all-done.4 = bf16[32,24,128]{2,1,0:T(8,128)(2,1)S(1)} async-done(((bf16[32,24,128]{2,1,0:T(8,128)(2,1)}), bf16[32,24,128]{2,1,0:T(8,128)(2,1)S(1)}, u32[]{:S(2)}, u32[]{:S(2)}) %all-to-all-start.4) | async-done | bytes 196640 | tf_op jit(solution)/shard_map/all_to_all | solution.py:360
  170.3 0.4 combine.1
  170.7 10.2 %all_to_all.47 = bf16[16,16,128]{2,1,0:T(8,128)(2,1)S(1)} all-to-all(bf16[16,16,128]{2,1,0:T(8,128)(2,1)S(1)} %bitcast.15), channel_id=1, replica_groups=mesh['sp'=32,'tp_0'=4,'tp_1'=4] {'tp_0','tp_1'}, dimensions={0} | all-to-all | bytes 131072 | tf_op jit(solution)/shard_map/all_to_all | solution.py:362
  180.9 0.6 copy_bitcast_fusion
  (5 shorter events, 0.0 us)
Async XLA Ops:
  0.0 16.9 %copy-start = (bf16[256,2048]{1,0:T(8,128)(2,1)S(1)}, bf16[256,2048]{1,0:T(8,128)(2,1)}, u32[]{:S(2)}) copy-start(bf16[256,2048]{1,0:T(8,128)(2,1)} %param.17) | copy-start | bytes 3145732
  1.3 3.7 %collective-permute-start = (bf16[128,128]{1,0:T(8,128)(2,1)S(1)}, bf16[128,128]{1,0:T(8,128)(2,1)S(1)}, u32[]{:S(2)}, u32[]{:S(2)}) collective-permute-start(bf16[128,128]{1,0:T(8,128)(2,1)S(1)} %get-tuple-element.17), channel_id=1, source_target_pairs={{0,16},{16,32},{32,48},{48,64},{64,80},{80,96},{96,112},{112,128},... | collective-permute-start | bytes 98312 | tf_op jit(solution)/shard_map/ppermute | solution.py:345
  5.0 10.9 %copy-start.4 = (s32[256,2]{0,1:T(2,128)S(1)}, s32[256,2]{0,1:T(2,128)}, u32[]{:S(2)}) copy-start(s32[256,2]{0,1:T(2,128)} %param.19) | copy-start | bytes 6148
  7.1 25.7 %all-to-all-start = ((bf16[16,256,128]{2,1,0:T(8,128)(2,1)}), bf16[16,256,128]{2,1,0:T(8,128)(2,1)S(1)}, u32[]{:S(2)}, u32[]{:S(2)}) async-start(bf16[16,256,128]{2,1,0:T(8,128)(2,1)} %attention_first.1), calls=%async_computation | async-start | bytes 2097152 | tf_op jit(solution)/shard_map/all_to_all | solution.py:348
  68.4 30.0 %copy-start.1 = (bf16[1,2048,256]{2,1,0:T(8,128)(2,1)S(1)}, bf16[1,2048,256]{2,1,0:T(8,128)(2,1)}, u32[]{:S(2)}) copy-start(bf16[1,2048,256]{2,1,0:T(8,128)(2,1)} %gate_ref.1) | copy-start | bytes 3145732
  68.5 30.0 %copy-start.2 = (bf16[1,2048,256]{2,1,0:T(8,128)(2,1)S(1)}, bf16[1,2048,256]{2,1,0:T(8,128)(2,1)}, u32[]{:S(2)}) copy-start(bf16[1,2048,256]{2,1,0:T(8,128)(2,1)} %up_ref.1) | copy-start | bytes 3145732
  68.5 30.0 %copy-start.3 = (bf16[1,256,2048]{2,1,0:T(8,128)(2,1)S(1)}, bf16[1,256,2048]{2,1,0:T(8,128)(2,1)}, u32[]{:S(2)}) copy-start(bf16[1,256,2048]{2,1,0:T(8,128)(2,1)} %down_ref.1) | copy-start | bytes 3145732
  68.5 30.0 %copy-start.5 = (f32[2048]{0:T(1024)S(1)}, f32[2048]{0:T(1024)}, u32[]{:S(2)}) copy-start(f32[2048]{0:T(1024)} %param.18) | copy-start | bytes 24580
  134.1 16.2 %copy-start.6 = (f32[256,2]{0,1:T(2,128)S(1)}, f32[256,2]{0,1:T(2,128)}, u32[]{:S(2)}) copy-start(f32[256,2]{0,1:T(2,128)} %param.20) | copy-start | bytes 6148
  135.2 35.1 %all-to-all-start.4 = ((bf16[32,24,128]{2,1,0:T(8,128)(2,1)}), bf16[32,24,128]{2,1,0:T(8,128)(2,1)S(1)}, u32[]{:S(2)}, u32[]{:S(2)}) async-start(bf16[32,24,128]{2,1,0:T(8,128)(2,1)} %bitcast.4), calls=%async_computation.4 | async-start | bytes 393216 | tf_op jit(solution)/shard_map/all_to_all | solution.py:360

commit v7 on v6

--- a/solution.py
+++ b/solution.py
@@ -18,7 +18,7 @@
 BF16 = jnp.bfloat16
 F32 = jnp.float32
 VMEM_SPEC = pl.BlockSpec(memory_space=pltpu.VMEM)
-LAG_NS = 17000
+LAG_NS = 16500
 
 
 def in_vmem(*arrays):
@@ -65,18 +65,11 @@
     return total.astype(BF16)
 
 
-def project(attended, w_ref, stage_ref, out_hbm, sems, row0):
-    copies = []
-    for j in range(stage_ref.shape[0] // 2):
-        both = dot(attended, w_ref[:, 2 * j * LANES : 2 * (j + 1) * LANES]).astype(BF16)
-        stage_ref[2 * j] = both[:, :LANES]
-        stage_ref[2 * j + 1] = both[:, LANES:]
-        pair = pl.ds(2 * j, 2)
-        copy = pltpu.make_async_copy(stage_ref.at[pair], out_hbm.at[pair, pl.ds(row0, WINDOW), :], sems.at[j])
-        copy.start()
-        copies.append(copy)
-    for copy in copies:
-        copy.wait()
+def project(attended, w_ref, out_ref, row0):
+    for t in range(0, out_ref.shape[0], 2):
+        both = dot(attended, w_ref[:, t * LANES : (t + 2) * LANES]).astype(BF16)
+        out_ref[t, row0 : row0 + WINDOW, :] = both[:, :LANES]
+        out_ref[t + 1, row0 : row0 + WINDOW, :] = both[:, LANES:]
 
 
 def window_mask():
@@ -85,53 +78,93 @@
     return (col > row) & (col <= row + WINDOW), col
 
 
-def later_body(sinks_ref, q_ref, kv_ref, w_ref, out_hbm, stage_ref, sems):
+def fill_slots(cap, experts, routes_ref, weights_ref, send_ref, take_ref, cols_ref):
+    tokens = routes_ref.shape[1]
+    slots = send_ref.shape[0]
+    expert_row = lax.broadcasted_iota(jnp.int32, (experts, tokens), 0)
+    picks = [routes_ref[k : k + 1, :] for k in range(2)]
+    hot = [(pick == expert_row).astype(F32) for pick in picks]
+    r = lax.broadcasted_iota(jnp.int32, (tokens, tokens), 0)
+    c = lax.broadcasted_iota(jnp.int32, (tokens, tokens), 1)
+    ahead = dot((hot[0] + hot[1]).astype(BF16), (r < c).astype(BF16))
+    targets = [picks[k].astype(F32) * cap + jnp.sum(ahead * hot[k], axis=0, keepdims=True) for k in range(2)]
+    slot_row = lax.broadcasted_iota(jnp.int32, (slots, tokens), 0)
+    here = [slot_row == target.astype(jnp.int32) for target in targets]
+    send_ref[...] = (here[0] | here[1]).astype(F32).astype(BF16)
+    row = lax.broadcasted_iota(jnp.int32, (8, tokens), 0)
+    rows = [*targets, weights_ref[0:1, :], weights_ref[1:2, :]]
+    table = jnp.zeros((8, tokens), F32)
+    for i, values in enumerate(rows):
+        table = jnp.where(row == i, values, table)
+    cols = jnp.transpose(table)
+    cols_ref[...] = cols
+    slot_lane = lax.broadcasted_iota(jnp.int32, (tokens, slots), 1)
+    for k in range(2):
+        target = cols[:, k : k + 1].astype(jnp.int32)
+        take_ref[k * tokens : (k + 1) * tokens, :] = (slot_lane == target).astype(F32).astype(BF16)
+
+
+def later_body(cap, experts, sinks_ref, q_ref, kv_ref, w_ref, routes_ref, weights_ref, out_ref, send_ref, take_ref, cols_ref):
     keys, values = both_places(kv_ref[...].astype(F32))
     inside, _ = window_mask()
-    project(attend(q_ref[WINDOW:, :], keys, values, inside, sinks_ref[...]), w_ref, stage_ref, out_hbm, sems, WINDOW)
-
-
-def first_body(sinks_ref, q_ref, kv_ref, before_ref, w_ref, partial_ref, out_hbm, stage_ref, sems):
+    project(attend(q_ref[WINDOW:, :], keys, values, inside, sinks_ref[...]), w_ref, out_ref, WINDOW)
+    fill_slots(cap, experts, routes_ref, weights_ref, send_ref, take_ref, cols_ref)
+
+
+def first_body(sinks_ref, q_ref, kv_ref, before_ref, w_ref, partial_ref, out_ref):
     keys, values = both_places(jnp.concatenate([before_ref[...], kv_ref[:WINDOW, :]], axis=0).astype(F32))
     inside, col = window_mask()
     allowed = inside & ((col >= WINDOW) | (lax.axis_index("sp") > 0))
-    project(attend(q_ref[:WINDOW, :], keys, values, allowed, sinks_ref[...]), w_ref, stage_ref, out_hbm, sems, 0)
-
-
-def stages(shares):
-    return [pltpu.VMEM((shares, WINDOW, LANES), BF16), pltpu.SemaphoreType.DMA((shares // 2,))]
-
-
-def attention_later(sinks, q, kv, w):
-    shares = w.shape[1] // LANES
-    return pl.pallas_call(
-        later_body,
-        out_shape=pltpu.HBM((shares, q.shape[0], LANES), BF16),
-        in_specs=[VMEM_SPEC] * 4,
-        out_specs=pl.BlockSpec(memory_space=pltpu.HBM),
-        scratch_shapes=stages(shares),
+    project(attend(q_ref[:WINDOW, :], keys, values, allowed, sinks_ref[...]), w_ref, out_ref, 0)
+
+
+def later_and_slots(sinks, q, kv, w, routes, weights, experts, cap):
+    tokens = q.shape[0]
+    slots = experts * cap
+    return pl.pallas_call(
+        functools.partial(later_body, cap, experts),
+        out_shape=(
+            vmem_out((w.shape[1] // LANES, tokens, LANES)),
+            vmem_out((slots, tokens)),
+            vmem_out((2 * tokens, slots)),
+            pltpu.VMEM((tokens, 8), F32),
+        ),
+        in_specs=[VMEM_SPEC] * 6,
+        out_specs=(VMEM_SPEC,) * 4,
         compiler_params=small_kernel(16),
         cost_estimate=pl.CostEstimate(flops=10**9, bytes_accessed=2**20, transcendentals=2**16),
-        name="attention_later",
-    )(*in_vmem(sinks, q, kv, w))
+        name="later_and_slots",
+    )(*in_vmem(sinks, q, kv, w, routes, weights))
 
 
 def attention_first(sinks, q, kv, before, w, partial):
     shares = w.shape[1] // LANES
     return pl.pallas_call(
         first_body,
-        out_shape=pltpu.HBM(partial.shape, BF16),
-        in_specs=[VMEM_SPEC] * 5 + [pl.BlockSpec(memory_space=pltpu.HBM)],
-        out_specs=pl.BlockSpec(memory_space=pltpu.HBM),
-        scratch_shapes=stages(shares),
+        out_shape=vmem_out(partial.shape),
+        in_specs=[VMEM_SPEC] * 6,
+        out_specs=VMEM_SPEC,
         input_output_aliases={5: 0},
         compiler_params=small_kernel(16),
         name="attention_first",
-    )(*in_vmem(sinks, q, kv, before, w), *in_hbm(partial))
-
-
-def load_body(sinks_hbm, q_hbm, k_hbm, v_hbm, w_hbm, last_ref, kv_ref, sinks_ref, q_ref, w_ref, k_ref, v_ref, sinks_smem, sems):
-    pairs = ((k_hbm, k_ref), (v_hbm, v_ref), (q_hbm, q_ref), (w_hbm, w_ref), (sinks_hbm, sinks_smem))
+    )(*in_vmem(sinks, q, kv, before, w, partial))
+
+
+def load_body(*refs):
+    sources, (last_ref, kv_ref, sinks_ref, q_ref, w_ref, routes_ref, weights_ref, own_ref) = refs[:8], refs[8:16]
+    k_ref, v_ref, sinks_smem, sems = refs[16:]
+    k_hbm, v_hbm, q_hbm, w_hbm, sinks_hbm, routes_hbm, weights_hbm, stream_hbm = sources
+    first_col = pl.multiple_of(lax.axis_index(TP) * LANES, LANES)
+    pairs = (
+        (k_hbm, k_ref),
+        (v_hbm, v_ref),
+        (q_hbm, q_ref),
+        (w_hbm, w_ref),
+        (sinks_hbm, sinks_smem),
+        (routes_hbm, routes_ref),
+        (weights_hbm, weights_ref),
+        (stream_hbm.at[:, pl.ds(first_col, LANES)], own_ref),
+    )
     copies = [pltpu.make_async_copy(source, target, sems.at[i]) for i, (source, target) in enumerate(pairs)]
     for copy in copies:
         copy.start()
@@ -155,21 +188,35 @@
     copies[4].wait()
     row = lax.broadcasted_iota(jnp.int32, sinks_ref.shape, 0)
     sinks_ref[...] = jnp.where(row == 0, sinks_smem[0], sinks_smem[1])
-    copies[2].wait()
-    copies[3].wait()
-
-
-def loaded(sinks, q, k, v, w):
+    for i in (2, 3, 5, 6, 7):
+        copies[i].wait()
+
+
+def loaded(k, v, q, w, sinks, routes, weights, stream_in):
     rows = q.shape[0]
     return pl.pallas_call(
         load_body,
-        out_shape=(vmem_out((WINDOW, LANES)), vmem_out((rows, LANES)), pltpu.VMEM((8, LANES), F32), vmem_out(q.shape), vmem_out(w.shape)),
-        in_specs=[pl.BlockSpec(memory_space=pltpu.HBM)] * 5,
-        out_specs=(VMEM_SPEC,) * 5,
-        scratch_shapes=[pltpu.VMEM(k.shape, BF16), pltpu.VMEM(v.shape, BF16), pltpu.SMEM(sinks.shape, F32), pltpu.SemaphoreType.DMA((5,))],
+        out_shape=(
+            vmem_out((WINDOW, LANES)),
+            vmem_out((rows, LANES)),
+            pltpu.VMEM((8, LANES), F32),
+            vmem_out(q.shape),
+            vmem_out(w.shape),
+            pltpu.VMEM(routes.shape, jnp.int32),
+            pltpu.VMEM(weights.shape, F32),
+            vmem_out((rows, LANES)),
+        ),
+        in_specs=[pl.BlockSpec(memory_space=pltpu.HBM)] * 8,
+        out_specs=(VMEM_SPEC,) * 8,
+        scratch_shapes=[
+            pltpu.VMEM(k.shape, BF16),
+            pltpu.VMEM(v.shape, BF16),
+            pltpu.SMEM(sinks.shape, F32),
+            pltpu.SemaphoreType.DMA((8,)),
+        ],
         compiler_params=small_kernel(16),
         name="load",
-    )(*in_hbm(sinks, q, k, v, w))
+    )(*in_hbm(k, v, q, w, sinks, routes, weights, stream_in))
 
 
 def copies_body(rows_ref, out_ref):
@@ -212,50 +259,6 @@
         compiler_params=small_kernel(16),
         name="total",
     )(*in_vmem(parts))
-
-
-def slots_body(cap, experts, routes_ref, wide_ref, send_ref, take_ref):
-    tokens = routes_ref.shape[0]
-    slots = send_ref.shape[0]
-    lane = lax.broadcasted_iota(jnp.int32, (tokens, LANES), 1)
-    picks = [routes_ref[:, k : k + 1] for k in range(2)]
-    hot = [(picks[k] == lane).astype(F32) for k in range(2)]
-    r = lax.broadcasted_iota(jnp.int32, (tokens, tokens), 0)
-    c = lax.broadcasted_iota(jnp.int32, (tokens, tokens), 1)
-    ahead = dot((c < r).astype(BF16), (hot[0] + hot[1]).astype(BF16))
-    slot_lane = lax.broadcasted_iota(jnp.int32, (tokens, slots), 1)
-    for k in range(2):
-        rank = jnp.sum(ahead * hot[k], axis=1, keepdims=True).astype(jnp.int32)
-        target = picks[k] * cap + rank
-        take_ref[k * tokens : (k + 1) * tokens, :] = (slot_lane == target).astype(F32).astype(BF16)
-    sub = lax.broadcasted_iota(jnp.int32, (experts, tokens), 0)
-    picks_w = [wide_ref[k : k + 1, :] for k in range(2)]
-    hot_w = [(picks_w[k] == sub).astype(F32) for k in range(2)]
-    ahead_w = dot((hot_w[0] + hot_w[1]).astype(BF16), (r < c).astype(BF16))
-    slot_sub = lax.broadcasted_iota(jnp.int32, (slots, tokens), 0)
-    hit = None
-    for k in range(2):
-        rank = jnp.sum(ahead_w * hot_w[k], axis=0, keepdims=True).astype(jnp.int32)
-        target = picks_w[k] * cap + rank
-        here = slot_sub == target
-        hit = here if hit is None else hit | here
-    send_ref[...] = hit.astype(F32).astype(BF16)
-
-
-def slot_matrices(routes, experts, cap):
-    tokens = routes.shape[0]
-    slots = experts * cap
-    return pl.pallas_call(
-        functools.partial(slots_body, cap, experts),
-        out_shape=(
-            vmem_out((slots, tokens)),
-            vmem_out((2 * tokens, slots)),
-        ),
-        in_specs=[VMEM_SPEC] * 2,
-        out_specs=(VMEM_SPEC, VMEM_SPEC),
-        compiler_params=small_kernel(16),
-        name="slots",
-    )(*in_vmem(routes, routes.T))
 
 
 def stream_body(arrived_ref, own_ref, send_ref, stream_ref, rows_ref):
@@ -308,7 +311,7 @@
 def combine_body(rows_ref, take_ref, weights_ref, stream_ref, out_ref):
     tokens = stream_ref.shape[0]
     taken = dot(take_ref[...], rows_ref[...])
-    moe = taken[:tokens] * weights_ref[:, 0:1] + taken[tokens:] * weights_ref[:, 1:2]
+    moe = taken[:tokens] * weights_ref[:, 2:3] + taken[tokens:] * weights_ref[:, 3:4]
     out_ref[...] = (stream_ref[...].astype(F32) + moe).astype(BF16)
 
 
@@ -320,7 +323,7 @@
         out_specs=VMEM_SPEC,
         compiler_params=small_kernel(16),
         name="combine",
-    )(*in_vmem(rows, take), weights, *in_vmem(stream))
+    )(*in_vmem(rows, take, weights, stream))
 
 
 def per_device(
@@ -340,15 +343,14 @@
     tokens = query_rows.shape[0]
     tp_size = lax.axis_size(TP)
     experts = lax.axis_size("sp")
-    tp_index = lax.axis_index(TP)
-    last, kv, sinks, queries, out_share = loaded(sink_logits, query_rows, key_rows, value_rows, out_weight)
+    cap = 3 * tokens * routes.shape[1] // (2 * experts)
+    last, kv, sinks, queries, out_share, choices, weights, own = loaded(
+        key_rows, value_rows, query_rows, out_weight, sink_logits, routes.T, route_weights.T, stream_in
+    )
     before = lax.ppermute(last, "sp", [(i, i + 1) for i in range(experts - 1)])
-    later = attention_later(sinks, queries, kv, out_share)
+    later, send, take, cols = later_and_slots(sinks, queries, kv, out_share, choices, weights, experts, cap)
     partial = attention_first(sinks, queries, kv, before, out_share, later)
     arrived = lax.all_to_all(partial, TP, split_axis=0, concat_axis=0, tiled=True)
-    cap = 3 * tokens * routes.shape[1] // (2 * experts)
-    send, take = slot_matrices(routes, experts, cap)
-    own = lax.dynamic_slice_in_dim(stream_in, tp_index * LANES, LANES, 1)
     stream, rows = stream_and_rows(arrived, own, send)
     rows = lax.all_to_all(rows.reshape(experts, cap, LANES), "sp", split_axis=0, concat_axis=0, tiled=True)
     slots = experts * cap
@@ -358,7 +360,7 @@
     parts = expert(features, gain, gate_weight, up_weight, down_weight, 384)
     summed = total(lax.all_to_all(parts, TP, split_axis=0, concat_axis=0, tiled=True))
     returned = lax.all_to_all(summed.reshape(experts, cap, LANES), "sp", split_axis=0, concat_axis=0, tiled=True)
-    out = combine(returned.reshape(slots, LANES), take, route_weights, stream)
+    out = combine(returned.reshape(slots, LANES), take, cols, stream)
     return lax.all_to_all(out, TP, split_axis=0, concat_axis=1, tiled=True)
 
 

time: 182 us -> 179 us (0.984)
  blocking collectives: 108 us -> 167 us
  waiting for transfers between devices: 35.6 us -> 0.01 us
  starting transfers between devices: 25.7 us -> 1.74 us
  Pallas kernels: 11.5 us -> 8.93 us
    all_to_all x0 -> x2, blocking collectives: none -> 59.2 us  [the longest x1 34.1 us: per_device(): lax.all_to_all(summed.reshape(experts, cap, LANES), 'sp', split_axis=0, c...]
    all_to_all x2 -> x0, waiting for transfers between devices: 35.6 us -> none  [the longest x1 19.8 us: per_device(): lax.all_to_all(summed.reshape(experts, cap, LANES), 'sp', split_axis=0, c...]
    all_to_all x2 -> x0, starting transfers between devices: 24 us -> none  [the longest x1 15.1 us: per_device(): lax.all_to_all(summed.reshape(experts, cap, LANES), 'sp', split_axis=0, c...]
    pallas_call x3 -> x2, Pallas kernels: 4.74 us -> 2.8 us  [the longest x1 1.61 us: later_and_slots(): pl.pallas_call(functools.partial(later_body, cap, experts), out_shape=(vm...]
  transfers between devices with their start and end apart: 3 -> 1, of which waited for: 2 -> 0; matrix products, arithmetic and copies ran while one was open for 0% -> 0% of each run, Pallas kernels for 2% -> 1%
where the time goes in v7:
time: 179 us
  blocking collectives  167 us (93%)
  Pallas kernels  8.93 us (5%)
    all_to_all x1, blocking collectives, per_device(): lax.all_to_all(rows.reshape(experts, cap, LANES), 'sp', split_axis=0, con...  35 us
    all_to_all x1, blocking collectives, per_device(): lax.all_to_all(summed.reshape(experts, cap, LANES), 'sp', split_axis=0, c...  34.1 us
    all_to_all x1, blocking collectives, per_device(): lax.all_to_all(parts, TP, split_axis=0, concat_axis=0, tiled=True)  31.9 us
    all_to_all x1, blocking collectives, per_device(): lax.all_to_all(copies, TP, split_axis=0, concat_axis=0, tiled=True)  31.1 us
    all_to_all x1, blocking collectives, per_device(): lax.all_to_all(partial, TP, split_axis=0, concat_axis=0, tiled=True)  25.1 us
    all_to_all x1, blocking collectives, per_device(): return lax.all_to_all(out, TP, split_axis=0, concat_axis=1, tiled=True)  10.2 us
  transfers between devices with their start and end apart: 1, of which 0 were waited for; matrix products, arithmetic and copies ran while one was open for 0% of the time, Pallas kernels for 1%

profile of v7, /device:TPU:2, one launch (start us, length us, event | category | flops | bytes accessed | tf_op | source)
XLA Modules:
  0.0 178.9 jit_solution(1810440793660187203)
XLA Ops:
  0.0 1.3 load.1
  1.3 1.7 collective-permute-start
  3.0 1.6 later_and_slots.1
  4.7 0.0 collective-permute-done.before_ref
  4.7 1.2 attention_first.1
  5.9 25.1 %all_to_all.44.arrived_ref = bf16[16,256,128]{2,1,0:T(8,128)(2,1)S(1)} all-to-all(bf16[16,256,128]{2,1,0:T(8,128)(2,1)S(1)} %attention_first.1), channel_id=1, replica_groups=mesh['sp'=32,'tp_0'=4,'tp_1'=4] {'tp_0','tp_1'}, dimensions={0} | all-to-all | bytes 2097152 | tf_op jit(solution)/shard_map/all_to_all | solution.py:353
  31.0 0.4 stream.1
  31.3 35.0 %all_to_all.45 = bf16[32,24,128]{2,1,0:T(8,128)(2,1)S(1)} all-to-all(bf16[32,24,128]{2,1,0:T(8,128)(2,1)S(1)} %bitcast.18), channel_id=1, replica_groups=mesh['sp'=32,'tp_0'=4,'tp_1'=4] {'sp'}, dimensions={0} | all-to-all | bytes 393216 | tf_op jit(solution)/shard_map/all_to_all | solution.py:355
  66.3 0.6 copies.1
  66.9 0.0 copy-start
  67.0 0.0 copy-start.1
  67.0 0.0 copy-start.2
  67.0 0.0 copy-start.3
  67.0 31.1 %all_to_all.46.x_ref = bf16[16,768,128]{2,1,0:T(8,128)(2,1)S(1)} all-to-all(bf16[16,768,128]{2,1,0:T(8,128)(2,1)S(1)} %copies.1), channel_id=1, replica_groups=mesh['sp'=32,'tp_0'=4,'tp_1'=4] {'tp_0','tp_1'}, dimensions={0} | all-to-all | bytes 6291456 | tf_op jit(solution)/shard_map/all_to_all | solution.py:359
  98.1 0.0 copy-done
  98.1 0.0 copy-done.1
  98.1 0.0 copy-done.2
  98.1 0.0 copy-done.3
  98.1 3.1 %expert.1 = bf16[16,768,128]{2,1,0:T(8,128)(2,1)S(1)} custom-call(bf16[16,768,128]{2,1,0:T(8,128)(2,1)S(1)} %all_to_all.46.x_ref, f32[1,2048]{1,0:T(1,128)S(1)} %bitcast.19, bf16[1,2048,256]{2,1,0:T(8,128)(2,1)S(1)} %copy-done, bf16[1,2048,256]{2,1,0:T(8,128)(2,1)S(1)} %copy-done.1, bf16[1,256,2048]{2,1,0:T(8,128)(2,1)S(1)} %copy-done.2), custom_call_target="tpu_custom_call" | custom-call | flops 2415919104 | bytes 6291456 | tf_op jit(solution)/shard_map/expert/pallas_call | solution.py:300
  101.2 31.9 %all_to_all.47.parts_ref = bf16[16,768,128]{2,1,0:T(8,128)(2,1)S(1)} all-to-all(bf16[16,768,128]{2,1,0:T(8,128)(2,1)S(1)} %expert.1), channel_id=1, replica_groups=mesh['sp'=32,'tp_0'=4,'tp_1'=4] {'tp_0','tp_1'}, dimensions={0} | all-to-all | bytes 6291456 | tf_op jit(solution)/shard_map/all_to_all | solution.py:361
  133.1 0.4 total.1
  133.5 34.1 %all_to_all.48 = bf16[32,24,128]{2,1,0:T(8,128)(2,1)S(1)} all-to-all(bf16[32,24,128]{2,1,0:T(8,128)(2,1)S(1)} %bitcast.16), channel_id=1, replica_groups=mesh['sp'=32,'tp_0'=4,'tp_1'=4] {'sp'}, dimensions={0} | all-to-all | bytes 393216 | tf_op jit(solution)/shard_map/all_to_all | solution.py:362
  167.6 0.4 combine.1
  168.0 10.2 %all_to_all.49 = bf16[16,16,128]{2,1,0:T(8,128)(2,1)S(1)} all-to-all(bf16[16,16,128]{2,1,0:T(8,128)(2,1)S(1)} %bitcast.17), channel_id=1, replica_groups=mesh['sp'=32,'tp_0'=4,'tp_1'=4] {'tp_0','tp_1'}, dimensions={0} | all-to-all | bytes 131072 | tf_op jit(solution)/shard_map/all_to_all | solution.py:364
  178.2 0.6 copy_bitcast_fusion
Async XLA Ops:
  1.3 3.4 %collective-permute-start = (bf16[128,128]{1,0:T(8,128)(2,1)S(1)}, bf16[128,128]{1,0:T(8,128)(2,1)S(1)}, u32[]{:S(2)}, u32[]{:S(2)}) collective-permute-start(bf16[128,128]{1,0:T(8,128)(2,1)S(1)} %get-tuple-element.22), channel_id=1, source_target_pairs={{0,16},{16,32},{32,48},{48,64},{64,80},{80,96},{96,112},{112,128},... | collective-permute-start | bytes 98312 | tf_op jit(solution)/shard_map/ppermute | solution.py:350
  66.9 31.2 %copy-start = (bf16[1,2048,256]{2,1,0:T(8,128)(2,1)S(1)}, bf16[1,2048,256]{2,1,0:T(8,128)(2,1)}, u32[]{:S(2)}) copy-start(bf16[1,2048,256]{2,1,0:T(8,128)(2,1)} %gate_ref.1) | copy-start | bytes 3145732
  67.0 31.2 %copy-start.1 = (bf16[1,2048,256]{2,1,0:T(8,128)(2,1)S(1)}, bf16[1,2048,256]{2,1,0:T(8,128)(2,1)}, u32[]{:S(2)}) copy-start(bf16[1,2048,256]{2,1,0:T(8,128)(2,1)} %up_ref.1) | copy-start | bytes 3145732
  67.0 31.2 %copy-start.2 = (bf16[1,256,2048]{2,1,0:T(8,128)(2,1)S(1)}, bf16[1,256,2048]{2,1,0:T(8,128)(2,1)}, u32[]{:S(2)}) copy-start(bf16[1,256,2048]{2,1,0:T(8,128)(2,1)} %down_ref.1) | copy-start | bytes 3145732
  67.0 31.2 %copy-start.3 = (f32[2048]{0:T(1024)S(1)}, f32[2048]{0:T(1024)}, u32[]{:S(2)}) copy-start(f32[2048]{0:T(1024)} %param.18) | copy-start | bytes 24580

commit v8 on v7

--- a/solution.py
+++ b/solution.py
@@ -13,12 +13,13 @@
 WINDOW = 128
 LANES = 128
 TP = ("tp_0", "tp_1")
-SP_TP = ("sp", "tp_0", "tp_1")
+SP = ("z", "core")
+PLANES = ("core", "tp_0", "tp_1")
+SIDE = 4
 NORM_EPS = 1e-06
 BF16 = jnp.bfloat16
 F32 = jnp.float32
 VMEM_SPEC = pl.BlockSpec(memory_space=pltpu.VMEM)
-LAG_NS = 16500
 
 
 def in_vmem(*arrays):
@@ -114,7 +115,7 @@
 def first_body(sinks_ref, q_ref, kv_ref, before_ref, w_ref, partial_ref, out_ref):
     keys, values = both_places(jnp.concatenate([before_ref[...], kv_ref[:WINDOW, :]], axis=0).astype(F32))
     inside, col = window_mask()
-    allowed = inside & ((col >= WINDOW) | (lax.axis_index("sp") > 0))
+    allowed = inside & ((col >= WINDOW) | (lax.axis_index(SP) > 0))
     project(attend(q_ref[:WINDOW, :], keys, values, allowed, sinks_ref[...]), w_ref, out_ref, 0)
 
 
@@ -220,10 +221,6 @@
 
 
 def copies_body(rows_ref, out_ref):
-    @pl.when(lax.axis_index("sp") % 2 == 1)
-    def _():
-        pl.delay(LAG_NS)
-
     rows = rows_ref[...]
     for t in range(out_ref.shape[0]):
         out_ref[t] = rows
@@ -242,7 +239,7 @@
 
 def total_body(parts_ref, out_ref):
     rows = parts_ref.shape[1]
-    block = 64
+    block = 128
     for lo in range(0, rows, block):
         summed = parts_ref[0, lo : lo + block, :].astype(F32)
         for t in range(1, parts_ref.shape[0]):
@@ -283,17 +280,19 @@
 
 def expert_body(block, x_ref, gain_ref, gate_ref, up_ref, down_ref, out_ref):
     shares, rows, _ = x_ref.shape
+    flipped = lax.axis_index("core") == 1
+    place = [jnp.where(flipped, t % SIDE * SIDE + t // SIDE, t) for t in range(shares)]
     for lo in range(0, rows, block):
-        stream = jnp.concatenate([x_ref[t, lo : lo + block, :] for t in range(shares)], axis=1).astype(F32)
+        stream = jnp.concatenate([x_ref[place[t], lo : lo + block, :] for t in range(shares)], axis=1).astype(F32)
+        scaled = (stream * gain_ref[...]).astype(BF16)
         scale = lax.rsqrt(jnp.mean(stream * stream, axis=-1, keepdims=True) + NORM_EPS)
-        normed = (stream * scale * gain_ref[...]).astype(BF16)
-        gate_act = dot(normed, gate_ref[0])
-        up_act = dot(normed, up_ref[0])
+        gate_act = dot(scaled, gate_ref[0]) * scale
+        up_act = dot(scaled, up_ref[0]) * scale
         hidden = (gate_act * jax.nn.sigmoid(gate_act) * up_act).astype(BF16)
         for t in range(0, shares, 2):
             both = dot(hidden, down_ref[0, :, t * LANES : (t + 2) * LANES]).astype(BF16)
-            out_ref[t, lo : lo + block, :] = both[:, :LANES]
-            out_ref[t + 1, lo : lo + block, :] = both[:, LANES:]
+            out_ref[place[t], lo : lo + block, :] = both[:, :LANES]
+            out_ref[place[t + 1], lo : lo + block, :] = both[:, LANES:]
 
 
 def expert(x, gain, gate, up, down, block):
@@ -324,6 +323,19 @@
         compiler_params=small_kernel(16),
         name="combine",
     )(*in_vmem(rows, take, weights, stream))
+
+
+def lines(core, dim):
+    at = [[core * SIDE * SIDE + y * SIDE + x for x in range(SIDE)] for y in range(SIDE)]
+    return at if dim == 1 else [list(line) for line in zip(*at)]
+
+
+LINES = lines(0, 1) + lines(1, 0)
+CROSSING = lines(0, 0) + lines(1, 1)
+
+
+def along(parts, groups):
+    return lax.all_to_all(parts, PLANES, split_axis=0, concat_axis=0, axis_index_groups=groups, tiled=True)
 
 
 def per_device(
@@ -342,44 +354,47 @@
 ):
     tokens = query_rows.shape[0]
     tp_size = lax.axis_size(TP)
-    experts = lax.axis_size("sp")
+    experts = lax.axis_size(SP)
     cap = 3 * tokens * routes.shape[1] // (2 * experts)
     last, kv, sinks, queries, out_share, choices, weights, own = loaded(
         key_rows, value_rows, query_rows, out_weight, sink_logits, routes.T, route_weights.T, stream_in
     )
-    before = lax.ppermute(last, "sp", [(i, i + 1) for i in range(experts - 1)])
+    before = lax.ppermute(last, SP, [(i, i + 1) for i in range(experts - 1)])
     later, send, take, cols = later_and_slots(sinks, queries, kv, out_share, choices, weights, experts, cap)
     partial = attention_first(sinks, queries, kv, before, out_share, later)
     arrived = lax.all_to_all(partial, TP, split_axis=0, concat_axis=0, tiled=True)
     stream, rows = stream_and_rows(arrived, own, send)
-    rows = lax.all_to_all(rows.reshape(experts, cap, LANES), "sp", split_axis=0, concat_axis=0, tiled=True)
+    rows = lax.all_to_all(rows.reshape(experts, cap, LANES), SP, split_axis=0, concat_axis=0, tiled=True)
     slots = experts * cap
     gain = norm_gain.reshape(1, -1)
-    copies = copied(rows.reshape(slots, LANES), tp_size)
-    features = lax.all_to_all(copies, TP, split_axis=0, concat_axis=0, tiled=True)
-    parts = expert(features, gain, gate_weight, up_weight, down_weight, 384)
-    summed = total(lax.all_to_all(parts, TP, split_axis=0, concat_axis=0, tiled=True))
-    returned = lax.all_to_all(summed.reshape(experts, cap, LANES), "sp", split_axis=0, concat_axis=0, tiled=True)
+    features = rows.reshape(slots, LANES)
+    for groups in (LINES, CROSSING):
+        features = along(copied(features, SIDE), groups).reshape(-1, LANES)
+    parts = expert(features.reshape(tp_size, slots, LANES), gain, gate_weight, up_weight, down_weight, 384)
+    for groups in (CROSSING, LINES):
+        parts = total(along(parts.reshape(SIDE, -1, LANES), groups))
+    summed = parts
+    returned = lax.all_to_all(summed.reshape(experts, cap, LANES), SP, split_axis=0, concat_axis=0, tiled=True)
     out = combine(returned.reshape(slots, LANES), take, cols, stream)
     return lax.all_to_all(out, TP, split_axis=0, concat_axis=1, tiled=True)
 
 
 def solution(mesh):
-    finer = Mesh(mesh.devices.reshape(mesh.shape["sp"], 4, 4), ("sp", "tp_0", "tp_1"))
+    finer = Mesh(mesh.devices.reshape(-1, 2, SIDE, SIDE), (*SP, *TP))
     placed = (
-        P("sp", TP),
-        P("sp", None),
-        P("sp", None),
+        P(SP, TP),
+        P(SP, None),
+        P(SP, None),
         P(TP),
         P(TP, None),
-        P("sp", None),
+        P(SP, None),
         P(),
-        P("sp", None),
-        P("sp", None),
-        P("sp", None, TP),
-        P("sp", None, TP),
-        P("sp", TP, None),
+        P(SP, None),
+        P(SP, None),
+        P(SP, None, TP),
+        P(SP, None, TP),
+        P(SP, TP, None),
     )
     return jax.shard_map(
-        per_device, mesh=finer, in_specs=placed, out_specs=P(SP_TP, None), check_vma=False
+        per_device, mesh=finer, in_specs=placed, out_specs=P((*SP, *TP), None), check_vma=False
     )

time: 179 us -> 178 us (level)
    all_to_all x4 -> x6, blocking collectives: 132 us -> 131 us  [the longest x4 73.2 us: along(): lax.all_to_all(parts, PLANES, split_axis=0, concat_axis=0, axis_index_gro...]
where the time goes in v8:
time: 178 us
  blocking collectives  167 us (94%)
  Pallas kernels  8.61 us (5%)
    all_to_all x4, blocking collectives, along(): lax.all_to_all(parts, PLANES, split_axis=0, concat_axis=0, axis_index_gro...  73.2 us
    all_to_all x1, blocking collectives, per_device(): lax.all_to_all(rows.reshape(experts, cap, LANES), SP, split_axis=0, conca...  35 us
    all_to_all x1, blocking collectives, per_device(): lax.all_to_all(partial, TP, split_axis=0, concat_axis=0, tiled=True)  25.1 us
    all_to_all x1, blocking collectives, per_device(): lax.all_to_all(summed.reshape(experts, cap, LANES), SP, split_axis=0, con...  22.9 us
    all_to_all x1, blocking collectives, per_device(): return lax.all_to_all(out, TP, split_axis=0, concat_axis=1, tiled=True)  10.6 us
  transfers between devices with their start and end apart: 1, of which 0 were waited for; matrix products, arithmetic and copies ran while one was open for 0% of the time, Pallas kernels for 1%

profile of v8, /device:TPU:2, one launch (start us, length us, event | category | flops | bytes accessed | tf_op | source)
XLA Modules:
  0.0 178.0 jit_solution(16473757705404459683)
XLA Ops:
  0.0 1.3 load.1
  1.3 1.7 collective-permute-start
  3.0 1.6 later_and_slots.1
  4.7 0.0 collective-permute-done.before_ref
  4.7 1.2 attention_first.1
  5.9 25.1 %all_to_all.54.arrived_ref = bf16[16,256,128]{2,1,0:T(8,128)(2,1)S(1)} all-to-all(bf16[16,256,128]{2,1,0:T(8,128)(2,1)S(1)} %attention_first.1), channel_id=1, replica_groups=mesh['z'=16,'core'=2,'tp_0'=4,'tp_1'=4] {'tp_0','tp_1'}, dimensions={0} | all-to-all | bytes 2097152 | tf_op jit(solution)/shard_map/all_to_all | solution.py:365
  31.0 0.4 stream.1
  31.3 35.0 %all_to_all.55 = bf16[32,24,128]{2,1,0:T(8,128)(2,1)S(1)} all-to-all(bf16[32,24,128]{2,1,0:T(8,128)(2,1)S(1)} %bitcast.26), channel_id=1, replica_groups=mesh['z'=16,'core'=2,'tp_0'=4,'tp_1'=4] {'z','core'}, dimensions={0} | all-to-all | bytes 393216 | tf_op jit(solution)/shard_map/all_to_all | solution.py:367
  66.3 0.1 copies.2
  66.4 11.8 %all_to_all.56 = bf16[4,768,128]{2,1,0:T(8,128)(2,1)S(1)} all-to-all(bf16[4,768,128]{2,1,0:T(8,128)(2,1)S(1)} %copies.2), channel_id=1, replica_groups={{0,1,2,3},{4,5,6,7},{8,9,10,11},{12,13,14,15},{16,20,24,28},{17,21,25,2..., dimensions={0} | all-to-all | bytes 1572864 | tf_op jit(solution)/shard_map/all_to_all | solution.py:338
  78.2 0.4 copies.3
  78.6 0.0 copy-start
  78.6 0.0 copy-start.1
  78.6 0.0 copy-start.2
  78.7 0.0 copy-start.3
  78.7 24.9 %all_to_all.57 = bf16[4,3072,128]{2,1,0:T(8,128)(2,1)S(1)} all-to-all(bf16[4,3072,128]{2,1,0:T(8,128)(2,1)S(1)} %copies.3), channel_id=1, replica_groups={{0,4,8,12},{1,5,9,13},{2,6,10,14},{3,7,11,15},{16,17,18,19},{20,21,22,2..., dimensions={0} | all-to-all | bytes 6291456 | tf_op jit(solution)/shard_map/all_to_all | solution.py:338
  103.6 0.0 copy-done
  103.6 0.0 copy-done.1
  103.6 0.0 copy-done.2
  103.6 0.0 copy-done.3
  103.6 2.8 %expert.1 = bf16[16,768,128]{2,1,0:T(8,128)(2,1)S(1)} custom-call(bf16[16,768,128]{2,1,0:T(8,128)(2,1)S(1)} %bitcast.18, f32[1,2048]{1,0:T(1,128)S(1)} %bitcast.27, bf16[1,2048,256]{2,1,0:T(8,128)(2,1)S(1)} %copy-done, bf16[1,2048,256]{2,1,0:T(8,128)(2,1)S(1)} %copy-done.1, bf16[1,256,2048]{2,1,0:T(8,128)(2,1)S(1)} %copy-done.2), custom_call_target="tpu_custom_call" | custom-call | flops 2415919104 | bytes 6291456 | tf_op jit(solution)/shard_map/expert/pallas_call | solution.py:299
  106.4 24.6 %all_to_all.58.parts_ref = bf16[4,3072,128]{2,1,0:T(8,128)(2,1)S(1)} all-to-all(bf16[4,3072,128]{2,1,0:T(8,128)(2,1)S(1)} %bitcast.19), channel_id=1, replica_groups={{0,4,8,12},{1,5,9,13},{2,6,10,14},{3,7,11,15},{16,17,18,19},{20,21,22,2..., dimensions={0} | all-to-all | bytes 6291456 | tf_op jit(solution)/shard_map/all_to_all | solution.py:338
  131.0 0.4 total.2
  131.4 11.9 %all_to_all.59.parts_ref = bf16[4,768,128]{2,1,0:T(8,128)(2,1)S(1)} all-to-all(bf16[4,768,128]{2,1,0:T(8,128)(2,1)S(1)} %bitcast.21), channel_id=1, replica_groups={{0,1,2,3},{4,5,6,7},{8,9,10,11},{12,13,14,15},{16,20,24,28},{17,21,25,2..., dimensions={0} | all-to-all | bytes 1572864 | tf_op jit(solution)/shard_map/all_to_all | solution.py:338
  143.3 0.1 total.3
  143.4 22.9 %all_to_all.60 = bf16[32,24,128]{2,1,0:T(8,128)(2,1)S(1)} all-to-all(bf16[32,24,128]{2,1,0:T(8,128)(2,1)S(1)} %bitcast.24), channel_id=1, replica_groups=mesh['z'=16,'core'=2,'tp_0'=4,'tp_1'=4] {'z','core'}, dimensions={0} | all-to-all | bytes 393216 | tf_op jit(solution)/shard_map/all_to_all | solution.py:377
  166.4 0.4 combine.1
  166.7 10.6 %all_to_all.61 = bf16[16,16,128]{2,1,0:T(8,128)(2,1)S(1)} all-to-all(bf16[16,16,128]{2,1,0:T(8,128)(2,1)S(1)} %bitcast.25), channel_id=1, replica_groups=mesh['z'=16,'core'=2,'tp_0'=4,'tp_1'=4] {'tp_0','tp_1'}, dimensions={0} | all-to-all | bytes 131072 | tf_op jit(solution)/shard_map/all_to_all | solution.py:379
  177.4 0.6 copy_bitcast_fusion
Async XLA Ops:
  1.3 3.4 %collective-permute-start = (bf16[128,128]{1,0:T(8,128)(2,1)S(1)}, bf16[128,128]{1,0:T(8,128)(2,1)S(1)}, u32[]{:S(2)}, u32[]{:S(2)}) collective-permute-start(bf16[128,128]{1,0:T(8,128)(2,1)S(1)} %get-tuple-element.22), channel_id=1, source_target_pairs={{0,16},{16,32},{32,48},{48,64},{64,80},{80,96},{96,112},{112,128},... | collective-permute-start | bytes 98312 | tf_op jit(solution)/shard_map/ppermute | solution.py:362
  78.6 25.0 %copy-start = (bf16[1,2048,256]{2,1,0:T(8,128)(2,1)S(1)}, bf16[1,2048,256]{2,1,0:T(8,128)(2,1)}, u32[]{:S(2)}) copy-start(bf16[1,2048,256]{2,1,0:T(8,128)(2,1)} %gate_ref.1) | copy-start | bytes 3145732
  78.6 24.9 %copy-start.1 = (bf16[1,2048,256]{2,1,0:T(8,128)(2,1)S(1)}, bf16[1,2048,256]{2,1,0:T(8,128)(2,1)}, u32[]{:S(2)}) copy-start(bf16[1,2048,256]{2,1,0:T(8,128)(2,1)} %up_ref.1) | copy-start | bytes 3145732
  78.6 24.9 %copy-start.2 = (bf16[1,256,2048]{2,1,0:T(8,128)(2,1)S(1)}, bf16[1,256,2048]{2,1,0:T(8,128)(2,1)}, u32[]{:S(2)}) copy-start(bf16[1,256,2048]{2,1,0:T(8,128)(2,1)} %down_ref.1) | copy-start | bytes 3145732
  78.7 24.9 %copy-start.3 = (f32[2048]{0:T(1024)S(1)}, f32[2048]{0:T(1024)}, u32[]{:S(2)}) copy-start(f32[2048]{0:T(1024)} %param.18) | copy-start | bytes 24580

commit v9 on v8

--- a/solution.py
+++ b/solution.py
@@ -370,7 +370,7 @@
     features = rows.reshape(slots, LANES)
     for groups in (LINES, CROSSING):
         features = along(copied(features, SIDE), groups).reshape(-1, LANES)
-    parts = expert(features.reshape(tp_size, slots, LANES), gain, gate_weight, up_weight, down_weight, 384)
+    parts = expert(features.reshape(tp_size, slots, LANES), gain, gate_weight, up_weight, down_weight, slots)
     for groups in (CROSSING, LINES):
         parts = total(along(parts.reshape(SIDE, -1, LANES), groups))
     summed = parts

time: 178 us -> 178 us (level)
  no operation moved by 1% of the time
where the time goes in v9:
time: 178 us
  blocking collectives  167 us (94%)
  Pallas kernels  8.48 us (5%)
    all_to_all x4, blocking collectives, along(): lax.all_to_all(parts, PLANES, split_axis=0, concat_axis=0, axis_index_gro...  73.2 us
    all_to_all x1, blocking collectives, per_device(): lax.all_to_all(rows.reshape(experts, cap, LANES), SP, split_axis=0, conca...  35 us
    all_to_all x1, blocking collectives, per_device(): lax.all_to_all(partial, TP, split_axis=0, concat_axis=0, tiled=True)  25.1 us
    all_to_all x1, blocking collectives, per_device(): lax.all_to_all(summed.reshape(experts, cap, LANES), SP, split_axis=0, con...  22.9 us
    all_to_all x1, blocking collectives, per_device(): return lax.all_to_all(out, TP, split_axis=0, concat_axis=1, tiled=True)  10.6 us
  transfers between devices with their start and end apart: 1, of which 0 were waited for; matrix products, arithmetic and copies ran while one was open for 0% of the time, Pallas kernels for 1%

profile of v9, /device:TPU:2, one launch (start us, length us, event | category | flops | bytes accessed | tf_op | source)
XLA Modules:
  0.0 177.9 jit_solution(3691318810474094112)
XLA Ops:
  0.0 1.3 load.1
  1.3 1.7 collective-permute-start
  3.0 1.6 later_and_slots.1
  4.7 0.0 collective-permute-done.before_ref
  4.7 1.2 attention_first.1
  5.9 25.1 %all_to_all.54.arrived_ref = bf16[16,256,128]{2,1,0:T(8,128)(2,1)S(1)} all-to-all(bf16[16,256,128]{2,1,0:T(8,128)(2,1)S(1)} %attention_first.1), channel_id=1, replica_groups=mesh['z'=16,'core'=2,'tp_0'=4,'tp_1'=4] {'tp_0','tp_1'}, dimensions={0} | all-to-all | bytes 2097152 | tf_op jit(solution)/shard_map/all_to_all | solution.py:365
  31.0 0.4 stream.1
  31.3 35.0 %all_to_all.55 = bf16[32,24,128]{2,1,0:T(8,128)(2,1)S(1)} all-to-all(bf16[32,24,128]{2,1,0:T(8,128)(2,1)S(1)} %bitcast.26), channel_id=1, replica_groups=mesh['z'=16,'core'=2,'tp_0'=4,'tp_1'=4] {'z','core'}, dimensions={0} | all-to-all | bytes 393216 | tf_op jit(solution)/shard_map/all_to_all | solution.py:367
  66.3 0.1 copies.2
  66.4 11.8 %all_to_all.56 = bf16[4,768,128]{2,1,0:T(8,128)(2,1)S(1)} all-to-all(bf16[4,768,128]{2,1,0:T(8,128)(2,1)S(1)} %copies.2), channel_id=1, replica_groups={{0,1,2,3},{4,5,6,7},{8,9,10,11},{12,13,14,15},{16,20,24,28},{17,21,25,2..., dimensions={0} | all-to-all | bytes 1572864 | tf_op jit(solution)/shard_map/all_to_all | solution.py:338
  78.2 0.4 copies.3
  78.6 0.0 copy-start
  78.6 0.0 copy-start.1
  78.6 0.0 copy-start.2
  78.7 0.0 copy-start.3
  78.7 24.9 %all_to_all.57 = bf16[4,3072,128]{2,1,0:T(8,128)(2,1)S(1)} all-to-all(bf16[4,3072,128]{2,1,0:T(8,128)(2,1)S(1)} %copies.3), channel_id=1, replica_groups={{0,4,8,12},{1,5,9,13},{2,6,10,14},{3,7,11,15},{16,17,18,19},{20,21,22,2..., dimensions={0} | all-to-all | bytes 6291456 | tf_op jit(solution)/shard_map/all_to_all | solution.py:338
  103.6 0.0 copy-done
  103.6 0.0 copy-done.1
  103.6 0.0 copy-done.2
  103.6 0.0 copy-done.3
  103.6 2.6 %expert.1 = bf16[16,768,128]{2,1,0:T(8,128)(2,1)S(1)} custom-call(bf16[16,768,128]{2,1,0:T(8,128)(2,1)S(1)} %bitcast.18, f32[1,2048]{1,0:T(1,128)S(1)} %bitcast.27, bf16[1,2048,256]{2,1,0:T(8,128)(2,1)S(1)} %copy-done, bf16[1,2048,256]{2,1,0:T(8,128)(2,1)S(1)} %copy-done.1, bf16[1,256,2048]{2,1,0:T(8,128)(2,1)S(1)} %copy-done.2), custom_call_target="tpu_custom_call" | custom-call | flops 2415919104 | bytes 6291456 | tf_op jit(solution)/shard_map/expert/pallas_call | solution.py:299
  106.2 24.6 %all_to_all.58.parts_ref = bf16[4,3072,128]{2,1,0:T(8,128)(2,1)S(1)} all-to-all(bf16[4,3072,128]{2,1,0:T(8,128)(2,1)S(1)} %bitcast.19), channel_id=1, replica_groups={{0,4,8,12},{1,5,9,13},{2,6,10,14},{3,7,11,15},{16,17,18,19},{20,21,22,2..., dimensions={0} | all-to-all | bytes 6291456 | tf_op jit(solution)/shard_map/all_to_all | solution.py:338
  130.9 0.4 total.2
  131.3 11.9 %all_to_all.59.parts_ref = bf16[4,768,128]{2,1,0:T(8,128)(2,1)S(1)} all-to-all(bf16[4,768,128]{2,1,0:T(8,128)(2,1)S(1)} %bitcast.21), channel_id=1, replica_groups={{0,1,2,3},{4,5,6,7},{8,9,10,11},{12,13,14,15},{16,20,24,28},{17,21,25,2..., dimensions={0} | all-to-all | bytes 1572864 | tf_op jit(solution)/shard_map/all_to_all | solution.py:338
  143.2 0.1 total.3
  143.3 22.9 %all_to_all.60 = bf16[32,24,128]{2,1,0:T(8,128)(2,1)S(1)} all-to-all(bf16[32,24,128]{2,1,0:T(8,128)(2,1)S(1)} %bitcast.24), channel_id=1, replica_groups=mesh['z'=16,'core'=2,'tp_0'=4,'tp_1'=4] {'z','core'}, dimensions={0} | all-to-all | bytes 393216 | tf_op jit(solution)/shard_map/all_to_all | solution.py:377
  166.2 0.4 combine.1
  166.6 10.6 %all_to_all.61 = bf16[16,16,128]{2,1,0:T(8,128)(2,1)S(1)} all-to-all(bf16[16,16,128]{2,1,0:T(8,128)(2,1)S(1)} %bitcast.25), channel_id=1, replica_groups=mesh['z'=16,'core'=2,'tp_0'=4,'tp_1'=4] {'tp_0','tp_1'}, dimensions={0} | all-to-all | bytes 131072 | tf_op jit(solution)/shard_map/all_to_all | solution.py:379
  177.2 0.6 copy_bitcast_fusion
Async XLA Ops:
  1.3 3.4 %collective-permute-start = (bf16[128,128]{1,0:T(8,128)(2,1)S(1)}, bf16[128,128]{1,0:T(8,128)(2,1)S(1)}, u32[]{:S(2)}, u32[]{:S(2)}) collective-permute-start(bf16[128,128]{1,0:T(8,128)(2,1)S(1)} %get-tuple-element.22), channel_id=1, source_target_pairs={{0,16},{16,32},{32,48},{48,64},{64,80},{80,96},{96,112},{112,128},... | collective-permute-start | bytes 98312 | tf_op jit(solution)/shard_map/ppermute | solution.py:362
  78.6 25.0 %copy-start = (bf16[1,2048,256]{2,1,0:T(8,128)(2,1)S(1)}, bf16[1,2048,256]{2,1,0:T(8,128)(2,1)}, u32[]{:S(2)}) copy-start(bf16[1,2048,256]{2,1,0:T(8,128)(2,1)} %gate_ref.1) | copy-start | bytes 3145732
  78.6 24.9 %copy-start.1 = (bf16[1,2048,256]{2,1,0:T(8,128)(2,1)S(1)}, bf16[1,2048,256]{2,1,0:T(8,128)(2,1)}, u32[]{:S(2)}) copy-start(bf16[1,2048,256]{2,1,0:T(8,128)(2,1)} %up_ref.1) | copy-start | bytes 3145732
  78.6 24.9 %copy-start.2 = (bf16[1,256,2048]{2,1,0:T(8,128)(2,1)S(1)}, bf16[1,256,2048]{2,1,0:T(8,128)(2,1)}, u32[]{:S(2)}) copy-start(bf16[1,256,2048]{2,1,0:T(8,128)(2,1)} %down_ref.1) | copy-start | bytes 3145732
  78.7 24.9 %copy-start.3 = (f32[2048]{0:T(1024)S(1)}, f32[2048]{0:T(1024)}, u32[]{:S(2)}) copy-start(f32[2048]{0:T(1024)} %param.18) | copy-start | bytes 24580

commit v10 on v9

--- a/solution.py
+++ b/solution.py
@@ -156,9 +156,11 @@
     k_ref, v_ref, sinks_smem, sems = refs[16:]
     k_hbm, v_hbm, q_hbm, w_hbm, sinks_hbm, routes_hbm, weights_hbm, stream_hbm = sources
     first_col = pl.multiple_of(lax.axis_index(TP) * LANES, LANES)
+    group = lax.axis_index(TP) * (q_ref.shape[1] // HEAD_DIM) // REP
+    heads = pl.ds(pl.multiple_of(group // 2 * LANES, LANES), LANES)
     pairs = (
-        (k_hbm, k_ref),
-        (v_hbm, v_ref),
+        (k_hbm.at[:, heads], k_ref),
+        (v_hbm.at[:, heads], v_ref),
         (q_hbm, q_ref),
         (w_hbm, w_ref),
         (sinks_hbm, sinks_smem),
@@ -169,14 +171,11 @@
     copies = [pltpu.make_async_copy(source, target, sems.at[i]) for i, (source, target) in enumerate(pairs)]
     for copy in copies:
         copy.start()
-    group = lax.axis_index(TP) * (q_ref.shape[1] // HEAD_DIM) // REP
     low = lax.broadcasted_iota(jnp.int32, kv_ref.shape, 1) < HEAD_DIM
 
     def head(ref):
-        picked = ref[:, :LANES].astype(F32)
-        for c in range(LANES, ref.shape[1], LANES):
-            picked = jnp.where(group // 2 == c // LANES, ref[:, c : c + LANES].astype(F32), picked)
-        return picked, jnp.concatenate([picked[:, HEAD_DIM:], picked[:, :HEAD_DIM]], axis=1)
+        both = ref[...].astype(F32)
+        return both, jnp.concatenate([both[:, HEAD_DIM:], both[:, :HEAD_DIM]], axis=1)
 
     copies[0].wait()
     key, key_swapped = head(k_ref)
@@ -210,8 +209,8 @@
         in_specs=[pl.BlockSpec(memory_space=pltpu.HBM)] * 8,
         out_specs=(VMEM_SPEC,) * 8,
         scratch_shapes=[
-            pltpu.VMEM(k.shape, BF16),
-            pltpu.VMEM(v.shape, BF16),
+            pltpu.VMEM((rows, LANES), BF16),
+            pltpu.VMEM((rows, LANES), BF16),
             pltpu.SMEM(sinks.shape, F32),
             pltpu.SemaphoreType.DMA((8,)),
         ],

time: 178 us -> 178 us (level)
  no operation moved by 1% of the time
where the time goes in v10:
time: 178 us
  blocking collectives  167 us (94%)
  Pallas kernels  8.42 us (5%)
    all_to_all x4, blocking collectives, along(): lax.all_to_all(parts, PLANES, split_axis=0, concat_axis=0, axis_index_gro...  73.2 us
    all_to_all x1, blocking collectives, per_device(): lax.all_to_all(rows.reshape(experts, cap, LANES), SP, split_axis=0, conca...  35.2 us
    all_to_all x1, blocking collectives, per_device(): lax.all_to_all(partial, TP, split_axis=0, concat_axis=0, tiled=True)  25 us
    all_to_all x1, blocking collectives, per_device(): lax.all_to_all(summed.reshape(experts, cap, LANES), SP, split_axis=0, con...  22.9 us
    all_to_all x1, blocking collectives, per_device(): return lax.all_to_all(out, TP, split_axis=0, concat_axis=1, tiled=True)  10.6 us
  transfers between devices with their start and end apart: 1, of which 0 were waited for; matrix products, arithmetic and copies ran while one was open for 0% of the time, Pallas kernels for 1%

profile of v10, /device:TPU:2, one launch (start us, length us, event | category | flops | bytes accessed | tf_op | source)
XLA Modules:
  0.0 177.9 jit_solution(18004031771521023941)
XLA Ops:
  0.0 1.2 load.1
  1.2 1.7 collective-permute-start
  3.0 1.6 later_and_slots.1
  4.6 0.0 collective-permute-done.before_ref
  4.6 1.2 attention_first.1
  5.8 25.0 %all_to_all.54.arrived_ref = bf16[16,256,128]{2,1,0:T(8,128)(2,1)S(1)} all-to-all(bf16[16,256,128]{2,1,0:T(8,128)(2,1)S(1)} %attention_first.1), channel_id=1, replica_groups=mesh['z'=16,'core'=2,'tp_0'=4,'tp_1'=4] {'tp_0','tp_1'}, dimensions={0} | all-to-all | bytes 2097152 | tf_op jit(solution)/shard_map/all_to_all | solution.py:364
  30.8 0.4 stream.1
  31.1 35.2 %all_to_all.55 = bf16[32,24,128]{2,1,0:T(8,128)(2,1)S(1)} all-to-all(bf16[32,24,128]{2,1,0:T(8,128)(2,1)S(1)} %bitcast.26), channel_id=1, replica_groups=mesh['z'=16,'core'=2,'tp_0'=4,'tp_1'=4] {'z','core'}, dimensions={0} | all-to-all | bytes 393216 | tf_op jit(solution)/shard_map/all_to_all | solution.py:366
  66.3 0.1 copies.2
  66.5 11.8 %all_to_all.56 = bf16[4,768,128]{2,1,0:T(8,128)(2,1)S(1)} all-to-all(bf16[4,768,128]{2,1,0:T(8,128)(2,1)S(1)} %copies.2), channel_id=1, replica_groups={{0,1,2,3},{4,5,6,7},{8,9,10,11},{12,13,14,15},{16,20,24,28},{17,21,25,2..., dimensions={0} | all-to-all | bytes 1572864 | tf_op jit(solution)/shard_map/all_to_all | solution.py:337
  78.2 0.4 copies.3
  78.6 0.0 copy-start
  78.7 0.0 copy-start.1
  78.7 0.0 copy-start.2
  78.7 0.0 copy-start.3
  78.7 24.9 %all_to_all.57 = bf16[4,3072,128]{2,1,0:T(8,128)(2,1)S(1)} all-to-all(bf16[4,3072,128]{2,1,0:T(8,128)(2,1)S(1)} %copies.3), channel_id=1, replica_groups={{0,4,8,12},{1,5,9,13},{2,6,10,14},{3,7,11,15},{16,17,18,19},{20,21,22,2..., dimensions={0} | all-to-all | bytes 6291456 | tf_op jit(solution)/shard_map/all_to_all | solution.py:337
  103.6 0.0 copy-done
  103.6 0.0 copy-done.1
  103.6 0.0 copy-done.2
  103.6 0.0 copy-done.3
  103.6 2.6 %expert.1 = bf16[16,768,128]{2,1,0:T(8,128)(2,1)S(1)} custom-call(bf16[16,768,128]{2,1,0:T(8,128)(2,1)S(1)} %bitcast.18, f32[1,2048]{1,0:T(1,128)S(1)} %bitcast.27, bf16[1,2048,256]{2,1,0:T(8,128)(2,1)S(1)} %copy-done, bf16[1,2048,256]{2,1,0:T(8,128)(2,1)S(1)} %copy-done.1, bf16[1,256,2048]{2,1,0:T(8,128)(2,1)S(1)} %copy-done.2), custom_call_target="tpu_custom_call" | custom-call | flops 2415919104 | bytes 6291456 | tf_op jit(solution)/shard_map/expert/pallas_call | solution.py:298
  106.3 24.6 %all_to_all.58.parts_ref = bf16[4,3072,128]{2,1,0:T(8,128)(2,1)S(1)} all-to-all(bf16[4,3072,128]{2,1,0:T(8,128)(2,1)S(1)} %bitcast.19), channel_id=1, replica_groups={{0,4,8,12},{1,5,9,13},{2,6,10,14},{3,7,11,15},{16,17,18,19},{20,21,22,2..., dimensions={0} | all-to-all | bytes 6291456 | tf_op jit(solution)/shard_map/all_to_all | solution.py:337
  130.9 0.4 total.2
  131.3 11.9 %all_to_all.59.parts_ref = bf16[4,768,128]{2,1,0:T(8,128)(2,1)S(1)} all-to-all(bf16[4,768,128]{2,1,0:T(8,128)(2,1)S(1)} %bitcast.21), channel_id=1, replica_groups={{0,1,2,3},{4,5,6,7},{8,9,10,11},{12,13,14,15},{16,20,24,28},{17,21,25,2..., dimensions={0} | all-to-all | bytes 1572864 | tf_op jit(solution)/shard_map/all_to_all | solution.py:337
  143.2 0.1 total.3
  143.3 22.9 %all_to_all.60 = bf16[32,24,128]{2,1,0:T(8,128)(2,1)S(1)} all-to-all(bf16[32,24,128]{2,1,0:T(8,128)(2,1)S(1)} %bitcast.24), channel_id=1, replica_groups=mesh['z'=16,'core'=2,'tp_0'=4,'tp_1'=4] {'z','core'}, dimensions={0} | all-to-all | bytes 393216 | tf_op jit(solution)/shard_map/all_to_all | solution.py:376
  166.3 0.4 combine.1
  166.6 10.6 %all_to_all.61 = bf16[16,16,128]{2,1,0:T(8,128)(2,1)S(1)} all-to-all(bf16[16,16,128]{2,1,0:T(8,128)(2,1)S(1)} %bitcast.25), channel_id=1, replica_groups=mesh['z'=16,'core'=2,'tp_0'=4,'tp_1'=4] {'tp_0','tp_1'}, dimensions={0} | all-to-all | bytes 131072 | tf_op jit(solution)/shard_map/all_to_all | solution.py:378
  177.2 0.6 copy_bitcast_fusion
Async XLA Ops:
  1.2 3.4 %collective-permute-start = (bf16[128,128]{1,0:T(8,128)(2,1)S(1)}, bf16[128,128]{1,0:T(8,128)(2,1)S(1)}, u32[]{:S(2)}, u32[]{:S(2)}) collective-permute-start(bf16[128,128]{1,0:T(8,128)(2,1)S(1)} %get-tuple-element.22), channel_id=1, source_target_pairs={{0,16},{16,32},{32,48},{48,64},{64,80},{80,96},{96,112},{112,128},... | collective-permute-start | bytes 98312 | tf_op jit(solution)/shard_map/ppermute | solution.py:361
  78.6 25.0 %copy-start = (bf16[1,2048,256]{2,1,0:T(8,128)(2,1)S(1)}, bf16[1,2048,256]{2,1,0:T(8,128)(2,1)}, u32[]{:S(2)}) copy-start(bf16[1,2048,256]{2,1,0:T(8,128)(2,1)} %gate_ref.1) | copy-start | bytes 3145732
  78.7 24.9 %copy-start.1 = (bf16[1,2048,256]{2,1,0:T(8,128)(2,1)S(1)}, bf16[1,2048,256]{2,1,0:T(8,128)(2,1)}, u32[]{:S(2)}) copy-start(bf16[1,2048,256]{2,1,0:T(8,128)(2,1)} %up_ref.1) | copy-start | bytes 3145732
  78.7 24.9 %copy-start.2 = (bf16[1,256,2048]{2,1,0:T(8,128)(2,1)S(1)}, bf16[1,256,2048]{2,1,0:T(8,128)(2,1)}, u32[]{:S(2)}) copy-start(bf16[1,256,2048]{2,1,0:T(8,128)(2,1)} %down_ref.1) | copy-start | bytes 3145732
  78.7 24.9 %copy-start.3 = (f32[2048]{0:T(1024)S(1)}, f32[2048]{0:T(1024)}, u32[]{:S(2)}) copy-start(f32[2048]{0:T(1024)} %param.18) | copy-start | bytes 24580

commit v11 on v10

--- a/solution.py
+++ b/solution.py
@@ -238,7 +238,7 @@
 
 def total_body(parts_ref, out_ref):
     rows = parts_ref.shape[1]
-    block = 128
+    block = 256
     for lo in range(0, rows, block):
         summed = parts_ref[0, lo : lo + block, :].astype(F32)
         for t in range(1, parts_ref.shape[0]):

time: 178 us -> 178 us (level)
  no operation moved by 1% of the time
where the time goes in v11:
time: 178 us
  blocking collectives  167 us (94%)
  Pallas kernels  8.42 us (5%)
    all_to_all x4, blocking collectives, along(): lax.all_to_all(parts, PLANES, split_axis=0, concat_axis=0, axis_index_gro...  73.2 us
    all_to_all x1, blocking collectives, per_device(): lax.all_to_all(rows.reshape(experts, cap, LANES), SP, split_axis=0, conca...  35.2 us
    all_to_all x1, blocking collectives, per_device(): lax.all_to_all(partial, TP, split_axis=0, concat_axis=0, tiled=True)  25 us
    all_to_all x1, blocking collectives, per_device(): lax.all_to_all(summed.reshape(experts, cap, LANES), SP, split_axis=0, con...  22.9 us
    all_to_all x1, blocking collectives, per_device(): return lax.all_to_all(out, TP, split_axis=0, concat_axis=1, tiled=True)  10.6 us
  transfers between devices with their start and end apart: 1, of which 0 were waited for; matrix products, arithmetic and copies ran while one was open for 0% of the time, Pallas kernels for 1%

profile of v11, /device:TPU:2, one launch (start us, length us, event | category | flops | bytes accessed | tf_op | source)
XLA Modules:
  0.0 177.9 jit_solution(18004031771521023941)
XLA Ops:
  0.0 1.2 load.1
  1.2 1.7 collective-permute-start
  3.0 1.6 later_and_slots.1
  4.6 0.0 collective-permute-done.before_ref
  4.6 1.2 attention_first.1
  5.8 25.0 %all_to_all.54.arrived_ref = bf16[16,256,128]{2,1,0:T(8,128)(2,1)S(1)} all-to-all(bf16[16,256,128]{2,1,0:T(8,128)(2,1)S(1)} %attention_first.1), channel_id=1, replica_groups=mesh['z'=16,'core'=2,'tp_0'=4,'tp_1'=4] {'tp_0','tp_1'}, dimensions={0} | all-to-all | bytes 2097152 | tf_op jit(solution)/shard_map/all_to_all | solution.py:364
  30.8 0.4 stream.1
  31.1 35.2 %all_to_all.55 = bf16[32,24,128]{2,1,0:T(8,128)(2,1)S(1)} all-to-all(bf16[32,24,128]{2,1,0:T(8,128)(2,1)S(1)} %bitcast.26), channel_id=1, replica_groups=mesh['z'=16,'core'=2,'tp_0'=4,'tp_1'=4] {'z','core'}, dimensions={0} | all-to-all | bytes 393216 | tf_op jit(solution)/shard_map/all_to_all | solution.py:366
  66.3 0.1 copies.2
  66.5 11.8 %all_to_all.56 = bf16[4,768,128]{2,1,0:T(8,128)(2,1)S(1)} all-to-all(bf16[4,768,128]{2,1,0:T(8,128)(2,1)S(1)} %copies.2), channel_id=1, replica_groups={{0,1,2,3},{4,5,6,7},{8,9,10,11},{12,13,14,15},{16,20,24,28},{17,21,25,2..., dimensions={0} | all-to-all | bytes 1572864 | tf_op jit(solution)/shard_map/all_to_all | solution.py:337
  78.2 0.4 copies.3
  78.6 0.0 copy-start
  78.7 0.0 copy-start.1
  78.7 0.0 copy-start.2
  78.7 0.0 copy-start.3
  78.7 24.9 %all_to_all.57 = bf16[4,3072,128]{2,1,0:T(8,128)(2,1)S(1)} all-to-all(bf16[4,3072,128]{2,1,0:T(8,128)(2,1)S(1)} %copies.3), channel_id=1, replica_groups={{0,4,8,12},{1,5,9,13},{2,6,10,14},{3,7,11,15},{16,17,18,19},{20,21,22,2..., dimensions={0} | all-to-all | bytes 6291456 | tf_op jit(solution)/shard_map/all_to_all | solution.py:337
  103.6 0.0 copy-done
  103.6 0.0 copy-done.1
  103.6 0.0 copy-done.2
  103.6 0.0 copy-done.3
  103.6 2.6 %expert.1 = bf16[16,768,128]{2,1,0:T(8,128)(2,1)S(1)} custom-call(bf16[16,768,128]{2,1,0:T(8,128)(2,1)S(1)} %bitcast.18, f32[1,2048]{1,0:T(1,128)S(1)} %bitcast.27, bf16[1,2048,256]{2,1,0:T(8,128)(2,1)S(1)} %copy-done, bf16[1,2048,256]{2,1,0:T(8,128)(2,1)S(1)} %copy-done.1, bf16[1,256,2048]{2,1,0:T(8,128)(2,1)S(1)} %copy-done.2), custom_call_target="tpu_custom_call" | custom-call | flops 2415919104 | bytes 6291456 | tf_op jit(solution)/shard_map/expert/pallas_call | solution.py:298
  106.3 24.6 %all_to_all.58.parts_ref = bf16[4,3072,128]{2,1,0:T(8,128)(2,1)S(1)} all-to-all(bf16[4,3072,128]{2,1,0:T(8,128)(2,1)S(1)} %bitcast.19), channel_id=1, replica_groups={{0,4,8,12},{1,5,9,13},{2,6,10,14},{3,7,11,15},{16,17,18,19},{20,21,22,2..., dimensions={0} | all-to-all | bytes 6291456 | tf_op jit(solution)/shard_map/all_to_all | solution.py:337
  130.9 0.4 total.2
  131.3 11.9 %all_to_all.59.parts_ref = bf16[4,768,128]{2,1,0:T(8,128)(2,1)S(1)} all-to-all(bf16[4,768,128]{2,1,0:T(8,128)(2,1)S(1)} %bitcast.21), channel_id=1, replica_groups={{0,1,2,3},{4,5,6,7},{8,9,10,11},{12,13,14,15},{16,20,24,28},{17,21,25,2..., dimensions={0} | all-to-all | bytes 1572864 | tf_op jit(solution)/shard_map/all_to_all | solution.py:337
  143.2 0.1 total.3
  143.3 22.9 %all_to_all.60 = bf16[32,24,128]{2,1,0:T(8,128)(2,1)S(1)} all-to-all(bf16[32,24,128]{2,1,0:T(8,128)(2,1)S(1)} %bitcast.24), channel_id=1, replica_groups=mesh['z'=16,'core'=2,'tp_0'=4,'tp_1'=4] {'z','core'}, dimensions={0} | all-to-all | bytes 393216 | tf_op jit(solution)/shard_map/all_to_all | solution.py:376
  166.3 0.4 combine.1
  166.6 10.6 %all_to_all.61 = bf16[16,16,128]{2,1,0:T(8,128)(2,1)S(1)} all-to-all(bf16[16,16,128]{2,1,0:T(8,128)(2,1)S(1)} %bitcast.25), channel_id=1, replica_groups=mesh['z'=16,'core'=2,'tp_0'=4,'tp_1'=4] {'tp_0','tp_1'}, dimensions={0} | all-to-all | bytes 131072 | tf_op jit(solution)/shard_map/all_to_all | solution.py:378
  177.2 0.6 copy_bitcast_fusion
Async XLA Ops:
  1.2 3.4 %collective-permute-start = (bf16[128,128]{1,0:T(8,128)(2,1)S(1)}, bf16[128,128]{1,0:T(8,128)(2,1)S(1)}, u32[]{:S(2)}, u32[]{:S(2)}) collective-permute-start(bf16[128,128]{1,0:T(8,128)(2,1)S(1)} %get-tuple-element.22), channel_id=1, source_target_pairs={{0,16},{16,32},{32,48},{48,64},{64,80},{80,96},{96,112},{112,128},... | collective-permute-start | bytes 98312 | tf_op jit(solution)/shard_map/ppermute | solution.py:361
  78.6 25.0 %copy-start = (bf16[1,2048,256]{2,1,0:T(8,128)(2,1)S(1)}, bf16[1,2048,256]{2,1,0:T(8,128)(2,1)}, u32[]{:S(2)}) copy-start(bf16[1,2048,256]{2,1,0:T(8,128)(2,1)} %gate_ref.1) | copy-start | bytes 3145732
  78.7 24.9 %copy-start.1 = (bf16[1,2048,256]{2,1,0:T(8,128)(2,1)S(1)}, bf16[1,2048,256]{2,1,0:T(8,128)(2,1)}, u32[]{:S(2)}) copy-start(bf16[1,2048,256]{2,1,0:T(8,128)(2,1)} %up_ref.1) | copy-start | bytes 3145732
  78.7 24.9 %copy-start.2 = (bf16[1,256,2048]{2,1,0:T(8,128)(2,1)S(1)}, bf16[1,256,2048]{2,1,0:T(8,128)(2,1)}, u32[]{:S(2)}) copy-start(bf16[1,256,2048]{2,1,0:T(8,128)(2,1)} %down_ref.1) | copy-start | bytes 3145732
  78.7 24.9 %copy-start.3 = (f32[2048]{0:T(1024)S(1)}, f32[2048]{0:T(1024)}, u32[]{:S(2)}) copy-start(f32[2048]{0:T(1024)} %param.18) | copy-start | bytes 24580
